TPU v7x, 512 devices: a whole 4x4x16 slice. The times are simulated.
512 devices in a mesh: ep: 128 (over z, x, core), tp: 4 (over y).
Axes of the slice: x: 4, y: 4, z: 16, core: 2. Of those that a mesh axis runs over, the one named last changes fastest.
Arguments:
- hidden_in: bfloat16 [2048, 1024], P('ep', 'tp'), may hold values from -40 to 40
- norm_gain_attn: float32 [1024], replicated, may hold values from 0.1 to 1.9
- query_weight: bfloat16 [1024, 512], P(None, 'tp'), may hold values from -0.1875 to 0.1875
- key_weight: bfloat16 [1024, 512], P(None, 'tp'), may hold values from -0.1875 to 0.1875
- value_weight: bfloat16 [1024, 512], P(None, 'tp'), may hold values from -0.1875 to 0.1875
- query_gain: float32 [128], replicated, may hold values from 1 to 1.6
- key_gain: float32 [128], replicated, may hold values from 1 to 1.6
- lambda_head: float32 [4], P('tp'), may hold values from 0.3 to 0.8
- sub_gain: float32 [128], replicated, may hold values from 0.1 to 1.9
- out_weight: bfloat16 [512, 1024], P('tp'), may hold values from -0.25 to 0.25
- cache_key: bfloat16 [2048, 256, 512], P('ep', None, 'tp'), may hold values from -8 to 8
- cache_value: bfloat16 [2048, 256, 512], P('ep', None, 'tp'), may hold values from -6 to 6
- lengths: int32 [2048], P('ep'), may hold values from 1 to 256
- norm_gain_mix: float32 [1024], P('tp'), may hold values from 0.1 to 1.9
- route_ids: int32 [2048, 6], P('ep'), may hold values from 0 to 127, all different within a row; in each aligned block of 16 rows (0 to 15, 16 to 31, ...) at most 2 rows name the same one
- route_logits: float32 [2048, 6], P('ep'), may hold values from -4 to 4
- expert_gate: bfloat16 [128, 1024, 1024], P('ep', None, 'tp'), may hold values from -0.5 to 0.5
- expert_up: bfloat16 [128, 1024, 1024], P('ep', None, 'tp'), may hold values from -0.5 to 0.5
- expert_down: bfloat16 [128, 1024, 1024], P('ep', 'tp'), may hold values from -0.046875 to 0.046875
- dense_gate: bfloat16 [1024, 2048], P('tp', 'ep'), may hold values from -0.1875 to 0.1875
- dense_up: bfloat16 [1024, 2048], P('tp', 'ep'), may hold values from -0.1875 to 0.1875
- dense_down: bfloat16 [2048, 1024], P('ep', 'tp'), may hold values from -0.125 to 0.125
- branch_gate: float32 [1024], P('tp'), may hold values from -0.1875 to 0.1875
Outputs:
- layer_out: bfloat16 [2048, 1024], P('ep', 'tp')
- key_rows: bfloat16 [2048, 512], P('ep', 'tp')
- value_rows: bfloat16 [2048, 512], P('ep', 'tp')
Inputs may be any that keep to these rules, and one draw needn't show every extreme that they name: `route_ids`: each row names 6 different experts. Among the rows of one index of ep (aligned blocks of 16 rows) no expert is named by more than 2 rows, and in some blocks one expert is named by exactly 2.
All inputs are finite; a program needn't handle non-finite values.
Results may differ from a plain program's by a relative error of at most 0.0075.
Values may be sent and summed in bfloat16 or wider, within the bound.
No kernel may reach another device: no remote copies, remote signals or barrier semaphores. Data moves between devices by JAX's collectives and lax.ppermute only.
A program may use at most 64 MiB of HBM per device.

v0:
```python
import math

import jax
import jax.numpy as jnp
from jax import lax
from jax.sharding import Mesh
from jax.sharding import PartitionSpec as P

EP = ("ep_0", "ep_1", "ep_2")


EPSILON = 1e-06
CLAMP_LIMIT = 7.0
SWISH_ALPHA = 1.702
OUT_SCALE = 0.2 + 0.6 * math.exp(-0.6)


def laid_out(blocks, dim):
    blocks = jnp.moveaxis(blocks, 0, dim)
    dims = blocks.shape
    return blocks.reshape(*dims[:dim], dims[dim] * dims[dim + 1], *dims[dim + 2 :])


def from_everyone(x, axis):
    copies = jnp.broadcast_to(x, (lax.axis_size(axis), *x.shape))
    return lax.all_to_all(copies, axis, split_axis=0, concat_axis=0, tiled=True)


def collect(x, axis, dim):
    return laid_out(from_everyone(x, axis), dim)


def cut_along(x, dim, length):
    dims = x.shape
    blocks = x.reshape(*dims[:dim], length, dims[dim] // length, *dims[dim + 1 :])
    return jnp.moveaxis(blocks, dim, 0)


def summed_on_arrival(x, axis, dim):
    length = lax.axis_size(axis)
    blocks = lax.all_to_all(cut_along(x, dim, length), axis, 0, 0, tiled=True)
    return jnp.sum(blocks, axis=0)


def taken_together(x, axis):
    return from_everyone(x, axis).sum(axis=0)


def together(arrays, axis):
    ends = [0]
    for a in arrays:
        ends.append(ends[-1] + a.size)
    subtotal = taken_together(jnp.concatenate([a.ravel() for a in arrays]), axis)
    return tuple((subtotal[b:e].reshape(a.shape) for a, b, e in zip(arrays, ends, ends[1:])))


def gather_turned(arrays, axis, dims):
    turned = [jnp.moveaxis(a, dim, 0) for a, dim in zip(arrays, dims)]
    both = jnp.concatenate([t.reshape(len(t), -1) for t in turned], axis=1)
    whole, at, done = (lax.all_gather(both, axis, axis=0, tiled=True), 0, [])
    for t, dim in zip(turned, dims):
        section = whole[:, at : at + t[0].size].reshape(-1, *t.shape[1:])
        done.append(jnp.moveaxis(section, 0, dim))
        at += t[0].size
    return tuple(done)


def stacked_from(x, axes, sequence):
    blocks = x[None]
    for k in sequence:
        blocks = lax.all_gather(blocks, axes[k], axis=0, tiled=True)
    block = [lax.axis_size(axes[k]) for k in reversed(sequence)]
    blocks = blocks.reshape(*block, *x.shape)
    turned = sorted(range(len(sequence)), key=lambda place: sequence[len(sequence) - 1 - place])
    return blocks.transpose(*turned, *range(len(sequence), blocks.ndim)).reshape(-1, *x.shape)


def whole_of(x, axes, sequence, dim):
    return laid_out(stacked_from(x, axes, sequence), dim)


def rms_scale(values, scale_gain):
    mean_square = jnp.mean(values * values, axis=-1, keepdims=True)
    return values * lax.rsqrt(mean_square + EPSILON) * scale_gain


def clamped_unit(gate_pre, up_pre):
    gate_cut = jnp.minimum(gate_pre, CLAMP_LIMIT)
    up_cut = jnp.clip(up_pre, -CLAMP_LIMIT, CLAMP_LIMIT)
    return (up_cut + 1.0) * gate_cut * jax.nn.sigmoid(SWISH_ALPHA * gate_cut)


def attend(
    normed,
    query_weight,
    key_weight,
    value_weight,
    query_gain,
    key_gain,
    lambda_head,
    sub_gain,
    cache_key,
    cache_value,
    lengths,
):
    seq_count = normed.shape[0]
    head_count = lambda_head.shape[0]
    qk_size = query_gain.shape[0] // 2
    val_size = value_weight.shape[1] // head_count
    cache_len = cache_key.shape[1]
    scale_factor = qk_size ** (-0.5)
    query_pre = jnp.dot(normed, query_weight, preferred_element_type=jnp.float32)
    query_rows = rms_scale(
        query_pre.reshape(seq_count, head_count, 2, qk_size), query_gain.reshape(2, qk_size)
    ).astype(jnp.bfloat16)
    key_pre = jnp.dot(normed, key_weight, preferred_element_type=jnp.float32)
    key_rows = rms_scale(
        key_pre.reshape(seq_count, head_count, 2, qk_size), key_gain.reshape(2, qk_size)
    ).astype(jnp.bfloat16)
    value_rows = jnp.dot(normed, value_weight, preferred_element_type=jnp.float32).astype(
        jnp.bfloat16
    )
    key_past = cache_key.reshape(seq_count, cache_len, head_count, 2, qk_size)
    past_score = (
        jnp.einsum("shmd,sjhmd->shmj", query_rows, key_past, preferred_element_type=jnp.float32)
        * scale_factor
    )
    own_score = (
        jnp.einsum("shmd,shmd->shm", query_rows, key_rows, preferred_element_type=jnp.float32)
        * scale_factor
    )
    valid_mask = lax.iota(jnp.int32, cache_len)[None, :] < lengths[:, None]
    past_exp = jnp.where(valid_mask[:, None, None, :], jnp.exp(past_score), 0.0)
    own_exp = jnp.exp(own_score)
    denominator = jnp.sum(past_exp, axis=-1) + own_exp
    past_prob = past_exp / denominator[..., None]
    own_prob = own_exp / denominator
    weight_past = (past_prob[:, :, 0] - lambda_head[None, :, None] * past_prob[:, :, 1]).astype(
        jnp.bfloat16
    )
    weight_own = (own_prob[:, :, 0] - lambda_head[None, :] * own_prob[:, :, 1]).astype(jnp.bfloat16)
    value_past = cache_value.reshape(seq_count, cache_len, head_count, val_size)
    head_mix = jnp.einsum(
        "shj,sjhe->she", weight_past, value_past, preferred_element_type=jnp.float32
    )
    own_value = value_rows.reshape(seq_count, head_count, val_size).astype(jnp.float32)
    head_mix = head_mix + weight_own.astype(jnp.float32)[..., None] * own_value
    head_out = (rms_scale(head_mix, sub_gain) * OUT_SCALE).astype(jnp.bfloat16)
    return (
        head_out.reshape(seq_count, head_count * val_size),
        key_rows.reshape(seq_count, -1),
        value_rows,
    )


def body(
    hidden_in,
    norm_gain_attn,
    query_weight,
    key_weight,
    value_weight,
    query_gain,
    key_gain,
    lambda_head,
    sub_gain,
    out_weight,
    cache_key,
    cache_value,
    lengths,
    norm_gain_mix,
    route_ids,
    route_logits,
    expert_gate,
    expert_up,
    expert_down,
    dense_gate,
    dense_up,
    dense_down,
    branch_gate,
):
    seq_count, top_count = route_ids.shape
    full_rows = collect(hidden_in, "tp", 1)
    width_total = full_rows.shape[1]
    normed = rms_scale(full_rows.astype(jnp.float32), norm_gain_attn).astype(jnp.bfloat16)
    head_out, key_rows, value_rows = attend(
        normed,
        query_weight,
        key_weight,
        value_weight,
        query_gain,
        key_gain,
        lambda_head,
        sub_gain,
        cache_key,
        cache_value,
        lengths,
    )
    head_terms = jnp.dot(head_out, out_weight, preferred_element_type=jnp.float32)
    attn_part = summed_on_arrival(head_terms, "tp", 1)
    residual = hidden_in.astype(jnp.float32) + attn_part
    square_sum, gate_raw = together(
        (
            jnp.sum(residual * residual, axis=1),
            jnp.sum(residual * (norm_gain_mix * branch_gate)[None, :], axis=1),
        ),
        "tp",
    )
    inverse = lax.rsqrt(square_sum / width_total + EPSILON)
    mix_float = residual * inverse[:, None] * norm_gain_mix[None, :]
    gate_logit = gate_raw * inverse
    branch_weight = jax.nn.sigmoid(gate_logit)[:, None]
    mix_rows = mix_float.astype(jnp.bfloat16)
    route_weight = jax.nn.softmax(route_logits, axis=1)
    experts = lax.axis_size(EP) * expert_gate.shape[0]
    capacity = min(seq_count, 2 * ((seq_count * top_count + experts - 1) // experts))
    flat_ids = route_ids.reshape(-1)
    one_hot = (flat_ids[:, None] == lax.iota(jnp.int32, experts)[None, :]).astype(jnp.int32)
    route_rank = jnp.sum((jnp.cumsum(one_hot, axis=0) - one_hot) * one_hot, axis=1)
    slot_index = flat_ids * capacity + route_rank
    select_matrix = (
        lax.iota(jnp.int32, experts * capacity)[:, None] == slot_index[None, :]
    ).astype(jnp.bfloat16)
    route_rows = jnp.repeat(mix_rows, top_count, axis=0)
    placed = jnp.dot(select_matrix, route_rows, preferred_element_type=jnp.float32)
    arrived = collect(
        lax.all_to_all(
            placed.astype(jnp.bfloat16).reshape(experts, capacity, mix_rows.shape[1]),
            EP,
            split_axis=0,
            concat_axis=0,
            tiled=True,
        ),
        "tp",
        2,
    )
    source_count, item_count, width_now = arrived.shape
    flat_rows = arrived.reshape(source_count * item_count, width_now)
    gate_pre = jnp.dot(flat_rows, expert_gate[0], preferred_element_type=jnp.float32)
    up_pre = jnp.dot(flat_rows, expert_up[0], preferred_element_type=jnp.float32)
    activation = clamped_unit(gate_pre, up_pre).astype(jnp.bfloat16)
    partial_out = jnp.dot(activation, expert_down[0], preferred_element_type=jnp.float32)
    partial_out = partial_out.reshape(source_count, item_count, width_now)
    summed = summed_on_arrival(partial_out, "tp", 2).astype(jnp.bfloat16)
    returned = lax.all_to_all(summed, EP, split_axis=0, concat_axis=0, tiled=True)
    local_width = returned.shape[2]
    route_out = jnp.dot(
        select_matrix.T,
        returned.reshape(experts * capacity, local_width),
        preferred_element_type=jnp.float32,
    )
    routed = jnp.sum(
        route_out.reshape(seq_count, top_count, local_width) * route_weight[:, :, None], axis=1
    )
    pieces = gather_turned((dense_gate, dense_up), EP, (1, 1))
    gate_block = jnp.dot(mix_rows, pieces[0], preferred_element_type=jnp.float32)
    up_block = jnp.dot(mix_rows, pieces[1], preferred_element_type=jnp.float32)
    gate_full, up_full = together((gate_block, up_block), "tp")
    own_act = (jax.nn.silu(gate_full) * up_full).astype(jnp.bfloat16)
    dense_result = jnp.dot(
        own_act, whole_of(dense_down, EP, (1, 0, 2), 0), preferred_element_type=jnp.float32
    )
    layer_out = (residual + routed + branch_weight * dense_result).astype(jnp.bfloat16)
    return (layer_out, key_rows, value_rows)


def solution(mesh):
    split = Mesh(mesh.devices.reshape(16, 4, 2, mesh.shape["tp"]), ("ep_0", "ep_1", "ep_2", "tp"))
    in_specs = (
        P(EP, "tp"),
        P(),
        P(None, "tp"),
        P(None, "tp"),
        P(None, "tp"),
        P(),
        P(),
        P("tp"),
        P(),
        P("tp", None),
        P(EP, None, "tp"),
        P(EP, None, "tp"),
        P(EP),
        P("tp"),
        P(EP, None),
        P(EP, None),
        P(EP, None, "tp"),
        P(EP, None, "tp"),
        P(EP, "tp", None),
        P("tp", EP),
        P("tp", EP),
        P(EP, "tp"),
        P("tp"),
    )
    out_specs = (P(EP, "tp"), P(EP, "tp"), P(EP, "tp"))
    return jax.shard_map(body, mesh=split, in_specs=in_specs, out_specs=out_specs, check_vma=False)
```

profile of v0, /device:TPU:32, one launch (start us, length us, event | category | flops | bytes accessed | tf_op | source)
XLA Modules:
  0.0 202.3 jit_solution(13070366693453311810)
XLA Ops:
  7.2 1.4 broadcast_in_dim.25
  8.6 4.5 %all-to-all-start = ((bf16[4,16,256]{2,1,0:T(8,128)(2,1)}), bf16[4,16,256]{2,1,0:T(8,128)(2,1)S(1)}, u32[]{:S(2)}, u32[]{:S(2)}) async-start(bf16[4,16,256]{2,1,0:T(8,128)(2,1)} %broadcast_in_dim.25), calls=%async_computation | async-start | bytes 65536 | tf_op jit(solution)/shard_map/all_to_all | solution.py:26
  13.1 1.3 pad_maximum_fusion.1
  14.5 0.8 copy.83
  15.4 0.7 iota_compare_fusion.4
  16.1 0.7 mul.280
  16.9 0.7 mul.289
  17.6 1.5 copy.81
  19.7 0.2 copy.104
  21.2 0.2 fusion.22
  21.5 0.2 fusion.25
  22.0 0.2 fusion.23
  22.2 1.2 multiply_reduce_fusion.2
  23.5 0.8 convolution_bitcast_fusion.3
  24.3 4.8 %all-to-all-start.1 = ((f32[4,16,256]{2,1,0:T(8,128)}), f32[4,16,256]{2,1,0:T(8,128)S(1)}, u32[]{:S(2)}, u32[]{:S(2)}) async-start(f32[4,16,256]{2,1,0:T(8,128)} %convolution_bitcast_fusion.3), calls=%async_computation.1 | async-start | bytes 131072 | tf_op jit(solution)/shard_map/all_to_all | solution.py:41
  29.1 0.2 select_reduce_fusion
  29.3 5.4 %all-to-all-done.1 = f32[4,16,256]{2,1,0:T(8,128)S(1)} async-done(((f32[4,16,256]{2,1,0:T(8,128)}), f32[4,16,256]{2,1,0:T(8,128)S(1)}, u32[]{:S(2)}, u32[]{:S(2)}) %all-to-all-start.1) | async-done | bytes 65568 | tf_op jit(solution)/shard_map/all_to_all | solution.py:41
  34.9 0.6 broadcast_in_dim.27
  35.5 3.2 %all-to-all-start.2 = ((f32[4,1,32]{2,1,0:T(1,128)}), f32[4,1,32]{2,1,0:T(1,128)S(1)}, u32[]{:S(2)}, u32[]{:S(2)}) async-start(f32[4,1,32]{2,1,0:T(1,128)} %broadcast_in_dim.27), calls=%async_computation.2 | async-start | bytes 4096 | tf_op jit(solution)/shard_map/all_to_all | solution.py:26
  38.8 5.2 %all-to-all-done.2 = f32[4,1,32]{2,1,0:T(1,128)S(1)} async-done(((f32[4,1,32]{2,1,0:T(1,128)}), f32[4,1,32]{2,1,0:T(1,128)S(1)}, u32[]{:S(2)}, u32[]{:S(2)}) %all-to-all-start.2) | async-done | bytes 544 | tf_op jit(solution)/shard_map/all_to_all | solution.py:26
  44.2 0.2 convolution_convert_fusion
  44.4 36.1 %all_to_all.42 = bf16[128,2,256]{2,1,0:T(2,128)(2,1)S(1)} all-to-all(bf16[128,2,256]{2,1,0:T(2,128)(2,1)S(1)} %reshape.305), channel_id=1, replica_groups=mesh['ep_0'=16,'ep_1'=4,'ep_2'=2,'tp'=4] {'ep_0','ep_1','ep_2'}, dimensions={0} | all-to-all | bytes 262144 | tf_op jit(solution)/shard_map/all_to_all | solution.py:226
  80.5 1.1 broadcast_in_dim.29
  81.6 3.6 %all-to-all-start.4 = ((bf16[4,128,2,256]{3,2,1,0:T(2,128)(2,1)}), bf16[4,128,2,256]{3,2,1,0:T(2,128)(2,1)S(1)}, u32[]{:S(2)}, u32[]{:S(2)}) async-start(bf16[4,128,2,256]{3,2,1,0:T(2,128)(2,1)} %broadcast_in_dim.29), calls=%async_computation.4 | async-start | bytes 1048576 | tf_op jit(solution)/shard_map/all_to_all | solution.py:26
  85.2 0.2 copy.107
  85.4 9.8 %all-to-all-done.4 = bf16[4,128,2,256]{3,2,1,0:T(2,128)(2,1)S(1)} async-done(((bf16[4,128,2,256]{3,2,1,0:T(2,128)(2,1)}), bf16[4,128,2,256]{3,2,1,0:T(2,128)(2,1)S(1)}, u32[]{:S(2)}, u32[]{:S(2)}) %all-to-all-start.4) | async-done | bytes 524320 | tf_op jit(solution)/shard_map/all_to_all | solution.py:26
  95.2 0.7 copy.85
  96.0 0.3 convolution_minimum_fusion
  96.3 0.3 fusion.3
  96.7 0.3 convolution_bitcast_fusion
  97.1 1.1 copy.88
  98.1 3.5 %all-to-all-start.5 = ((f32[4,128,2,256]{3,1,2,0:T(8,128)}), f32[4,128,2,256]{3,1,2,0:T(8,128)S(1)}, u32[]{:S(2)}, u32[]{:S(2)}) async-start(f32[4,128,2,256]{3,1,2,0:T(8,128)} %copy.88), calls=%async_computation.5 | async-start | bytes 2097152 | tf_op jit(solution)/shard_map/all_to_all | solution.py:41
  101.7 11.9 %all-gather = bf16[64,256]{1,0:T(8,128)(2,1)S(1)} all-gather(bf16[16,256]{1,0:T(8,128)(2,1)S(1)} %copy-done.8), channel_id=2, replica_groups=mesh['ep_0'=16,'ep_1'=4,'ep_2'=2,'tp'=4] {'ep_1'}, dimensions={0}, use_global_device_ids=true | all-gather | bytes 40960 | tf_op jit(solution)/shard_map/all_gather | solution.py:71
  113.6 31.7 %all_gather.14 = bf16[64,16,256]{2,1,0:T(8,128)(2,1)} all-gather(bf16[4,16,256]{2,1,0:T(8,128)(2,1)S(1)} %bitcast.104), channel_id=1, replica_groups=mesh['ep_0'=16,'ep_1'=4,'ep_2'=2,'tp'=4] {'ep_0'}, dimensions={0}, use_global_device_ids=true | all-gather | bytes 557056 | tf_op jit(solution)/shard_map/all_gather | solution.py:71
  145.4 0.8 copy.90
  146.2 8.6 %all-to-all-start.6 = ((bf16[128,2,256]{2,1,0:T(2,128)(2,1)}), bf16[128,2,256]{2,1,0:T(2,128)(2,1)S(1)}, u32[]{:S(2)}, u32[]{:S(2)}) async-start(bf16[128,2,256]{2,1,0:T(2,128)(2,1)} %copy.90), calls=%async_computation.6 | async-start | bytes 262144 | tf_op jit(solution)/shard_map/all_to_all | solution.py:244
  154.9 6.9 %all-gather.4.cloned.1.call-done = bf16[2048,512]{1,0:T(8,128)(2,1)} async-done(((bf16[16,512]{1,0:T(8,128)(2,1)}), bf16[2048,512]{1,0:T(8,128)(2,1)}) %all-gather.4.cloned.1.call-update) | async-done | bytes 2097168 | tf_op jit(solution)/shard_map/all_gather | solution.py:60
  161.8 1.6 convolution_bitcast_fusion.2
  163.4 1.6 convolution_bitcast_fusion.1
  165.1 6.8 %all-to-all-done.6 = bf16[128,2,256]{2,1,0:T(2,128)(2,1)S(1)} async-done(((bf16[128,2,256]{2,1,0:T(2,128)(2,1)}), bf16[128,2,256]{2,1,0:T(2,128)(2,1)S(1)}, u32[]{:S(2)}, u32[]{:S(2)}) %all-to-all-start.6) | async-done | bytes 131104 | tf_op jit(solution)/shard_map/all_to_all | solution.py:244
  171.9 1.5 broadcast_in_dim.30
  173.5 4.7 %all-to-all-start.7 = ((f32[4,1,65536]{2,1,0:T(1,128)}), f32[4,1,65536]{2,1,0:T(1,128)S(1)}, u32[]{:S(2)}, u32[]{:S(2)}) async-start(f32[4,1,65536]{2,1,0:T(1,128)} %broadcast_in_dim.30), calls=%async_computation.7 | async-start | bytes 2097152 | tf_op jit(solution)/shard_map/all_to_all | solution.py:26
  178.5 0.6 multiply_convert_fusion.6
  179.1 1.2 all-gather.6.cloned.1.call-done
  180.4 1.3 copy.93
  181.9 11.6 %all-to-all-done.7 = f32[4,1,65536]{2,1,0:T(1,128)S(1)} async-done(((f32[4,1,65536]{2,1,0:T(1,128)}), f32[4,1,65536]{2,1,0:T(1,128)S(1)}, u32[]{:S(2)}, u32[]{:S(2)}) %all-to-all-start.7) | async-done | bytes 1048608 | tf_op jit(solution)/shard_map/all_to_all | solution.py:26
  193.5 1.0 reduce_sum.139
  194.6 0.9 fusion.6
  (91 shorter events, 3.2 us)
Async XLA Ops:
  7.2 14.8 %copy-start = (bf16[16,256,128]{2,1,0:T(8,128)(2,1)S(1)}, bf16[16,256,128]{2,1,0:T(8,128)(2,1)}, u32[]{:S(2)}) copy-start(bf16[16,256,128]{2,1,0:T(8,128)(2,1)} %param.34) | copy-start | bytes 3145732
  7.2 12.6 %copy-start.5 = (bf16[128,1024]{1,0:T(8,128)(2,1)S(1)}, bf16[128,1024]{1,0:T(8,128)(2,1)}, u32[]{:S(2)}) copy-start(bf16[128,1024]{1,0:T(8,128)(2,1)} %param.32) | copy-start | bytes 786436
  7.2 13.1 %copy-start.10 = (f32[1024]{0:T(1024)S(1)}, f32[1024]{0:T(1024)}, u32[]{:S(2)}) copy-start(f32[1024]{0:T(1024)} %param.24) | copy-start | bytes 12292
  7.2 13.1 %copy-start.3 = (bf16[1024,128]{1,0:T(8,128)(2,1)S(1)}, bf16[1024,128]{1,0:T(8,128)(2,1)}, u32[]{:S(2)}) copy-start(bf16[1024,128]{1,0:T(8,128)(2,1)} %param.25) | copy-start | bytes 786436
  7.2 13.4 %copy-start.4 = (bf16[1024,128]{1,0:T(8,128)(2,1)S(1)}, bf16[1024,128]{1,0:T(8,128)(2,1)}, u32[]{:S(2)}) copy-start(bf16[1024,128]{1,0:T(8,128)(2,1)} %param.26) | copy-start | bytes 786436
  8.6 11.4 %all-to-all-start = ((bf16[4,16,256]{2,1,0:T(8,128)(2,1)}), bf16[4,16,256]{2,1,0:T(8,128)(2,1)S(1)}, u32[]{:S(2)}, u32[]{:S(2)}) async-start(bf16[4,16,256]{2,1,0:T(8,128)(2,1)} %broadcast_in_dim.25), calls=%async_computation | async-start | bytes 65536 | tf_op jit(solution)/shard_map/all_to_all | solution.py:26
  13.1 148.7 %all-gather.4.cloned.1.call-start = ((), (), s32[]{:S(2)}) async-start(), calls=%async_computation.8 | async-start | bytes 2113536 | tf_op jit(solution)/shard_map/all_gather | solution.py:60
  19.9 3.5 %copy-start.13 = (f32[128]{0:T(128)S(1)}, f32[128]{0:T(128)}, u32[]{:S(2)}) copy-start(f32[128]{0:T(128)} %param.31) | copy-start | bytes 1540
  20.2 9.1 %copy-start.11 = (f32[256]{0:T(256)S(1)}, f32[256]{0:T(256)}, u32[]{:S(2)}) copy-start(f32[256]{0:T(256)} %param.36) | copy-start | bytes 3076
  20.2 9.1 %copy-start.12 = (f32[256]{0:T(256)S(1)}, f32[256]{0:T(256)}, u32[]{:S(2)}) copy-start(f32[256]{0:T(256)} %param.45) | copy-start | bytes 3076
  20.3 14.4 %copy-start.6 = (bf16[16,256]{1,0:T(8,128)(2,1)S(1)}, bf16[16,256]{1,0:T(8,128)(2,1)}, u32[]{:S(2)}) copy-start(bf16[16,256]{1,0:T(8,128)(2,1)} %param.23) | copy-start | bytes 24580
  21.9 63.3 %copy-start.1 = (bf16[1,256,1024]{2,1,0:T(8,128)(2,1)S(1)}, bf16[1,256,1024]{2,1,0:T(8,128)(2,1)}, u32[]{:S(2)}) copy-start(bf16[1,256,1024]{2,1,0:T(8,128)(2,1)} %param.41) | copy-start | bytes 1572868
  23.4 62.0 %copy-start.9 = (bf16[16,128]{1,0:T(8,128)(2,1)}, bf16[16,128]{1,0:T(8,128)(2,1)S(1)}, u32[]{:S(2)}) copy-start(bf16[16,128]{1,0:T(8,128)(2,1)S(1)} %get-tuple-element.18) | copy-start | bytes 12292
  24.3 10.4 %all-to-all-start.1 = ((f32[4,16,256]{2,1,0:T(8,128)}), f32[4,16,256]{2,1,0:T(8,128)S(1)}, u32[]{:S(2)}, u32[]{:S(2)}) async-start(f32[4,16,256]{2,1,0:T(8,128)} %convolution_bitcast_fusion.3), calls=%async_computation.1 | async-start | bytes 131072 | tf_op jit(solution)/shard_map/all_to_all | solution.py:41
  35.5 8.4 %all-to-all-start.2 = ((f32[4,1,32]{2,1,0:T(1,128)}), f32[4,1,32]{2,1,0:T(1,128)S(1)}, u32[]{:S(2)}, u32[]{:S(2)}) async-start(f32[4,1,32]{2,1,0:T(1,128)} %broadcast_in_dim.27), calls=%async_computation.2 | async-start | bytes 4096 | tf_op jit(solution)/shard_map/all_to_all | solution.py:26
  81.6 14.4 %copy-start.2 = (bf16[1,1024,256]{2,1,0:T(8,128)(2,1)S(1)}, bf16[1,1024,256]{2,1,0:T(8,128)(2,1)}, u32[]{:S(2)}) copy-start(bf16[1,1024,256]{2,1,0:T(8,128)(2,1)} %param.39) | copy-start | bytes 1572868
  81.6 13.6 %all-to-all-start.4 = ((bf16[4,128,2,256]{3,2,1,0:T(2,128)(2,1)}), bf16[4,128,2,256]{3,2,1,0:T(2,128)(2,1)S(1)}, u32[]{:S(2)}, u32[]{:S(2)}) async-start(bf16[4,128,2,256]{3,2,1,0:T(2,128)(2,1)} %broadcast_in_dim.29), calls=%async_computation.4 | async-start | bytes 1048576 | tf_op jit(solution)/shard_map/all_to_all | solution.py:26
  85.4 10.9 %copy-start.15 = (bf16[1,1024,256]{2,1,0:T(8,128)(2,1)S(1)}, bf16[1,1024,256]{2,1,0:T(8,128)(2,1)}, u32[]{:S(2)}) copy-start(bf16[1,1024,256]{2,1,0:T(8,128)(2,1)} %param.40) | copy-start | bytes 1572868
  97.0 4.6 %copy-start.8 = (bf16[16,256]{1,0:T(8,128)(2,1)S(1)}, bf16[16,256]{1,0:T(8,128)(2,1)}, u32[]{:S(2)}) copy-start(bf16[16,256]{1,0:T(8,128)(2,1)} %param.44) | copy-start | bytes 24580
  98.1 47.2 %all-to-all-start.5 = ((f32[4,128,2,256]{3,1,2,0:T(8,128)}), f32[4,128,2,256]{3,1,2,0:T(8,128)S(1)}, u32[]{:S(2)}, u32[]{:S(2)}) async-start(f32[4,128,2,256]{3,1,2,0:T(8,128)} %copy.88), calls=%async_computation.5 | async-start | bytes 2097152 | tf_op jit(solution)/shard_map/all_to_all | solution.py:41
  101.6 78.7 %all-gather.6.cloned.1.call-start = ((), (), s32[]{:S(2)}) async-start(), calls=%async_computation.9 | async-start | bytes 1572864 | tf_op jit(solution)/shard_map/all_gather | solution.py:71
  146.2 25.7 %all-to-all-start.6 = ((bf16[128,2,256]{2,1,0:T(2,128)(2,1)}), bf16[128,2,256]{2,1,0:T(2,128)(2,1)S(1)}, u32[]{:S(2)}, u32[]{:S(2)}) async-start(bf16[128,2,256]{2,1,0:T(2,128)(2,1)} %copy.90), calls=%async_computation.6 | async-start | bytes 262144 | tf_op jit(solution)/shard_map/all_to_all | solution.py:244
  165.0 13.2 %copy-start.7 = (f32[16,6]{0,1:T(8,128)S(1)}, f32[16,6]{0,1:T(8,128)}, u32[]{:S(2)}) copy-start(f32[16,6]{0,1:T(8,128)} %param.38) | copy-start | bytes 1156
  165.1 13.4 %copy-start.14 = (f32[128]{0:T(128)S(1)}, f32[128]{0:T(128)}, u32[]{:S(2)}) copy-start(f32[128]{0:T(128)} %param.29) | copy-start | bytes 1540
  173.5 20.0 %all-to-all-start.7 = ((f32[4,1,65536]{2,1,0:T(1,128)}), f32[4,1,65536]{2,1,0:T(1,128)S(1)}, u32[]{:S(2)}, u32[]{:S(2)}) async-start(f32[4,1,65536]{2,1,0:T(1,128)} %broadcast_in_dim.30), calls=%async_computation.7 | async-start | bytes 2097152 | tf_op jit(solution)/shard_map/all_to_all | solution.py:26
Sparse Core Ops, SparseCore 0:
  17.0 144.7 all-gather.3
  163.9 16.4 all-gather.5
where the time goes:
time: 203 us; the launch traced here: 202 us
  blocking collectives  79.8 us (39%)
  waiting for transfers between devices  47 us (23%)
  starting transfers between devices  32.9 us (16%)
  between operations  15.2 us (7%)
  local copies, waits for them, and re-layouts  13.8 us (7%)
  matrix products  8.19 us (4%)
  other arithmetic  5.41 us (3%)
    all_gather x2, blocking collectives, stacked_from(): blocks = lax.all_gather(blocks, axes[k], axis=0, tiled=True)  43.6 us
    all_to_all x1, blocking collectives, body(): lax.all_to_all(placed.astype(jnp.bfloat16).reshape(experts, capacity, mix...  36.1 us
    all_to_all x4, waiting for transfers between devices, from_everyone(): return lax.all_to_all(copies, axis, split_axis=0, concat_axis=0, tiled=True)  26.5 us
    all_to_all x4, starting transfers between devices, from_everyone(): return lax.all_to_all(copies, axis, split_axis=0, concat_axis=0, tiled=True)  16 us
    all_to_all x1, starting transfers between devices, body(): lax.all_to_all(summed, EP, split_axis=0, concat_axis=0, tiled=True)  8.63 us
    all_to_all x2, starting transfers between devices, summed_on_arrival(): blocks = lax.all_to_all(cut_along(x, dim, length), axis, 0, 0, tiled=True)  8.31 us
    all_gather x1, waiting for transfers between devices, gather_turned(): whole, at, done = (lax.all_gather(both, axis, axis=0, tiled=True), 0, [])  6.94 us
    all_to_all x1, waiting for transfers between devices, body(): lax.all_to_all(summed, EP, split_axis=0, concat_axis=0, tiled=True)  6.83 us
  transfers between devices with their start and end apart: 9, of which 7 were waited for; matrix products, arithmetic and copies ran while one was open for 12% of the time, Pallas kernels for 0%

commit v1 on v0

v1 whole, which is shorter than its diff:
```python
import math

import jax
import jax.numpy as jnp
from jax import lax
from jax.sharding import Mesh
from jax.sharding import PartitionSpec as P

EP = ("ep_0", "ep_1", "ep_2")
PLANE = ("ep_1", "ep_2")
BLOCK = ("ep_1", "ep_2", "tp")
CAP = 2


EPSILON = 1e-06
CLAMP_LIMIT = 7.0
SWISH_ALPHA = 1.702
OUT_SCALE = 0.2 + 0.6 * math.exp(-0.6)


def from_everyone(x, axis):
    copies = jnp.broadcast_to(x, (lax.axis_size(axis), *x.shape))
    return lax.all_to_all(copies, axis, split_axis=0, concat_axis=0, tiled=True)


def rms_scale(values, scale_gain):
    mean_square = jnp.mean(values * values, axis=-1, keepdims=True)
    return values * lax.rsqrt(mean_square + EPSILON) * scale_gain


def clamped_unit(gate_pre, up_pre):
    gate_cut = jnp.minimum(gate_pre, CLAMP_LIMIT)
    up_cut = jnp.clip(up_pre, -CLAMP_LIMIT, CLAMP_LIMIT)
    return (up_cut + 1.0) * gate_cut * jax.nn.sigmoid(SWISH_ALPHA * gate_cut)


def attend(
    normed,
    query_weight,
    key_weight,
    value_weight,
    query_gain,
    key_gain,
    lambda_head,
    sub_gain,
    cache_key,
    cache_value,
    lengths,
):
    seq_count = normed.shape[0]
    head_count = lambda_head.shape[0]
    qk_size = query_gain.shape[0] // 2
    val_size = value_weight.shape[1] // head_count
    cache_len = cache_key.shape[1]
    scale_factor = qk_size ** (-0.5)
    query_pre = jnp.dot(normed, query_weight, preferred_element_type=jnp.float32)
    query_rows = rms_scale(
        query_pre.reshape(seq_count, head_count, 2, qk_size), query_gain.reshape(2, qk_size)
    ).astype(jnp.bfloat16)
    key_pre = jnp.dot(normed, key_weight, preferred_element_type=jnp.float32)
    key_rows = rms_scale(
        key_pre.reshape(seq_count, head_count, 2, qk_size), key_gain.reshape(2, qk_size)
    ).astype(jnp.bfloat16)
    value_rows = jnp.dot(normed, value_weight, preferred_element_type=jnp.float32).astype(
        jnp.bfloat16
    )
    key_past = cache_key.reshape(seq_count, cache_len, head_count, 2, qk_size)
    past_score = (
        jnp.einsum("shmd,sjhmd->shmj", query_rows, key_past, preferred_element_type=jnp.float32)
        * scale_factor
    )
    own_score = (
        jnp.einsum("shmd,shmd->shm", query_rows, key_rows, preferred_element_type=jnp.float32)
        * scale_factor
    )
    valid_mask = lax.iota(jnp.int32, cache_len)[None, :] < lengths[:, None]
    past_exp = jnp.where(valid_mask[:, None, None, :], jnp.exp(past_score), 0.0)
    own_exp = jnp.exp(own_score)
    denominator = jnp.sum(past_exp, axis=-1) + own_exp
    past_prob = past_exp / denominator[..., None]
    own_prob = own_exp / denominator
    weight_past = (past_prob[:, :, 0] - lambda_head[None, :, None] * past_prob[:, :, 1]).astype(
        jnp.bfloat16
    )
    weight_own = (own_prob[:, :, 0] - lambda_head[None, :] * own_prob[:, :, 1]).astype(jnp.bfloat16)
    value_past = cache_value.reshape(seq_count, cache_len, head_count, val_size)
    head_mix = jnp.einsum(
        "shj,sjhe->she", weight_past, value_past, preferred_element_type=jnp.float32
    )
    own_value = value_rows.reshape(seq_count, head_count, val_size).astype(jnp.float32)
    head_mix = head_mix + weight_own.astype(jnp.float32)[..., None] * own_value
    head_out = (rms_scale(head_mix, sub_gain) * OUT_SCALE).astype(jnp.bfloat16)
    return (
        head_out.reshape(seq_count, head_count * val_size),
        key_rows.reshape(seq_count, -1),
        value_rows,
    )


def routing_tables(route_ids, route_weight):
    line = lax.axis_size("ep_0")
    plane = lax.axis_size("ep_1") * lax.axis_size("ep_2")
    seq_count, top_count = route_ids.shape
    packed = jnp.concatenate([route_ids.astype(jnp.float32).T, route_weight.T], axis=0)
    seen = from_everyone(packed, "ep_0")
    seen = seen.transpose(1, 0, 2).reshape(2 * top_count, line * seq_count)
    first = (lax.axis_index("ep_0") * plane).astype(jnp.float32)
    wanted = first + lax.broadcasted_iota(jnp.float32, (plane, 1), 0)
    named = [(seen[k][None, :] == wanted).astype(jnp.float32) for k in range(top_count)]
    match = sum(named)
    weight = sum(n * seen[top_count + k][None, :] for k, n in enumerate(named))
    total = line * seq_count
    row = lax.broadcasted_iota(jnp.int32, (total, total), 0)
    col = lax.broadcasted_iota(jnp.int32, (total, total), 1)
    earlier = ((row // seq_count == col // seq_count) & (row < col)).astype(jnp.bfloat16)
    rank = jnp.dot(match.astype(jnp.bfloat16), earlier, preferred_element_type=jnp.float32)
    slot = jnp.where(match > 0, rank, -1.0)
    shape = (plane, line, CAP, total)
    at_z = lax.broadcasted_iota(jnp.int32, shape, 1)
    at_slot = lax.broadcasted_iota(jnp.int32, shape, 2)
    of_z = lax.broadcasted_iota(jnp.int32, shape, 3) // seq_count
    hit = (at_z == of_z) & (slot[:, None, None, :] == at_slot.astype(jnp.float32))
    select = hit.astype(jnp.bfloat16).reshape(plane * line * CAP, total)
    scaled = jnp.where(hit, weight[:, None, None, :], 0.0).reshape(plane * line * CAP, total)
    upper = scaled.astype(jnp.bfloat16)
    lower = (scaled - upper.astype(jnp.float32)).astype(jnp.bfloat16)
    return select, upper, lower


def plane_weights(dense_gate, dense_up, dense_down):
    mine = jnp.concatenate([dense_gate.T, dense_up.T, dense_down], axis=0)
    units = dense_down.shape[0]
    seen = from_everyone(mine[None], PLANE).reshape(-1, *mine.shape)
    width = mine.shape[1]
    gate = seen[:, :units].reshape(-1, width)
    up = seen[:, units : 2 * units].reshape(-1, width)
    down = seen[:, 2 * units :].reshape(-1, width)
    return gate, up, down


def own_columns(x, axis):
    count = lax.axis_size(axis)
    width = x.shape[1] // count
    mine = lax.axis_index(axis)
    return sum(
        jnp.where(mine == k, x[:, k * width : (k + 1) * width], 0.0) for k in range(count)
    )


def body(
    hidden_in,
    norm_gain_attn,
    query_weight,
    key_weight,
    value_weight,
    query_gain,
    key_gain,
    lambda_head,
    sub_gain,
    out_weight,
    cache_key,
    cache_value,
    lengths,
    norm_gain_mix,
    route_ids,
    route_logits,
    expert_gate,
    expert_up,
    expert_down,
    dense_gate,
    dense_up,
    dense_down,
    branch_gate,
):
    seq_count = route_ids.shape[0]
    width = hidden_in.shape[1]
    line = lax.axis_size("ep_0")
    plane = lax.axis_size("ep_1") * lax.axis_size("ep_2")
    tp = lax.axis_size("tp")
    pieces = from_everyone(hidden_in, "tp")
    full_rows = jnp.concatenate([pieces[k] for k in range(tp)], axis=1).astype(jnp.float32)
    width_total = full_rows.shape[1]
    select, upper, lower = routing_tables(route_ids, jax.nn.softmax(route_logits, axis=1))
    gate_rows, up_rows, down_rows = plane_weights(dense_gate, dense_up, dense_down)
    normed = rms_scale(full_rows, norm_gain_attn).astype(jnp.bfloat16)
    head_out, key_rows, value_rows = attend(
        normed,
        query_weight,
        key_weight,
        value_weight,
        query_gain,
        key_gain,
        lambda_head,
        sub_gain,
        cache_key,
        cache_value,
        lengths,
    )
    head_terms = jnp.dot(head_out, out_weight, preferred_element_type=jnp.float32)
    residual_full = full_rows + from_everyone(head_terms, "tp").sum(axis=0)
    square_sum = jnp.sum(residual_full * residual_full, axis=1, keepdims=True)
    inverse = lax.rsqrt(square_sum / width_total + EPSILON)
    residual = own_columns(residual_full, "tp")
    mix_rows = (residual * inverse * norm_gain_mix[None, :]).astype(jnp.bfloat16)
    rows = from_everyone(mix_rows, "ep_0").reshape(line * seq_count, width)
    placed = jnp.dot(select, rows, preferred_element_type=jnp.float32).astype(jnp.bfloat16)
    placed = placed.reshape(plane, 1, line * CAP, width)
    placed = jnp.broadcast_to(placed, (plane, tp, line * CAP, width))
    arrived = lax.all_to_all(
        placed.reshape(plane * tp, line * CAP, width), BLOCK, 0, 0, tiled=True
    ).reshape(plane, tp, line * CAP, width)
    item_rows = jnp.concatenate(
        [arrived[:, k].reshape(plane * line * CAP, width) for k in range(tp)], axis=1
    )
    gate_pre = jnp.dot(item_rows, expert_gate[0], preferred_element_type=jnp.float32)
    up_pre = jnp.dot(item_rows, expert_up[0], preferred_element_type=jnp.float32)
    activation = clamped_unit(gate_pre, up_pre).astype(jnp.bfloat16)
    sent = jnp.stack(
        [
            jnp.dot(
                activation,
                expert_down[0][:, k * width : (k + 1) * width],
                preferred_element_type=jnp.float32,
            )
            .astype(jnp.bfloat16)
            .reshape(plane, line * CAP, width)
            for k in range(tp)
        ],
        axis=1,
    )
    returned = lax.all_to_all(
        sent.reshape(plane * tp, line * CAP, width), BLOCK, 0, 0, tiled=True
    ).reshape(plane, tp, line * CAP, width)
    route_out = jnp.sum(returned.astype(jnp.float32), axis=1).astype(jnp.bfloat16)
    route_out = route_out.reshape(plane * line * CAP, width)
    turned = (((0,), (0,)), ((), ()))
    routed = lax.dot_general(
        upper, route_out, turned, preferred_element_type=jnp.float32
    ) + lax.dot_general(lower, route_out, turned, preferred_element_type=jnp.float32)
    across = (((1,), (1,)), ((), ()))
    gate_part = lax.dot_general(rows, gate_rows, across, preferred_element_type=jnp.float32)
    up_part = lax.dot_general(rows, up_rows, across, preferred_element_type=jnp.float32)
    logit_part = jnp.sum(rows.astype(jnp.float32) * branch_gate[None, :], axis=1)
    units = gate_part.shape[1]
    logit_rows = jnp.broadcast_to(
        logit_part.reshape(-1, 2 * units), (8, (line * seq_count) // (2 * units), 2 * units)
    ).reshape(-1, 2 * units)
    together = jnp.concatenate(
        [jnp.concatenate([gate_part, up_part], axis=1), logit_rows], axis=0
    )
    summed = from_everyone(together, "tp").sum(axis=0)
    count = line * seq_count
    dense_act = (jax.nn.silu(summed[:count, :units]) * summed[:count, units:]).astype(jnp.bfloat16)
    logits = summed[count : count + count // (2 * units)].reshape(-1, 1)
    dense = jnp.dot(dense_act, down_rows, preferred_element_type=jnp.float32)
    back = (routed + jax.nn.sigmoid(logits) * dense).astype(jnp.bfloat16)
    home = lax.all_to_all(
        back.reshape(line, seq_count, width), "ep_0", 0, 0, tiled=True
    )
    layer_out = (residual + jnp.sum(home.astype(jnp.float32), axis=0)).astype(jnp.bfloat16)
    return (layer_out, key_rows, value_rows)


def solution(mesh):
    split = Mesh(mesh.devices.reshape(16, 4, 2, mesh.shape["tp"]), ("ep_0", "ep_1", "ep_2", "tp"))
    in_specs = (
        P(EP, "tp"),
        P(),
        P(None, "tp"),
        P(None, "tp"),
        P(None, "tp"),
        P(),
        P(),
        P("tp"),
        P(),
        P("tp", None),
        P(EP, None, "tp"),
        P(EP, None, "tp"),
        P(EP),
        P("tp"),
        P(EP, None),
        P(EP, None),
        P(EP, None, "tp"),
        P(EP, None, "tp"),
        P(EP, "tp", None),
        P("tp", EP),
        P("tp", EP),
        P(EP, "tp"),
        P("tp"),
    )
    out_specs = (P(EP, "tp"), P(EP, "tp"), P(EP, "tp"))
    return jax.shard_map(body, mesh=split, in_specs=in_specs, out_specs=out_specs, check_vma=False)
```

time: 203 us -> 160 us (0.79)
  blocking collectives: 79.8 us -> 0 us
  waiting for transfers between devices: 47 us -> 79 us
  starting transfers between devices: 32.9 us -> 49.6 us
  between operations: 15.2 us -> 1.74 us
  other arithmetic: 5.41 us -> 8.95 us
  matrix products: 8.19 us -> 5.99 us
    all_gather x2 -> x0, blocking collectives: 43.6 us -> none  [stacked_from(): blocks = lax.all_gather(blocks, axes[k], axis=0, tiled=True)]
    all_to_all x1 -> x0, blocking collectives: 36.1 us -> none  [body(): lax.all_to_all(placed.astype(jnp.bfloat16).reshape(experts, capacity, mix...]
    all_to_all x3, waiting for transfers between devices: 12.2 us -> 35.6 us  [the longest x1 13.1 us: body(): lax.all_to_all(back.reshape(line, seq_count, width), 'ep_0', 0, 0, tiled=...]
    all_to_all x4 -> x6, starting transfers between devices: 16 us -> 37.1 us  [from_everyone(): return lax.all_to_all(copies, axis, split_axis=0, concat_axis=0, tiled=True)]
    all_to_all x4 -> x6, waiting for transfers between devices: 26.5 us -> 43.4 us  [from_everyone(): return lax.all_to_all(copies, axis, split_axis=0, concat_axis=0, tiled=True)]
    all_gather x2 -> x0, waiting for transfers between devices: 8.19 us -> none  [the longest x1 6.94 us: gather_turned(): whole, at, done = (lax.all_gather(both, axis, axis=0, tiled=True), 0, [])]
    all_to_all x3, starting transfers between devices: 16.9 us -> 12.5 us  [the longest x1 4.59 us: body(): lax.all_to_all(back.reshape(line, seq_count, width), 'ep_0', 0, 0, tiled=...]
    transpose x3 -> x0, local copies, waits for them, and re-layouts: 3.07 us -> none  [the longest x1 1.34 us: stacked_from(): blocks.transpose(*turned, *range(len(sequence), blocks.ndim))]
  transfers between devices with their start and end apart: 9 -> 9, of which waited for: 7 -> 8; matrix products, arithmetic and copies ran while one was open for 12% -> 12% of each run, Pallas kernels for 0% -> 0%
where the time goes in v1:
time: 160 us; the launch traced here: 158 us
  waiting for transfers between devices  79 us (49%)
  starting transfers between devices  49.6 us (31%)
  local copies, waits for them, and re-layouts  13.1 us (8%)
  other arithmetic  8.95 us (6%)
  matrix products  5.99 us (4%)
  between operations  1.74 us (1%)
    all_to_all x6, waiting for transfers between devices, from_everyone(): return lax.all_to_all(copies, axis, split_axis=0, concat_axis=0, tiled=True)  43.4 us
    all_to_all x6, starting transfers between devices, from_everyone(): return lax.all_to_all(copies, axis, split_axis=0, concat_axis=0, tiled=True)  37.1 us
    all_to_all x1, waiting for transfers between devices, body(): lax.all_to_all(back.reshape(line, seq_count, width), 'ep_0', 0, 0, tiled=...  13.1 us
    all_to_all x1, waiting for transfers between devices, body(): lax.all_to_all(sent.reshape(plane * tp, line * CAP, width), BLOCK, 0, 0,...  11.3 us
    all_to_all x1, waiting for transfers between devices, body(): lax.all_to_all(placed.reshape(plane * tp, line * CAP, width), BLOCK, 0, 0...  11.1 us
    all_to_all x1, starting transfers between devices, body(): lax.all_to_all(back.reshape(line, seq_count, width), 'ep_0', 0, 0, tiled=...  4.59 us
    broadcast_in_dim x6, local copies, waits for them, and re-layouts, from_everyone(): copies = jnp.broadcast_to(x, (lax.axis_size(axis), *x.shape))  4.5 us
    all_to_all x1, starting transfers between devices, body(): lax.all_to_all(sent.reshape(plane * tp, line * CAP, width), BLOCK, 0, 0,...  4.06 us
  transfers between devices with their start and end apart: 9, of which 8 were waited for; matrix products, arithmetic and copies ran while one was open for 12% of the time, Pallas kernels for 0%

profile of v1, /device:TPU:32, one launch (start us, length us, event | category | flops | bytes accessed | tf_op | source)
XLA Modules:
  0.0 158.4 jit_solution(16080127196354414378)
XLA Ops:
  0.6 1.4 broadcast_in_dim.82
  2.0 4.5 %all-to-all-start = ((bf16[4,16,256]{2,1,0:T(8,128)(2,1)}), bf16[4,16,256]{2,1,0:T(8,128)(2,1)S(1)}, u32[]{:S(2)}, u32[]{:S(2)}) async-start(bf16[4,16,256]{2,1,0:T(8,128)(2,1)} %broadcast_in_dim.82), calls=%async_computation | async-start | bytes 65536 | tf_op jit(solution)/shard_map/all_to_all | solution.py:23
  6.5 0.7 iota_compare_fusion.1
  7.3 0.7 reduce_max.9
  8.0 0.7 fusion.65
  8.7 0.7 divide_bitcast_fusion.1
  9.4 0.7 convert_bitcast_fusion
  10.1 0.7 pad_maximum_fusion.6
  10.8 0.7 mul.315
  11.5 0.7 mul.324
  12.3 1.5 copy.34
  14.5 0.7 reshape.965
  15.2 15.2 %all-to-all-start.2 = ((f32[16,1,192]{2,1,0:T(1,128)}), f32[16,1,192]{2,1,0:T(1,128)S(1)}, u32[]{:S(2)}, u32[]{:S(2)}) async-start(f32[16,1,192]{2,1,0:T(1,128)} %reshape.965), calls=%async_computation.2 | async-start | bytes 32768 | tf_op jit(solution)/shard_map/all_to_all | solution.py:23
  31.8 0.2 fusion.38
  32.3 0.2 fusion.36
  32.8 0.3 multiply_reduce_fusion.2
  33.3 8.4 %all-to-all-done.2 = f32[16,1,192]{2,1,0:T(1,128)S(1)} async-done(((f32[16,1,192]{2,1,0:T(1,128)}), f32[16,1,192]{2,1,0:T(1,128)S(1)}, u32[]{:S(2)}, u32[]{:S(2)}) %all-to-all-start.2) | async-done | bytes 12320 | tf_op jit(solution)/shard_map/all_to_all | solution.py:23
  41.7 0.7 broadcast_in_dim.85
  42.4 4.9 %all-to-all-start.1 = ((f32[4,16,1024]{2,1,0:T(8,128)}), f32[4,16,1024]{2,1,0:T(8,128)S(1)}, u32[]{:S(2)}, u32[]{:S(2)}) async-start(f32[4,16,1024]{2,1,0:T(8,128)} %broadcast_in_dim.85), calls=%async_computation.1 | async-start | bytes 524288 | tf_op jit(solution)/shard_map/all_to_all | solution.py:23
  47.4 0.5 broadcast.872
  47.9 0.7 reduce.60
  48.7 0.3 slice_reduce_fusion.5
  50.0 4.0 %all-to-all-done.1 = f32[4,16,1024]{2,1,0:T(8,128)S(1)} async-done(((f32[4,16,1024]{2,1,0:T(8,128)}), f32[4,16,1024]{2,1,0:T(8,128)S(1)}, u32[]{:S(2)}, u32[]{:S(2)}) %all-to-all-start.1) | async-done | bytes 262176 | tf_op jit(solution)/shard_map/all_to_all | solution.py:23
  54.0 0.7 broadcast_in_dim.94
  54.7 4.3 %all-to-all-start.6 = ((bf16[8,1,48,256]{3,2,1,0:T(8,128)(2,1)}), bf16[8,1,48,256]{3,2,1,0:T(8,128)(2,1)S(1)}, u32[]{:S(2)}, u32[]{:S(2)}) async-start(bf16[8,1,48,256]{3,2,1,0:T(8,128)(2,1)} %broadcast_in_dim.94), calls=%async_computation.6 | async-start | bytes 393216 | tf_op jit(solution)/shard_map/all_to_all | solution.py:23
  59.3 6.6 %all-to-all-done.6 = bf16[8,1,48,256]{3,2,1,0:T(8,128)(2,1)S(1)} async-done(((bf16[8,1,48,256]{3,2,1,0:T(8,128)(2,1)}), bf16[8,1,48,256]{3,2,1,0:T(8,128)(2,1)S(1)}, u32[]{:S(2)}, u32[]{:S(2)}) %all-to-all-start.6) | async-done | bytes 196640 | tf_op jit(solution)/shard_map/all_to_all | solution.py:23
  65.8 0.6 broadcast_in_dim.91
  66.5 4.7 %all-to-all-start.3 = ((bf16[16,16,256]{2,1,0:T(8,128)(2,1)}), bf16[16,16,256]{2,1,0:T(8,128)(2,1)S(1)}, u32[]{:S(2)}, u32[]{:S(2)}) async-start(bf16[16,16,256]{2,1,0:T(8,128)(2,1)} %broadcast_in_dim.91), calls=%async_computation.3 | async-start | bytes 262144 | tf_op jit(solution)/shard_map/all_to_all | solution.py:23
  71.1 0.3 convolution_select_fusion
  71.4 0.3 fusion.8
  72.0 13.2 %all-to-all-done.3 = bf16[16,16,256]{2,1,0:T(8,128)(2,1)S(1)} async-done(((bf16[16,16,256]{2,1,0:T(8,128)(2,1)}), bf16[16,16,256]{2,1,0:T(8,128)(2,1)S(1)}, u32[]{:S(2)}, u32[]{:S(2)}) %all-to-all-start.3) | async-done | bytes 131104 | tf_op jit(solution)/shard_map/all_to_all | solution.py:23
  85.5 0.9 broadcast_in_dim.93
  86.4 3.9 %all-to-all-start.4 = ((bf16[32,32,256]{2,1,0:T(8,128)(2,1)}), bf16[32,32,256]{2,1,0:T(8,128)(2,1)S(1)}, u32[]{:S(2)}, u32[]{:S(2)}) async-start(bf16[32,32,256]{2,1,0:T(8,128)(2,1)} %bitcast.20), calls=%async_computation.4 | async-start | bytes 1048576 | tf_op jit(solution)/shard_map/all_to_all | solution.py:209
  91.0 11.1 %all-to-all-done.4 = bf16[32,32,256]{2,1,0:T(8,128)(2,1)S(1)} async-done(((bf16[32,32,256]{2,1,0:T(8,128)(2,1)}), bf16[32,32,256]{2,1,0:T(8,128)(2,1)S(1)}, u32[]{:S(2)}, u32[]{:S(2)}) %all-to-all-start.4) | async-done | bytes 524320 | tf_op jit(solution)/shard_map/all_to_all | solution.py:209
  102.1 1.1 broadcast_in_dim.95
  103.1 3.5 %all-to-all-start.7 = ((f32[4,264,256]{2,1,0:T(8,128)}), f32[4,264,256]{2,1,0:T(8,128)S(1)}, u32[]{:S(2)}, u32[]{:S(2)}) async-start(f32[4,264,256]{2,1,0:T(8,128)} %broadcast_in_dim.95), calls=%async_computation.7 | async-start | bytes 2162688 | tf_op jit(solution)/shard_map/all_to_all | solution.py:23
  106.7 1.4 convolution_minimum_fusion
  108.1 0.3 fusion.4
  108.4 0.7 copy-done.1
  109.9 0.9 pad_maximum_fusion.1
  110.8 11.3 %all-to-all-done.7 = f32[4,264,256]{2,1,0:T(8,128)S(1)} async-done(((f32[4,264,256]{2,1,0:T(8,128)}), f32[4,264,256]{2,1,0:T(8,128)S(1)}, u32[]{:S(2)}, u32[]{:S(2)}) %all-to-all-start.7) | async-done | bytes 1081376 | tf_op jit(solution)/shard_map/all_to_all | solution.py:23
  122.1 4.1 %all-to-all-start.5 = ((bf16[32,32,256]{2,1,0:T(8,128)(2,1)}), bf16[32,32,256]{2,1,0:T(8,128)(2,1)S(1)}, u32[]{:S(2)}, u32[]{:S(2)}) async-start(bf16[32,32,256]{2,1,0:T(8,128)(2,1)} %bitcast.37), calls=%async_computation.5 | async-start | bytes 1048576 | tf_op jit(solution)/shard_map/all_to_all | solution.py:231
  126.6 11.3 %all-to-all-done.5 = bf16[32,32,256]{2,1,0:T(8,128)(2,1)S(1)} async-done(((bf16[32,32,256]{2,1,0:T(8,128)(2,1)}), bf16[32,32,256]{2,1,0:T(8,128)(2,1)S(1)}, u32[]{:S(2)}, u32[]{:S(2)}) %all-to-all-start.5) | async-done | bytes 524320 | tf_op jit(solution)/shard_map/all_to_all | solution.py:231
  138.5 0.8 fusion.5
  139.3 4.6 %all-to-all-start.8 = ((bf16[16,16,256]{2,1,0:T(8,128)(2,1)}), bf16[16,16,256]{2,1,0:T(8,128)(2,1)S(1)}, u32[]{:S(2)}, u32[]{:S(2)}) async-start(bf16[16,16,256]{2,1,0:T(8,128)(2,1)} %bitcast.47), calls=%async_computation.8 | async-start | bytes 262144 | tf_op jit(solution)/shard_map/all_to_all | solution.py:257
  144.1 0.6 multiply_convert_fusion.3
  144.7 13.1 %all-to-all-done.8 = bf16[16,16,256]{2,1,0:T(8,128)(2,1)S(1)} async-done(((bf16[16,16,256]{2,1,0:T(8,128)(2,1)}), bf16[16,16,256]{2,1,0:T(8,128)(2,1)S(1)}, u32[]{:S(2)}, u32[]{:S(2)}) %all-to-all-start.8) | async-done | bytes 131104 | tf_op jit(solution)/shard_map/all_to_all | solution.py:257
  157.8 0.6 add_convert_fusion
  (97 shorter events, 6.5 us)
Async XLA Ops:
  0.6 31.7 %copy-start = (bf16[16,256,128]{2,1,0:T(8,128)(2,1)S(1)}, bf16[16,256,128]{2,1,0:T(8,128)(2,1)}, u32[]{:S(2)}) copy-start(bf16[16,256,128]{2,1,0:T(8,128)(2,1)} %param.34) | copy-start | bytes 3145732
  2.0 13.2 %all-to-all-start = ((bf16[4,16,256]{2,1,0:T(8,128)(2,1)}), bf16[4,16,256]{2,1,0:T(8,128)(2,1)S(1)}, u32[]{:S(2)}, u32[]{:S(2)}) async-start(bf16[4,16,256]{2,1,0:T(8,128)(2,1)} %broadcast_in_dim.82), calls=%async_computation | async-start | bytes 65536 | tf_op jit(solution)/shard_map/all_to_all | solution.py:23
  12.3 18.3 %copy-start.2 = (bf16[1024,128]{1,0:T(8,128)(2,1)S(1)}, bf16[1024,128]{1,0:T(8,128)(2,1)}, u32[]{:S(2)}) copy-start(bf16[1024,128]{1,0:T(8,128)(2,1)} %param.25) | copy-start | bytes 786436
  12.3 18.3 %copy-start.5 = (f32[1024]{0:T(1024)S(1)}, f32[1024]{0:T(1024)}, u32[]{:S(2)}) copy-start(f32[1024]{0:T(1024)} %param.24) | copy-start | bytes 12292
  12.3 18.6 %copy-start.3 = (bf16[1024,128]{1,0:T(8,128)(2,1)S(1)}, bf16[1024,128]{1,0:T(8,128)(2,1)}, u32[]{:S(2)}) copy-start(bf16[1024,128]{1,0:T(8,128)(2,1)} %param.26) | copy-start | bytes 786436
  15.2 26.5 %all-to-all-start.2 = ((f32[16,1,192]{2,1,0:T(1,128)}), f32[16,1,192]{2,1,0:T(1,128)S(1)}, u32[]{:S(2)}, u32[]{:S(2)}) async-start(f32[16,1,192]{2,1,0:T(1,128)} %reshape.965), calls=%async_computation.2 | async-start | bytes 32768 | tf_op jit(solution)/shard_map/all_to_all | solution.py:23
  31.8 1.0 copy-start.12
  31.8 1.3 copy-start.4
  31.8 1.3 copy-start.9
  33.1 21.6 %copy-start.6 = (bf16[16,128]{1,0:T(8,128)(2,1)}, bf16[16,128]{1,0:T(8,128)(2,1)S(1)}, u32[]{:S(2)}) copy-start(bf16[16,128]{1,0:T(8,128)(2,1)S(1)} %get-tuple-element.41) | copy-start | bytes 12292
  42.4 16.8 %copy-start.7 = (f32[256]{0:T(256)S(1)}, f32[256]{0:T(256)}, u32[]{:S(2)}) copy-start(f32[256]{0:T(256)} %param.36) | copy-start | bytes 3076
  42.4 11.6 %all-to-all-start.1 = ((f32[4,16,1024]{2,1,0:T(8,128)}), f32[4,16,1024]{2,1,0:T(8,128)S(1)}, u32[]{:S(2)}, u32[]{:S(2)}) async-start(f32[4,16,1024]{2,1,0:T(8,128)} %broadcast_in_dim.85), calls=%async_computation.1 | async-start | bytes 524288 | tf_op jit(solution)/shard_map/all_to_all | solution.py:23
  54.7 11.1 %all-to-all-start.6 = ((bf16[8,1,48,256]{3,2,1,0:T(8,128)(2,1)}), bf16[8,1,48,256]{3,2,1,0:T(8,128)(2,1)S(1)}, u32[]{:S(2)}, u32[]{:S(2)}) async-start(bf16[8,1,48,256]{3,2,1,0:T(8,128)(2,1)} %broadcast_in_dim.94), calls=%async_computation.6 | async-start | bytes 393216 | tf_op jit(solution)/shard_map/all_to_all | solution.py:23
  59.0 26.1 %copy-start.8 = (f32[256]{0:T(256)S(1)}, f32[256]{0:T(256)}, u32[]{:S(2)}) copy-start(f32[256]{0:T(256)} %param.45) | copy-start | bytes 3076
  66.5 18.7 %all-to-all-start.3 = ((bf16[16,16,256]{2,1,0:T(8,128)(2,1)}), bf16[16,16,256]{2,1,0:T(8,128)(2,1)S(1)}, u32[]{:S(2)}, u32[]{:S(2)}) async-start(bf16[16,16,256]{2,1,0:T(8,128)(2,1)} %broadcast_in_dim.91), calls=%async_computation.3 | async-start | bytes 262144 | tf_op jit(solution)/shard_map/all_to_all | solution.py:23
  86.4 15.7 %all-to-all-start.4 = ((bf16[32,32,256]{2,1,0:T(8,128)(2,1)}), bf16[32,32,256]{2,1,0:T(8,128)(2,1)S(1)}, u32[]{:S(2)}, u32[]{:S(2)}) async-start(bf16[32,32,256]{2,1,0:T(8,128)(2,1)} %bitcast.20), calls=%async_computation.4 | async-start | bytes 1048576 | tf_op jit(solution)/shard_map/all_to_all | solution.py:209
  103.1 19.0 %all-to-all-start.7 = ((f32[4,264,256]{2,1,0:T(8,128)}), f32[4,264,256]{2,1,0:T(8,128)S(1)}, u32[]{:S(2)}, u32[]{:S(2)}) async-start(f32[4,264,256]{2,1,0:T(8,128)} %broadcast_in_dim.95), calls=%async_computation.7 | async-start | bytes 2162688 | tf_op jit(solution)/shard_map/all_to_all | solution.py:23
  106.7 1.4 copy-start.11
  108.1 1.0 copy-start.1
  122.1 15.8 %all-to-all-start.5 = ((bf16[32,32,256]{2,1,0:T(8,128)(2,1)}), bf16[32,32,256]{2,1,0:T(8,128)(2,1)S(1)}, u32[]{:S(2)}, u32[]{:S(2)}) async-start(bf16[32,32,256]{2,1,0:T(8,128)(2,1)} %bitcast.37), calls=%async_computation.5 | async-start | bytes 1048576 | tf_op jit(solution)/shard_map/all_to_all | solution.py:231
  138.2 5.8 %copy-start.10 = (f32[128]{0:T(128)S(1)}, f32[128]{0:T(128)}, u32[]{:S(2)}) copy-start(f32[128]{0:T(128)} %param.29) | copy-start | bytes 1540
  139.3 18.5 %all-to-all-start.8 = ((bf16[16,16,256]{2,1,0:T(8,128)(2,1)}), bf16[16,16,256]{2,1,0:T(8,128)(2,1)S(1)}, u32[]{:S(2)}, u32[]{:S(2)}) async-start(bf16[16,16,256]{2,1,0:T(8,128)(2,1)} %bitcast.47), calls=%async_computation.8 | async-start | bytes 262144 | tf_op jit(solution)/shard_map/all_to_all | solution.py:257

commit v2 on v1

v2 whole, which is shorter than its diff:
```python
import math

import jax
import jax.numpy as jnp
from jax import lax
from jax.experimental import pallas as pl
from jax.experimental.pallas import tpu as pltpu
from jax.sharding import Mesh
from jax.sharding import PartitionSpec as P

EP = ("ep_0", "ep_1", "ep_2")
PLANE = ("ep_1", "ep_2")
BLOCK = ("ep_1", "ep_2", "tp")
CAP = 2


EPSILON = 1e-06
CLAMP_LIMIT = 7.0
SWISH_ALPHA = 1.702
OUT_SCALE = 0.2 + 0.6 * math.exp(-0.6)


def from_everyone(x, axis):
    copies = jnp.broadcast_to(x, (lax.axis_size(axis), *x.shape))
    return lax.all_to_all(copies, axis, split_axis=0, concat_axis=0, tiled=True)


def rms_scale(values, scale_gain):
    mean_square = jnp.mean(values * values, axis=-1, keepdims=True)
    return values * lax.rsqrt(mean_square + EPSILON) * scale_gain


def clamped_unit(gate_pre, up_pre):
    gate_cut = jnp.minimum(gate_pre, CLAMP_LIMIT)
    up_cut = jnp.clip(up_pre, -CLAMP_LIMIT, CLAMP_LIMIT)
    return (up_cut + 1.0) * gate_cut * jax.nn.sigmoid(SWISH_ALPHA * gate_cut)


def attend(
    normed,
    query_weight,
    key_weight,
    value_weight,
    query_gain,
    key_gain,
    lambda_head,
    sub_gain,
    cache_key,
    cache_value,
    lengths,
):
    seq_count = normed.shape[0]
    head_count = lambda_head.shape[0]
    qk_size = query_gain.shape[0] // 2
    val_size = value_weight.shape[1] // head_count
    cache_len = cache_key.shape[1]
    scale_factor = qk_size ** (-0.5)
    query_pre = jnp.dot(normed, query_weight, preferred_element_type=jnp.float32)
    query_rows = rms_scale(
        query_pre.reshape(seq_count, head_count, 2, qk_size), query_gain.reshape(2, qk_size)
    ).astype(jnp.bfloat16)
    key_pre = jnp.dot(normed, key_weight, preferred_element_type=jnp.float32)
    key_rows = rms_scale(
        key_pre.reshape(seq_count, head_count, 2, qk_size), key_gain.reshape(2, qk_size)
    ).astype(jnp.bfloat16)
    value_rows = jnp.dot(normed, value_weight, preferred_element_type=jnp.float32).astype(
        jnp.bfloat16
    )
    key_past = cache_key.reshape(seq_count, cache_len, head_count, 2, qk_size)
    past_score = (
        jnp.einsum("shmd,sjhmd->shmj", query_rows, key_past, preferred_element_type=jnp.float32)
        * scale_factor
    )
    own_score = (
        jnp.einsum("shmd,shmd->shm", query_rows, key_rows, preferred_element_type=jnp.float32)
        * scale_factor
    )
    valid_mask = lax.iota(jnp.int32, cache_len)[None, :] < lengths[:, None]
    past_exp = jnp.where(valid_mask[:, None, None, :], jnp.exp(past_score), 0.0)
    own_exp = jnp.exp(own_score)
    denominator = jnp.sum(past_exp, axis=-1) + own_exp
    past_prob = past_exp / denominator[..., None]
    own_prob = own_exp / denominator
    weight_past = (past_prob[:, :, 0] - lambda_head[None, :, None] * past_prob[:, :, 1]).astype(
        jnp.bfloat16
    )
    weight_own = (own_prob[:, :, 0] - lambda_head[None, :] * own_prob[:, :, 1]).astype(jnp.bfloat16)
    value_past = cache_value.reshape(seq_count, cache_len, head_count, val_size)
    head_mix = jnp.einsum(
        "shj,sjhe->she", weight_past, value_past, preferred_element_type=jnp.float32
    )
    own_value = value_rows.reshape(seq_count, head_count, val_size).astype(jnp.float32)
    head_mix = head_mix + weight_own.astype(jnp.float32)[..., None] * own_value
    head_out = (rms_scale(head_mix, sub_gain) * OUT_SCALE).astype(jnp.bfloat16)
    return (
        head_out.reshape(seq_count, head_count * val_size),
        key_rows.reshape(seq_count, -1),
        value_rows,
    )


LANES = 128
TURNED = (((0,), (0,)), ((), ()))
ACROSS = (((1,), (1,)), ((), ()))
SCALARS = pl.BlockSpec(memory_space=pltpu.SMEM)
WHOLE = pl.BlockSpec(memory_space=pltpu.VMEM)


def mm(a, b):
    return jnp.dot(a, b, preferred_element_type=jnp.float32)


def routes_kernel(ids_ref, turned_ref, logits_ref, out_ref):
    ids = ids_ref[...]
    turned = turned_ref[...]
    count, top = ids.shape
    logits = logits_ref[...]
    grown = jnp.exp(logits - jnp.max(logits, axis=1, keepdims=True))
    weight = grown / jnp.sum(grown, axis=1, keepdims=True)
    upper = weight.astype(jnp.bfloat16).astype(jnp.float32)
    lower = weight - upper
    row = lax.broadcasted_iota(jnp.int32, (count, count), 0)
    col = lax.broadcasted_iota(jnp.int32, (count, count), 1)
    lane = lax.broadcasted_iota(jnp.int32, (count, LANES), 1)
    packed = jnp.zeros((count, LANES), jnp.float32)
    for k in range(top):
        mine = ids[:, k : k + 1]
        same = jnp.zeros((count, count), jnp.float32)
        for other in range(top):
            same = same + jnp.where(mine == turned[other : other + 1, :], 1.0, 0.0)
        rank = jnp.sum(jnp.where(col < row, same, 0.0), axis=1, keepdims=True)
        code = mine.astype(jnp.float32) * CAP + rank
        packed = jnp.where(lane == k, code, packed)
        packed = jnp.where(lane == top + k, upper[:, k : k + 1], packed)
        packed = jnp.where(lane == 2 * top + k, lower[:, k : k + 1], packed)
    out_ref[...] = packed


def mix_kernel(tp_ref, parts_ref, full_ref, lean_ref, gain_ref, routes_ref, res_ref, out_ref, *, top):
    residual = full_ref[...]
    tp = parts_ref.shape[0]
    for k in range(tp):
        residual = residual + parts_ref[k]
    total = residual.shape[1]
    width = total // tp
    inverse = lax.rsqrt(jnp.sum(residual * residual, axis=1, keepdims=True) / total + EPSILON)
    logit = jnp.sum(residual * lean_ref[...], axis=1, keepdims=True) * inverse
    branch = jax.nn.sigmoid(logit)
    upper = branch.astype(jnp.bfloat16).astype(jnp.float32)
    own = jnp.zeros((residual.shape[0], width), jnp.float32)
    for k in range(tp):
        own = own + jnp.where(tp_ref[0] == k, residual[:, k * width : (k + 1) * width], 0.0)
    res_ref[...] = own
    mix = (own * inverse * gain_ref[...]).astype(jnp.bfloat16)
    routes = routes_ref[...]
    lane = lax.broadcasted_iota(jnp.int32, routes.shape, 1)
    routes = jnp.where(lane == 3 * top, upper, routes)
    routes = jnp.where(lane == 3 * top + 1, branch - upper, routes)
    notes = routes.astype(jnp.bfloat16)
    for k in range(out_ref.shape[0]):
        out_ref[k, :, :width] = mix
        out_ref[k, :, width:] = notes


def slot_hits(notes, first, line, plane, top):
    total = notes.shape[0]
    slots = plane * line * CAP
    row = lax.broadcasted_iota(jnp.int32, (total, slots), 0)
    col = lax.broadcasted_iota(jnp.int32, (total, slots), 1)
    code = (first + col // (line * CAP)) * CAP + col % CAP
    here = row // (total // line) == (col // CAP) % line
    code = jnp.where(here, code, -1).astype(jnp.float32)
    return [notes[:, k : k + 1] == code for k in range(top)]


def outward_kernel(first_ref, seen_ref, out_ref, *, top):
    line, seq, wide = seen_ref.shape
    width = wide - LANES
    plane, tp, items, _ = out_ref.shape
    slots = line * CAP
    notes = seen_ref[:, :, width:].reshape(line * seq, LANES).astype(jnp.float32)
    rows = seen_ref[:, :, :width].reshape(line * seq, width)
    hits = slot_hits(notes, first_ref[0], line, plane, top)
    select = sum(jnp.where(h, 1.0, 0.0) for h in hits).astype(jnp.bfloat16)
    placed = lax.dot_general(select, rows, TURNED, preferred_element_type=jnp.float32)
    placed = placed.astype(jnp.bfloat16).reshape(plane, slots, width)
    for k in range(tp):
        out_ref[:, k, :slots, :] = placed
    dealt = rows.astype(jnp.float32).reshape(plane, tp, items - slots, width)
    out_ref[:, :, slots:, :] = dealt.astype(jnp.bfloat16)


def weights_kernel(first_ref, seen_ref, upper_ref, lower_ref, *, top, plane):
    line, seq, wide = seen_ref.shape
    width = wide - LANES
    notes = seen_ref[:, :, width:].reshape(line * seq, LANES).astype(jnp.float32)
    hits = slot_hits(notes, first_ref[0], line, plane, top)
    upper_ref[...] = sum(
        jnp.where(h, notes[:, top + k : top + k + 1], 0.0) for k, h in enumerate(hits)
    ).astype(jnp.bfloat16)
    lower_ref[...] = sum(
        jnp.where(h, notes[:, 2 * top + k : 2 * top + k + 1], 0.0) for k, h in enumerate(hits)
    ).astype(jnp.bfloat16)


def expert_kernel(seen_ref, gate_ref, up_ref, down_ref, dense_ref, out_ref, *, slots):
    plane, tp, items, width = seen_ref.shape
    gate_pre = up_pre = 0.0
    for k in range(tp):
        rows = seen_ref[:, k, :slots, :].reshape(plane * slots, width)
        gate_pre = gate_pre + mm(rows, gate_ref[0, k * width : (k + 1) * width, :])
        up_pre = up_pre + mm(rows, up_ref[0, k * width : (k + 1) * width, :])
    act = clamped_unit(gate_pre, up_pre).astype(jnp.bfloat16)
    for k in range(tp):
        part = mm(act, down_ref[0, :, k * width : (k + 1) * width]).astype(jnp.bfloat16)
        out_ref[:, k, :slots, :] = part.reshape(plane, slots, width)
    units = dense_ref.shape[2] // 3
    dealt = items - slots
    gate_pre = up_pre = 0.0
    for k in range(tp):
        rows = seen_ref[:, k, slots:, :].astype(jnp.float32).reshape(plane * dealt, width)
        rows = rows.astype(jnp.bfloat16)
        gate = dense_ref[:, k, :units, :].reshape(plane * units, width)
        up = dense_ref[:, k, units : 2 * units, :].reshape(plane * units, width)
        gate_pre = gate_pre + lax.dot_general(
            rows, gate, ACROSS, preferred_element_type=jnp.float32
        )
        up_pre = up_pre + lax.dot_general(rows, up, ACROSS, preferred_element_type=jnp.float32)
    act = (gate_pre / (1.0 + jnp.exp(-gate_pre)) * up_pre).astype(jnp.bfloat16)
    for k in range(tp):
        down = dense_ref[:, k, 2 * units :, :].reshape(plane * units, width)
        part = mm(act, down).reshape(plane, dealt, width)
        out_ref[:, k, slots:, :] = part.astype(jnp.bfloat16)


def inward_kernel(seen_ref, line_ref, upper_ref, lower_ref, out_ref, *, top):
    line, seq, width = out_ref.shape
    plane, tp, items, _ = seen_ref.shape
    slots = line * CAP
    whole = jnp.zeros((plane, slots, width), jnp.float32)
    for k in range(tp):
        whole = whole + seen_ref[:, k, :slots, :].astype(jnp.float32)
    whole = whole.astype(jnp.bfloat16).reshape(plane * slots, width)
    routed = mm(upper_ref[...], whole) + mm(lower_ref[...], whole)
    dense = seen_ref[:, :, slots:, :].astype(jnp.float32).reshape(line * seq, width)
    notes = line_ref[:, :, width:].reshape(line * seq, LANES).astype(jnp.float32)
    branch = notes[:, 3 * top : 3 * top + 1] + notes[:, 3 * top + 1 : 3 * top + 2]
    back = (routed + branch * dense).astype(jnp.bfloat16)
    out_ref[...] = back.reshape(line, seq, width)


def shaped(shape, dtype):
    return jax.ShapeDtypeStruct(shape, dtype)


def body(
    hidden_in,
    norm_gain_attn,
    query_weight,
    key_weight,
    value_weight,
    query_gain,
    key_gain,
    lambda_head,
    sub_gain,
    out_weight,
    cache_key,
    cache_value,
    lengths,
    norm_gain_mix,
    route_ids,
    route_logits,
    expert_gate,
    expert_up,
    expert_down,
    dense_gate,
    dense_up,
    dense_down,
    branch_gate,
):
    seq, top = route_ids.shape
    width = hidden_in.shape[1]
    units = dense_down.shape[0]
    line = lax.axis_size("ep_0")
    plane = lax.axis_size("ep_1") * lax.axis_size("ep_2")
    tp = lax.axis_size("tp")
    slots = line * CAP
    dealt = line * seq // (plane * tp)
    lean = norm_gain_mix * branch_gate
    lean_high = lean.astype(jnp.bfloat16)
    lean_low = (lean - lean_high.astype(jnp.float32)).astype(jnp.bfloat16)
    extra = jnp.zeros((8, width), jnp.bfloat16).at[0].set(lean_high).at[1].set(lean_low)
    mine = jnp.concatenate([hidden_in, dense_gate.T, dense_up.T, dense_down, extra], axis=0)
    pieces = from_everyone(mine, "tp")
    full_rows = jnp.concatenate([pieces[k, :seq] for k in range(tp)], axis=1).astype(jnp.float32)
    past = seq + 3 * units
    lean_full = jnp.concatenate(
        [
            pieces[k, past : past + 1].astype(jnp.float32)
            + pieces[k, past + 1 : past + 2].astype(jnp.float32)
            for k in range(tp)
        ],
        axis=1,
    )
    width_total = full_rows.shape[1]
    dense_weights = from_everyone(pieces[:, seq:past], PLANE).reshape(plane, tp, 3 * units, width)
    routes = pl.pallas_call(
        routes_kernel, out_shape=shaped((seq, LANES), jnp.float32), name="routes"
    )(route_ids, route_ids.T, route_logits)
    normed = rms_scale(full_rows, norm_gain_attn).astype(jnp.bfloat16)
    head_out, key_rows, value_rows = attend(
        normed,
        query_weight,
        key_weight,
        value_weight,
        query_gain,
        key_gain,
        lambda_head,
        sub_gain,
        cache_key,
        cache_value,
        lengths,
    )
    head_terms = jnp.dot(head_out, out_weight, preferred_element_type=jnp.float32)
    head_terms, dense_weights = lax.optimization_barrier((head_terms, dense_weights))
    parts = from_everyone(head_terms, "tp")
    residual, message = pl.pallas_call(
        lambda *refs: mix_kernel(*refs, top=top),
        out_shape=(
            shaped((seq, width), jnp.float32),
            shaped((line, seq, width + LANES), jnp.bfloat16),
        ),
        in_specs=[SCALARS] + [WHOLE] * 5,
        name="mix",
    )(
        lax.axis_index("tp").reshape(1),
        parts,
        full_rows,
        lean_full,
        norm_gain_mix[None, :],
        routes,
    )
    seen = lax.all_to_all(message, "ep_0", 0, 0, tiled=True)
    first = (lax.axis_index("ep_0") * plane).reshape(1)
    outward = pl.pallas_call(
        lambda *refs: outward_kernel(*refs, top=top),
        out_shape=shaped((plane, tp, slots + dealt, width), jnp.bfloat16),
        in_specs=[SCALARS, WHOLE],
        name="outward",
    )(first, seen)
    arrived = lax.all_to_all(
        outward.reshape(plane * tp, slots + dealt, width), BLOCK, 0, 0, tiled=True
    ).reshape(plane, tp, slots + dealt, width)
    upper, lower = pl.pallas_call(
        lambda *refs: weights_kernel(*refs, top=top, plane=plane),
        out_shape=(
            shaped((line * seq, plane * slots), jnp.bfloat16),
            shaped((line * seq, plane * slots), jnp.bfloat16),
        ),
        in_specs=[SCALARS, WHOLE],
        name="weights",
    )(first, seen)
    sent = pl.pallas_call(
        lambda *refs: expert_kernel(*refs, slots=slots),
        out_shape=shaped((plane, tp, slots + dealt, width), jnp.bfloat16),
        name="experts",
    )(arrived, expert_gate, expert_up, expert_down, dense_weights)
    returned = lax.all_to_all(
        sent.reshape(plane * tp, slots + dealt, width), BLOCK, 0, 0, tiled=True
    ).reshape(plane, tp, slots + dealt, width)
    back = pl.pallas_call(
        lambda *refs: inward_kernel(*refs, top=top),
        out_shape=shaped((line, seq, width), jnp.bfloat16),
        name="inward",
    )(returned, seen, upper, lower)
    home = lax.all_to_all(back, "ep_0", 0, 0, tiled=True)
    layer_out = (residual + jnp.sum(home.astype(jnp.float32), axis=0)).astype(jnp.bfloat16)
    return (layer_out, key_rows, value_rows)


def solution(mesh):
    split = Mesh(mesh.devices.reshape(16, 4, 2, mesh.shape["tp"]), ("ep_0", "ep_1", "ep_2", "tp"))
    in_specs = (
        P(EP, "tp"),
        P(),
        P(None, "tp"),
        P(None, "tp"),
        P(None, "tp"),
        P(),
        P(),
        P("tp"),
        P(),
        P("tp", None),
        P(EP, None, "tp"),
        P(EP, None, "tp"),
        P(EP),
        P("tp"),
        P(EP, None),
        P(EP, None),
        P(EP, None, "tp"),
        P(EP, None, "tp"),
        P(EP, "tp", None),
        P("tp", EP),
        P("tp", EP),
        P(EP, "tp"),
        P("tp"),
    )
    out_specs = (P(EP, "tp"), P(EP, "tp"), P(EP, "tp"))
    return jax.shard_map(body, mesh=split, in_specs=in_specs, out_specs=out_specs, check_vma=False)
```

time: 160 us -> 144 us (0.900)
  waiting for transfers between devices: 79 us -> 55 us
  blocking collectives: 0 us -> 17.7 us
  Pallas kernels: 0 us -> 13.9 us
  starting transfers between devices: 49.6 us -> 37.4 us
  other arithmetic: 8.95 us -> 3.28 us
  matrix products: 5.99 us -> 1.4 us
    all_to_all x6 -> x3, waiting for transfers between devices: 43.4 us -> 16.9 us  [from_everyone(): return lax.all_to_all(copies, axis, split_axis=0, concat_axis=0, tiled=True)]
    all_to_all x6 -> x3, starting transfers between devices: 37.1 us -> 13.2 us  [from_everyone(): return lax.all_to_all(copies, axis, split_axis=0, concat_axis=0, tiled=True)]
    all_to_all x0 -> x1, blocking collectives: none -> 17.7 us  [body(): lax.all_to_all(outward.reshape(plane * tp, slots + dealt, width), BLOCK,...]
    pallas_call x0 -> x6, Pallas kernels: none -> 13.9 us  [the longest x1 3.66 us: body(): pl.pallas_call(lambda *refs: expert_kernel(*refs, slots=slots), out_shape...]
    all_to_all x3, starting transfers between devices: 12.5 us -> 24.2 us  [the longest x1 15.2 us: body(): seen = lax.all_to_all(message, 'ep_0', 0, 0, tiled=True)]
    unnamed x29 -> x53, local copies, waits for them, and re-layouts: 3.35 us -> 9.39 us
    dot_general x13 -> x0, matrix products: 4.58 us -> none  [the longest x1 1.41 us: body(): jnp.dot(item_rows, expert_gate[0], preferred_element_type=jnp.float32)]
    all_to_all x3, waiting for transfers between devices: 35.6 us -> 38.1 us  [the longest x1 14.5 us: body(): seen = lax.all_to_all(message, 'ep_0', 0, 0, tiled=True)]
  transfers between devices with their start and end apart: 9 -> 6, of which waited for: 8 -> 6; matrix products, arithmetic and copies ran while one was open for 12% -> 4% of each run, Pallas kernels for 0% -> 3%
where the time goes in v2:
time: 144 us; the launch traced here: 143 us
  waiting for transfers between devices  55 us (38%)
  starting transfers between devices  37.4 us (26%)
  blocking collectives  17.7 us (12%)
  Pallas kernels  13.9 us (10%)
  local copies, waits for them, and re-layouts  12.6 us (9%)
  other arithmetic  3.28 us (2%)
  between operations  1.54 us (1%)
    all_to_all x1, blocking collectives, body(): lax.all_to_all(outward.reshape(plane * tp, slots + dealt, width), BLOCK,...  17.7 us
    all_to_all x3, waiting for transfers between devices, from_everyone(): return lax.all_to_all(copies, axis, split_axis=0, concat_axis=0, tiled=True)  16.9 us
    all_to_all x1, starting transfers between devices, body(): seen = lax.all_to_all(message, 'ep_0', 0, 0, tiled=True)  15.2 us
    all_to_all x1, waiting for transfers between devices, body(): seen = lax.all_to_all(message, 'ep_0', 0, 0, tiled=True)  14.5 us
    all_to_all x3, starting transfers between devices, from_everyone(): return lax.all_to_all(copies, axis, split_axis=0, concat_axis=0, tiled=True)  13.2 us
    all_to_all x1, waiting for transfers between devices, body(): home = lax.all_to_all(back, 'ep_0', 0, 0, tiled=True)  12.8 us
    all_to_all x1, waiting for transfers between devices, body(): lax.all_to_all(sent.reshape(plane * tp, slots + dealt, width), BLOCK, 0,...  10.8 us
    unnamed x53, local copies, waits for them, and re-layouts  9.39 us
  transfers between devices with their start and end apart: 6, of which 6 were waited for; matrix products, arithmetic and copies ran while one was open for 4% of the time, Pallas kernels for 3%

profile of v2, /device:TPU:32, one launch (start us, length us, event | category | flops | bytes accessed | tf_op | source)
XLA Modules:
  0.0 142.8 jit_solution(4450822856364267326)
XLA Ops:
  0.7 0.8 constant_dynamic-update-slice_fusion.4
  1.5 0.7 copy-done.11
  2.2 0.7 copy-done.12
  2.9 0.7 copy-done.13
  3.6 0.7 broadcast_in_dim.21
  4.3 4.6 %all-to-all-start = ((bf16[4,72,256]{2,1,0:T(8,128)(2,1)}), bf16[4,72,256]{2,1,0:T(8,128)(2,1)S(1)}, u32[]{:S(2)}, u32[]{:S(2)}) async-start(bf16[4,72,256]{2,1,0:T(8,128)(2,1)} %broadcast_in_dim.21), calls=%async_computation | async-start | bytes 294912 | tf_op jit(solution)/shard_map/all_to_all | solution.py:25
  8.9 1.5 %copy.29 = bf16[16,256,128]{1,2,0:T(8,128)(2,1)S(1)} copy(bf16[16,256,128]{2,1,0:T(8,128)(2,1)} %param.37) | data formatting | bytes 2097152 | tf_op args[10]
  11.4 0.7 copy.30.ids_ref
  12.1 0.7 copy.31.logits_ref
  12.7 1.7 %routes.1.refs_5_ = f32[16,128]{1,0:T(8,128)} custom-call(s32[16,6]{1,0:T(8,128)} %copy.30.ids_ref, s32[6,16]{1,0:T(8,128)} %bitcast.70, f32[16,6]{1,0:T(8,128)} %copy.31.logits_ref), custom_call_target="tpu_custom_call" | custom-call | tf_op jit(solution)/shard_map/routes/pallas_call | solution.py:307
  14.4 0.5 all-to-all-done
  14.9 0.1 multiply_reduce_fusion
  15.1 0.2 fusion.28
  15.5 0.2 fusion.29
  15.7 0.1 reduce_sum.57
  16.0 0.2 fusion.5
  16.3 0.2 fusion.8
  16.6 0.1 fusion.2
  16.8 0.9 broadcast_in_dim.23
  17.7 4.3 %all-to-all-start.1 = ((bf16[8,4,48,256]{3,2,1,0:T(8,128)(2,1)}), bf16[8,4,48,256]{3,2,1,0:T(8,128)(2,1)S(1)}, u32[]{:S(2)}, u32[]{:S(2)}) async-start(bf16[8,4,48,256]{3,2,1,0:T(8,128)(2,1)} %broadcast_in_dim.23), calls=%async_computation.1 | async-start | bytes 1572864 | tf_op jit(solution)/shard_map/all_to_all | solution.py:25
  22.0 0.2 fusion.6
  22.3 0.7 copy-done.21
  23.0 0.3 multiply_reduce_fusion.1
  23.4 0.5 copy-done.14
  24.0 0.2 fusion.11
  24.2 10.9 %all-to-all-done.1.refs_4_ = bf16[8,4,48,256]{3,2,1,0:T(8,128)(2,1)S(1)} async-done(((bf16[8,4,48,256]{3,2,1,0:T(8,128)(2,1)}), bf16[8,4,48,256]{3,2,1,0:T(8,128)(2,1)S(1)}, u32[]{:S(2)}, u32[]{:S(2)}) %all-to-all-start.1) | async-done | bytes 786464 | tf_op jit(solution)/shard_map/all_to_all | solution.py:25
  35.1 0.8 broadcast_in_dim.24
  35.9 4.3 %all-to-all-start.2 = ((f32[4,16,1024]{2,1,0:T(8,128)}), f32[4,16,1024]{2,1,0:T(8,128)S(1)}, u32[]{:S(2)}, u32[]{:S(2)}) async-start(f32[4,16,1024]{2,1,0:T(8,128)} %broadcast_in_dim.24), calls=%async_computation.2 | async-start | bytes 524288 | tf_op jit(solution)/shard_map/all_to_all | solution.py:25
  40.2 0.6 pad_maximum_fusion.refs_3_
  40.8 0.6 maximum_convert_fusion.refs_2_
  41.5 5.5 %all-to-all-done.2.refs_1_ = f32[4,16,1024]{2,1,0:T(8,128)S(1)} async-done(((f32[4,16,1024]{2,1,0:T(8,128)}), f32[4,16,1024]{2,1,0:T(8,128)S(1)}, u32[]{:S(2)}, u32[]{:S(2)}) %all-to-all-start.2) | async-done | bytes 262176 | tf_op jit(solution)/shard_map/all_to_all | solution.py:25
  46.9 0.7 copy-done.4
  47.6 1.8 %mix.1 = (f32[16,256]{1,0:T(8,128)}, bf16[16,16,384]{2,1,0:T(8,128)(2,1)}) custom-call(s32[1]{0:T(128)} %bitcast.refs_0_, f32[4,16,1024]{2,1,0:T(8,128)} %copy-done.4, f32[16,1024]{1,0:T(8,128)} %maximum_convert_fusion.refs_2_, f32[1,1024]{1,0:T(1,128)} %pad_maximum_fusion.refs_3_, f32[1,256]{1,0:T(1,128)} %bitcast.71, f32[16,128]{1,0:T(8,128)} %routes.1.refs_5_), custom_call_target="tpu_custom_call" | custom-call | tf_op jit(solution)/shard_map/mix/pallas_call | solution.py:327
  49.4 15.2 %all-to-all-start.3 = ((bf16[16,16,384]{2,1,0:T(8,128)(2,1)}), bf16[16,16,384]{2,1,0:T(8,128)(2,1)S(1)}, u32[]{:S(2)}, u32[]{:S(2)}) async-start(bf16[16,16,384]{2,1,0:T(8,128)(2,1)} %get-tuple-element.35), calls=%async_computation.3 | async-start | bytes 393216 | tf_op jit(solution)/shard_map/all_to_all | solution.py:343
  64.6 14.5 %all-to-all-done.3.refs_1_ = bf16[16,16,384]{2,1,0:T(8,128)(2,1)S(1)} async-done(((bf16[16,16,384]{2,1,0:T(8,128)(2,1)}), bf16[16,16,384]{2,1,0:T(8,128)(2,1)S(1)}, u32[]{:S(2)}, u32[]{:S(2)}) %all-to-all-start.3) | async-done | bytes 196640 | tf_op jit(solution)/shard_map/all_to_all | solution.py:343
  79.2 0.7 copy-done.2
  79.8 2.3 %outward.1 = bf16[8,4,40,256]{3,2,1,0:T(8,128)(2,1)} custom-call(s32[1]{0:T(128)} %bitcast.24.refs_0_, bf16[16,16,384]{2,1,0:T(8,128)(2,1)} %copy-done.2), custom_call_target="tpu_custom_call" | custom-call | tf_op jit(solution)/shard_map/outward/pallas_call | solution.py:345
  82.1 17.7 %all_to_all.35 = bf16[32,40,256]{2,1,0:T(8,128)(2,1)} all-to-all(bf16[32,40,256]{2,1,0:T(8,128)(2,1)} %bitcast.66), channel_id=1, replica_groups=mesh['ep_0'=16,'ep_1'=4,'ep_2'=2,'tp'=4] {'ep_1','ep_2','tp'}, dimensions={0} | all-to-all | bytes 1310720 | tf_op jit(solution)/shard_map/all_to_all | solution.py:351
  99.8 3.7 %experts.1 = bf16[8,4,40,256]{3,2,1,0:T(8,128)(2,1)} custom-call(bf16[8,4,40,256]{3,2,1,0:T(8,128)(2,1)} %bitcast.64, bf16[1,1024,256]{2,1,0:T(8,128)(2,1)} %refs_1_.1, bf16[1,1024,256]{2,1,0:T(8,128)(2,1)} %refs_2_.1, bf16[1,256,1024]{2,1,0:T(8,128)(2,1)} %refs_3_.1, bf16[8,4,48,256]{3,2,1,0:T(8,128)(2,1)} %copy-done.1), custom_call_target="tpu_custom_call" | custom-call | tf_op jit(solution)/shard_map/experts/pallas_call | solution.py:363
  103.4 3.9 %all-to-all-start.5 = ((bf16[32,40,256]{2,1,0:T(8,128)(2,1)}), bf16[32,40,256]{2,1,0:T(8,128)(2,1)S(1)}, u32[]{:S(2)}, u32[]{:S(2)}) async-start(bf16[32,40,256]{2,1,0:T(8,128)(2,1)} %bitcast.63), calls=%async_computation.5 | async-start | bytes 1310720 | tf_op jit(solution)/shard_map/all_to_all | solution.py:368
  107.4 2.3 %weights.1 = (bf16[256,256]{1,0:T(8,128)(2,1)}, bf16[256,256]{1,0:T(8,128)(2,1)}) custom-call(s32[1]{0:T(128)} %bitcast.24.refs_0_, bf16[16,16,384]{2,1,0:T(8,128)(2,1)} %copy-done.2), custom_call_target="tpu_custom_call" | custom-call | tf_op jit(solution)/shard_map/weights/pallas_call | solution.py:354
  109.7 10.8 %all-to-all-done.5 = bf16[32,40,256]{2,1,0:T(8,128)(2,1)S(1)} async-done(((bf16[32,40,256]{2,1,0:T(8,128)(2,1)}), bf16[32,40,256]{2,1,0:T(8,128)(2,1)S(1)}, u32[]{:S(2)}, u32[]{:S(2)}) %all-to-all-start.5) | async-done | bytes 655392 | tf_op jit(solution)/shard_map/all_to_all | solution.py:368
  120.4 0.9 copy-done.3
  121.3 2.2 %inward.1 = bf16[16,16,256]{2,1,0:T(8,128)(2,1)} custom-call(bf16[8,4,40,256]{3,2,1,0:T(8,128)(2,1)} %bitcast.65, bf16[16,16,384]{2,1,0:T(8,128)(2,1)} %copy-done.2, bf16[256,256]{1,0:T(8,128)(2,1)} %get-tuple-element.37.refs_2_, bf16[256,256]{1,0:T(8,128)(2,1)} %get-tuple-element.38.refs_3_), custom_call_target="tpu_custom_call" | custom-call | tf_op jit(solution)/shard_map/inward/pallas_call | solution.py:371
  123.5 5.1 %all-to-all-start.6 = ((bf16[16,16,256]{2,1,0:T(8,128)(2,1)}), bf16[16,16,256]{2,1,0:T(8,128)(2,1)S(1)}, u32[]{:S(2)}, u32[]{:S(2)}) async-start(bf16[16,16,256]{2,1,0:T(8,128)(2,1)} %inward.1), calls=%async_computation.6 | async-start | bytes 262144 | tf_op jit(solution)/shard_map/all_to_all | solution.py:376
  128.7 0.6 multiply_convert_fusion.3
  129.3 12.8 %all-to-all-done.6 = bf16[16,16,256]{2,1,0:T(8,128)(2,1)S(1)} async-done(((bf16[16,16,256]{2,1,0:T(8,128)(2,1)}), bf16[16,16,256]{2,1,0:T(8,128)(2,1)S(1)}, u32[]{:S(2)}, u32[]{:S(2)}) %all-to-all-start.6) | async-done | bytes 131104 | tf_op jit(solution)/shard_map/all_to_all | solution.py:376
  142.2 0.6 add_convert_fusion
  (69 shorter events, 1.3 us)
Async XLA Ops:
  0.6 21.4 %copy-start = (bf16[16,256,128]{2,1,0:T(8,128)(2,1)S(1)}, bf16[16,256,128]{2,1,0:T(8,128)(2,1)}, u32[]{:S(2)}) copy-start(bf16[16,256,128]{2,1,0:T(8,128)(2,1)} %param.38) | copy-start | bytes 3145732
  0.6 0.8 copy-start.15
  0.7 0.8 copy-start.17
  1.5 0.7 copy-start.11
  2.2 0.7 copy-start.12
  2.9 0.7 copy-start.13
  4.3 4.6 %copy-start.19 = (s32[16]{0:T(128)S(1)}, s32[16]{0:T(128)}, u32[]{:S(2)}) copy-start(s32[16]{0:T(128)} %param.39) | copy-start | bytes 196
  4.3 10.7 %all-to-all-start = ((bf16[4,72,256]{2,1,0:T(8,128)(2,1)}), bf16[4,72,256]{2,1,0:T(8,128)(2,1)S(1)}, u32[]{:S(2)}, u32[]{:S(2)}) async-start(bf16[4,72,256]{2,1,0:T(8,128)(2,1)} %broadcast_in_dim.21), calls=%async_computation | async-start | bytes 294912 | tf_op jit(solution)/shard_map/all_to_all | solution.py:25
  8.9 1.6 %copy-start.20 = (f32[128]{0:T(128)S(1)}, f32[128]{0:T(128)}, u32[]{:S(2)}) copy-start(f32[128]{0:T(128)} %param.33) | copy-start | bytes 1540
  8.9 1.7 %copy-start.22 = (f32[128]{0:T(128)S(1)}, f32[128]{0:T(128)}, u32[]{:S(2)}) copy-start(f32[128]{0:T(128)} %param.32) | copy-start | bytes 1540
  8.9 6.1 %copy-start.5 = (bf16[1024,128]{1,0:T(8,128)(2,1)S(1)}, bf16[1024,128]{1,0:T(8,128)(2,1)}, u32[]{:S(2)}) copy-start(bf16[1024,128]{1,0:T(8,128)(2,1)} %param.30) | copy-start | bytes 786436
  10.5 0.8 copy-start.9
  10.6 4.5 %copy-start.8 = (f32[1024]{0:T(1024)S(1)}, f32[1024]{0:T(1024)}, u32[]{:S(2)}) copy-start(f32[1024]{0:T(1024)} %param.28) | copy-start | bytes 12292
  11.4 0.7 copy-start.16
  12.1 3.4 %copy-start.6 = (bf16[1024,128]{1,0:T(8,128)(2,1)S(1)}, bf16[1024,128]{1,0:T(8,128)(2,1)}, u32[]{:S(2)}) copy-start(bf16[1024,128]{1,0:T(8,128)(2,1)} %param.29) | copy-start | bytes 786436
  17.7 17.4 %all-to-all-start.1 = ((bf16[8,4,48,256]{3,2,1,0:T(8,128)(2,1)}), bf16[8,4,48,256]{3,2,1,0:T(8,128)(2,1)S(1)}, u32[]{:S(2)}, u32[]{:S(2)}) async-start(bf16[8,4,48,256]{3,2,1,0:T(8,128)(2,1)} %broadcast_in_dim.23), calls=%async_computation.1 | async-start | bytes 1572864 | tf_op jit(solution)/shard_map/all_to_all | solution.py:25
  22.0 1.0 copy-start.21
  22.3 1.6 %copy-start.7 = (bf16[128,1024]{1,0:T(8,128)(2,1)S(1)}, bf16[128,1024]{1,0:T(8,128)(2,1)}, u32[]{:S(2)}) copy-start(bf16[128,1024]{1,0:T(8,128)(2,1)} %param.36) | copy-start | bytes 786436
  23.3 0.6 copy-start.14
  23.3 0.7 copy-start.18
  35.1 14.3 %copy-start.1 = (bf16[8,4,48,256]{3,2,1,0:T(8,128)(2,1)}, bf16[8,4,48,256]{3,2,1,0:T(8,128)(2,1)S(1)}, u32[]{:S(2)}) copy-start(bf16[8,4,48,256]{3,2,1,0:T(8,128)(2,1)S(1)} %all-to-all-done.1.refs_4_) | copy-start | bytes 2359300
  35.9 11.0 %all-to-all-start.2 = ((f32[4,16,1024]{2,1,0:T(8,128)}), f32[4,16,1024]{2,1,0:T(8,128)S(1)}, u32[]{:S(2)}, u32[]{:S(2)}) async-start(f32[4,16,1024]{2,1,0:T(8,128)} %broadcast_in_dim.24), calls=%async_computation.2 | async-start | bytes 524288 | tf_op jit(solution)/shard_map/all_to_all | solution.py:25
  46.9 0.7 copy-start.4
  49.4 29.7 %all-to-all-start.3 = ((bf16[16,16,384]{2,1,0:T(8,128)(2,1)}), bf16[16,16,384]{2,1,0:T(8,128)(2,1)S(1)}, u32[]{:S(2)}, u32[]{:S(2)}) async-start(bf16[16,16,384]{2,1,0:T(8,128)(2,1)} %get-tuple-element.35), calls=%async_computation.3 | async-start | bytes 393216 | tf_op jit(solution)/shard_map/all_to_all | solution.py:343
  79.2 0.7 copy-start.2
  103.4 17.0 %all-to-all-start.5 = ((bf16[32,40,256]{2,1,0:T(8,128)(2,1)}), bf16[32,40,256]{2,1,0:T(8,128)(2,1)S(1)}, u32[]{:S(2)}, u32[]{:S(2)}) async-start(bf16[32,40,256]{2,1,0:T(8,128)(2,1)} %bitcast.63), calls=%async_computation.5 | async-start | bytes 1310720 | tf_op jit(solution)/shard_map/all_to_all | solution.py:368
  120.4 0.9 copy-start.3
  123.5 18.7 %all-to-all-start.6 = ((bf16[16,16,256]{2,1,0:T(8,128)(2,1)}), bf16[16,16,256]{2,1,0:T(8,128)(2,1)S(1)}, u32[]{:S(2)}, u32[]{:S(2)}) async-start(bf16[16,16,256]{2,1,0:T(8,128)(2,1)} %inward.1), calls=%async_computation.6 | async-start | bytes 262144 | tf_op jit(solution)/shard_map/all_to_all | solution.py:376
  129.3 12.8 %copy-start.10 = (f32[16,256]{1,0:T(8,128)S(1)}, f32[16,256]{1,0:T(8,128)}, u32[]{:S(2)}) copy-start(f32[16,256]{1,0:T(8,128)} %get-tuple-element.34) | copy-start | bytes 49156

commit v3 on v2

--- a/solution.py
+++ b/solution.py
@@ -5,11 +5,12 @@
 from jax import lax
 from jax.experimental import pallas as pl
 from jax.experimental.pallas import tpu as pltpu
+
 from jax.sharding import Mesh
 from jax.sharding import PartitionSpec as P
 
+
 EP = ("ep_0", "ep_1", "ep_2")
-PLANE = ("ep_1", "ep_2")
 BLOCK = ("ep_1", "ep_2", "tp")
 CAP = 2
 
@@ -103,11 +104,36 @@
 TURNED = (((0,), (0,)), ((), ()))
 ACROSS = (((1,), (1,)), ((), ()))
 SCALARS = pl.BlockSpec(memory_space=pltpu.SMEM)
+LIMIT = pltpu.CompilerParams(vmem_limit_bytes=12 * 2**20)
 WHOLE = pl.BlockSpec(memory_space=pltpu.VMEM)
 
 
 def mm(a, b):
     return jnp.dot(a, b, preferred_element_type=jnp.float32)
+
+
+def far(x):
+    return pltpu.with_memory_space_constraint(x, pltpu.HBM)
+
+
+def near(x):
+    return pltpu.with_memory_space_constraint(x, pltpu.VMEM)
+
+
+def opening_kernel(hidden_ref, gate_ref, up_ref, down_ref, gain_ref, branch_ref, out_ref):
+    lean = gain_ref[...] * branch_ref[...]
+    high = lean.astype(jnp.bfloat16).astype(jnp.float32)
+    row = lax.broadcasted_iota(jnp.int32, (8, lean.shape[1]), 0)
+    extra = jnp.where(row == 0, high, jnp.where(row == 1, lean - high, 0.0))
+    extra = extra.astype(jnp.bfloat16)
+    seq, units = hidden_ref.shape[0], down_ref.shape[0]
+    past = seq + 3 * units
+    for k in range(out_ref.shape[0]):
+        out_ref[k, :seq, :] = hidden_ref[...]
+        out_ref[k, seq : seq + units, :] = gate_ref[...]
+        out_ref[k, seq + units : seq + 2 * units, :] = up_ref[...]
+        out_ref[k, seq + 2 * units : past, :] = down_ref[...]
+        out_ref[k, past:, :] = extra
 
 
 def routes_kernel(ids_ref, turned_ref, logits_ref, out_ref):
@@ -136,15 +162,19 @@
     out_ref[...] = packed
 
 
-def mix_kernel(tp_ref, parts_ref, full_ref, lean_ref, gain_ref, routes_ref, res_ref, out_ref, *, top):
-    residual = full_ref[...]
-    tp = parts_ref.shape[0]
+def mix_kernel(tp_ref, parts_ref, pieces_ref, gain_ref, routes_ref, res_ref, out_ref, *, top):
+    tp, seq, _ = parts_ref.shape
+    past = pieces_ref.shape[1] - 8
+    residual = jnp.concatenate([pieces_ref[k, :seq, :] for k in range(tp)], axis=1)
+    residual = residual.astype(jnp.float32)
     for k in range(tp):
         residual = residual + parts_ref[k]
+    ends = [pieces_ref[k, past:, :].astype(jnp.float32) for k in range(tp)]
+    lean = jnp.concatenate([end[0:1] + end[1:2] for end in ends], axis=1)
     total = residual.shape[1]
     width = total // tp
     inverse = lax.rsqrt(jnp.sum(residual * residual, axis=1, keepdims=True) / total + EPSILON)
-    logit = jnp.sum(residual * lean_ref[...], axis=1, keepdims=True) * inverse
+    logit = jnp.sum(residual * lean, axis=1, keepdims=True) * inverse
     branch = jax.nn.sigmoid(logit)
     upper = branch.astype(jnp.bfloat16).astype(jnp.float32)
     own = jnp.zeros((residual.shape[0], width), jnp.float32)
@@ -203,7 +233,16 @@
     ).astype(jnp.bfloat16)
 
 
-def expert_kernel(seen_ref, gate_ref, up_ref, down_ref, dense_ref, out_ref, *, slots):
+def expert_kernel(
+    seen_ref, gate_ref, up_ref, down_hbm, own_hbm, other_hbm, out_ref, down_ref, dense_ref, sems, *, slots
+):
+    fetches = [
+        pltpu.make_async_copy(own_hbm, dense_ref.at[0], sems.at[0]),
+        pltpu.make_async_copy(other_hbm, dense_ref.at[1], sems.at[1]),
+        pltpu.make_async_copy(down_hbm, down_ref, sems.at[2]),
+    ]
+    for fetch in fetches:
+        fetch.start()
     plane, tp, items, width = seen_ref.shape
     gate_pre = up_pre = 0.0
     for k in range(tp):
@@ -211,31 +250,36 @@
         gate_pre = gate_pre + mm(rows, gate_ref[0, k * width : (k + 1) * width, :])
         up_pre = up_pre + mm(rows, up_ref[0, k * width : (k + 1) * width, :])
     act = clamped_unit(gate_pre, up_pre).astype(jnp.bfloat16)
-    for k in range(tp):
-        part = mm(act, down_ref[0, :, k * width : (k + 1) * width]).astype(jnp.bfloat16)
-        out_ref[:, k, :slots, :] = part.reshape(plane, slots, width)
-    units = dense_ref.shape[2] // 3
+    _, columns, _, rows_each, _ = dense_ref.shape
+    units = rows_each // 3
+    every = 2 * columns * units
     dealt = items - slots
+    fetches[0].wait()
+    fetches[1].wait()
     gate_pre = up_pre = 0.0
     for k in range(tp):
         rows = seen_ref[:, k, slots:, :].astype(jnp.float32).reshape(plane * dealt, width)
         rows = rows.astype(jnp.bfloat16)
-        gate = dense_ref[:, k, :units, :].reshape(plane * units, width)
-        up = dense_ref[:, k, units : 2 * units, :].reshape(plane * units, width)
+        gate = dense_ref[:, :, k, :units, :].reshape(every, width)
+        up = dense_ref[:, :, k, units : 2 * units, :].reshape(every, width)
         gate_pre = gate_pre + lax.dot_general(
             rows, gate, ACROSS, preferred_element_type=jnp.float32
         )
         up_pre = up_pre + lax.dot_general(rows, up, ACROSS, preferred_element_type=jnp.float32)
-    act = (gate_pre / (1.0 + jnp.exp(-gate_pre)) * up_pre).astype(jnp.bfloat16)
-    for k in range(tp):
-        down = dense_ref[:, k, 2 * units :, :].reshape(plane * units, width)
-        part = mm(act, down).reshape(plane, dealt, width)
+    dense_act = (gate_pre / (1.0 + jnp.exp(-gate_pre)) * up_pre).astype(jnp.bfloat16)
+    for k in range(tp):
+        down = dense_ref[:, :, k, 2 * units :, :].reshape(every, width)
+        part = mm(dense_act, down).reshape(plane, dealt, width)
         out_ref[:, k, slots:, :] = part.astype(jnp.bfloat16)
+    fetches[2].wait()
+    for k in range(tp):
+        part = mm(act, down_ref[0, :, k * width : (k + 1) * width]).astype(jnp.bfloat16)
+        out_ref[:, k, :slots, :] = part.reshape(plane, slots, width)
 
 
 def inward_kernel(seen_ref, line_ref, upper_ref, lower_ref, out_ref, *, top):
     line, seq, width = out_ref.shape
-    plane, tp, items, _ = seen_ref.shape
+    plane, tp, _, _ = seen_ref.shape
     slots = line * CAP
     whole = jnp.zeros((plane, slots, width), jnp.float32)
     for k in range(tp):
@@ -286,26 +330,26 @@
     tp = lax.axis_size("tp")
     slots = line * CAP
     dealt = line * seq // (plane * tp)
-    lean = norm_gain_mix * branch_gate
-    lean_high = lean.astype(jnp.bfloat16)
-    lean_low = (lean - lean_high.astype(jnp.float32)).astype(jnp.bfloat16)
-    extra = jnp.zeros((8, width), jnp.bfloat16).at[0].set(lean_high).at[1].set(lean_low)
-    mine = jnp.concatenate([hidden_in, dense_gate.T, dense_up.T, dense_down, extra], axis=0)
-    pieces = from_everyone(mine, "tp")
+    past = seq + 3 * units
+    mine = pl.pallas_call(
+        opening_kernel, out_shape=shaped((tp, past + 8, width), jnp.bfloat16), name="opening", compiler_params=LIMIT
+    )(
+        *map(
+            far,
+            (
+                hidden_in,
+                dense_gate.T,
+                dense_up.T,
+                dense_down,
+                norm_gain_mix[None, :],
+                branch_gate[None, :],
+            ),
+        )
+    )
+    pieces = lax.all_to_all(mine, "tp", 0, 0, tiled=True)
     full_rows = jnp.concatenate([pieces[k, :seq] for k in range(tp)], axis=1).astype(jnp.float32)
-    past = seq + 3 * units
-    lean_full = jnp.concatenate(
-        [
-            pieces[k, past : past + 1].astype(jnp.float32)
-            + pieces[k, past + 1 : past + 2].astype(jnp.float32)
-            for k in range(tp)
-        ],
-        axis=1,
-    )
-    width_total = full_rows.shape[1]
-    dense_weights = from_everyone(pieces[:, seq:past], PLANE).reshape(plane, tp, 3 * units, width)
     routes = pl.pallas_call(
-        routes_kernel, out_shape=shaped((seq, LANES), jnp.float32), name="routes"
+        routes_kernel, out_shape=shaped((seq, LANES), jnp.float32), name="routes", compiler_params=LIMIT
     )(route_ids, route_ids.T, route_logits)
     normed = rms_scale(full_rows, norm_gain_attn).astype(jnp.bfloat16)
     head_out, key_rows, value_rows = attend(
@@ -322,7 +366,6 @@
         lengths,
     )
     head_terms = jnp.dot(head_out, out_weight, preferred_element_type=jnp.float32)
-    head_terms, dense_weights = lax.optimization_barrier((head_terms, dense_weights))
     parts = from_everyone(head_terms, "tp")
     residual, message = pl.pallas_call(
         lambda *refs: mix_kernel(*refs, top=top),
@@ -330,23 +373,33 @@
             shaped((seq, width), jnp.float32),
             shaped((line, seq, width + LANES), jnp.bfloat16),
         ),
-        in_specs=[SCALARS] + [WHOLE] * 5,
+        in_specs=[SCALARS] + [WHOLE] * 4,
         name="mix",
+        compiler_params=LIMIT,
     )(
         lax.axis_index("tp").reshape(1),
-        parts,
-        full_rows,
-        lean_full,
+        near(parts),
+        near(pieces),
         norm_gain_mix[None, :],
-        routes,
+        near(routes),
     )
     seen = lax.all_to_all(message, "ep_0", 0, 0, tiled=True)
+    columns = lax.axis_size("ep_1")
+    held = [pieces[:, seq:past]]
+    for shift in range(1, columns):
+        held.append(
+            lax.ppermute(held[0], "ep_1", [(i, (i + shift) % columns) for i in range(columns)])
+        )
+    own_dense, seen = lax.optimization_barrier((jnp.stack(held), seen))
+    seen = near(seen)
+    other_dense = lax.ppermute(own_dense, "ep_2", [(0, 1), (1, 0)])
     first = (lax.axis_index("ep_0") * plane).reshape(1)
     outward = pl.pallas_call(
         lambda *refs: outward_kernel(*refs, top=top),
         out_shape=shaped((plane, tp, slots + dealt, width), jnp.bfloat16),
         in_specs=[SCALARS, WHOLE],
         name="outward",
+        compiler_params=LIMIT,
     )(first, seen)
     arrived = lax.all_to_all(
         outward.reshape(plane * tp, slots + dealt, width), BLOCK, 0, 0, tiled=True
@@ -359,12 +412,27 @@
         ),
         in_specs=[SCALARS, WHOLE],
         name="weights",
+        compiler_params=LIMIT,
     )(first, seen)
     sent = pl.pallas_call(
         lambda *refs: expert_kernel(*refs, slots=slots),
         out_shape=shaped((plane, tp, slots + dealt, width), jnp.bfloat16),
+        in_specs=[WHOLE] * 3 + [pl.BlockSpec(memory_space=pl.ANY)] * 3,
+        scratch_shapes=[
+            pltpu.VMEM(expert_down.shape, expert_down.dtype),
+            pltpu.VMEM((2, *own_dense.shape), own_dense.dtype),
+            pltpu.SemaphoreType.DMA((3,)),
+        ],
         name="experts",
-    )(arrived, expert_gate, expert_up, expert_down, dense_weights)
+        compiler_params=LIMIT,
+    )(
+        near(arrived),
+        near(expert_gate),
+        near(expert_up),
+        far(expert_down),
+        far(own_dense),
+        far(other_dense),
+    )
     returned = lax.all_to_all(
         sent.reshape(plane * tp, slots + dealt, width), BLOCK, 0, 0, tiled=True
     ).reshape(plane, tp, slots + dealt, width)
@@ -372,7 +440,8 @@
         lambda *refs: inward_kernel(*refs, top=top),
         out_shape=shaped((line, seq, width), jnp.bfloat16),
         name="inward",
-    )(returned, seen, upper, lower)
+        compiler_params=LIMIT,
+    )(near(returned), seen, near(upper), near(lower))
     home = lax.all_to_all(back, "ep_0", 0, 0, tiled=True)
     layer_out = (residual + jnp.sum(home.astype(jnp.float32), axis=0)).astype(jnp.bfloat16)
     return (layer_out, key_rows, value_rows)

time: 144 us -> 125 us (0.87)
  starting transfers between devices: 37.4 us -> 55.4 us
  blocking collectives: 17.7 us -> 0 us
  local copies, waits for them, and re-layouts: 12.6 us -> 5.83 us
  waiting for transfers between devices: 55 us -> 49.5 us
  Pallas kernels: 13.9 us -> 8.55 us
    all_to_all x1 -> x0, blocking collectives: 17.7 us -> none  [body(): lax.all_to_all(outward.reshape(plane * tp, slots + dealt, width), BLOCK,...]
    all_to_all x1, waiting for transfers between devices: 14.5 us -> 0.01 us  [body(): seen = lax.all_to_all(message, 'ep_0', 0, 0, tiled=True)]
    all_to_all x0 -> x2, waiting for transfers between devices: none -> 12.9 us  [the longest x1 9.32 us: body(): lax.all_to_all(outward.reshape(plane * tp, slots + dealt, width), BLOCK,...]
    ppermute x0 -> x4, starting transfers between devices: none -> 12.3 us  [the longest x3 10.2 us: body(): lax.ppermute(held[0], 'ep_1', [(i, (i + shift) % columns) for i in range(...]
    all_to_all x3 -> x1, waiting for transfers between devices: 16.9 us -> 4.79 us  [from_everyone(): return lax.all_to_all(copies, axis, split_axis=0, concat_axis=0, tiled=True)]
    all_to_all x3 -> x1, starting transfers between devices: 13.2 us -> 3.4 us  [from_everyone(): return lax.all_to_all(copies, axis, split_axis=0, concat_axis=0, tiled=True)]
    all_to_all x0 -> x2, starting transfers between devices: none -> 8.63 us  [the longest x1 4.59 us: body(): pieces = lax.all_to_all(mine, 'tp', 0, 0, tiled=True)]
    all_to_all x1, starting transfers between devices: 5.1 us -> 12 us  [body(): home = lax.all_to_all(back, 'ep_0', 0, 0, tiled=True)]
  transfers between devices with their start and end apart: 6 -> 10, of which waited for: 6 -> 8; matrix products, arithmetic and copies ran while one was open for 4% -> 2% of each run, Pallas kernels for 3% -> 1%
where the time goes in v3:
time: 125 us; the launch traced here: 124 us
  starting transfers between devices  55.4 us (44%)
  waiting for transfers between devices  49.5 us (40%)
  Pallas kernels  8.55 us (7%)
  local copies, waits for them, and re-layouts  5.83 us (5%)
  other arithmetic  2.09 us (2%)
  between operations  1.61 us (1%)
  matrix products  1.4 us (1%)
    all_to_all x1, starting transfers between devices, body(): seen = lax.all_to_all(message, 'ep_0', 0, 0, tiled=True)  15.2 us
    all_to_all x1, waiting for transfers between devices, body(): home = lax.all_to_all(back, 'ep_0', 0, 0, tiled=True)  12.8 us
    all_to_all x1, waiting for transfers between devices, body(): lax.all_to_all(sent.reshape(plane * tp, slots + dealt, width), BLOCK, 0,...  12.4 us
    all_to_all x1, starting transfers between devices, body(): home = lax.all_to_all(back, 'ep_0', 0, 0, tiled=True)  12 us
    ppermute x3, starting transfers between devices, body(): lax.ppermute(held[0], 'ep_1', [(i, (i + shift) % columns) for i in range(...  10.2 us
    all_to_all x1, waiting for transfers between devices, body(): lax.all_to_all(outward.reshape(plane * tp, slots + dealt, width), BLOCK,...  9.32 us
    ppermute x3, waiting for transfers between devices, body(): lax.ppermute(held[0], 'ep_1', [(i, (i + shift) % columns) for i in range(...  4.91 us
    all_to_all x1, waiting for transfers between devices, from_everyone(): return lax.all_to_all(copies, axis, split_axis=0, concat_axis=0, tiled=True)  4.79 us
  transfers between devices with their start and end apart: 10, of which 8 were waited for; matrix products, arithmetic and copies ran while one was open for 2% of the time, Pallas kernels for 1%

profile of v3, /device:TPU:32, one launch (start us, length us, event | category | flops | bytes accessed | tf_op | source)
XLA Modules:
  0.0 124.4 jit_solution(6951030747168473051)
XLA Ops:
  0.6 1.5 %opening.1 = bf16[4,72,256]{2,1,0:T(8,128)(2,1)} custom-call(bf16[16,256]{1,0:T(8,128)(2,1)} %hidden_ref.1, bf16[16,256]{1,0:T(8,128)(2,1)} %bitcast.70, bf16[16,256]{1,0:T(8,128)(2,1)} %bitcast.71, bf16[16,256]{1,0:T(8,128)(2,1)} %down_ref.1, f32[1,256]{1,0:T(1,128)} %bitcast.61, f32[1,256]{1,0:T(1,128)} %bitcast.72), custom_call_target="tpu_custom_call" | custom-call | tf_op jit(solution)/shard_map/opening/pallas_call | solution.py:334
  2.2 4.6 %all-to-all-start = ((bf16[4,72,256]{2,1,0:T(8,128)(2,1)}), bf16[4,72,256]{2,1,0:T(8,128)(2,1)S(1)}, u32[]{:S(2)}, u32[]{:S(2)}) async-start(bf16[4,72,256]{2,1,0:T(8,128)(2,1)} %opening.1), calls=%async_computation | async-start | bytes 294912 | tf_op jit(solution)/shard_map/all_to_all | solution.py:349
  6.9 1.5 %copy.29 = bf16[16,256,128]{1,2,0:T(8,128)(2,1)S(1)} copy(bf16[16,256,128]{2,1,0:T(8,128)(2,1)} %param.33) | data formatting | bytes 2097152 | tf_op args[10]
  9.2 3.6 %all-to-all-done.refs_2_ = bf16[4,72,256]{2,1,0:T(8,128)(2,1)S(1)} async-done(((bf16[4,72,256]{2,1,0:T(8,128)(2,1)}), bf16[4,72,256]{2,1,0:T(8,128)(2,1)S(1)}, u32[]{:S(2)}, u32[]{:S(2)}) %all-to-all-start) | async-done | bytes 147488 | tf_op jit(solution)/shard_map/all_to_all | solution.py:349
  12.8 0.1 fusion
  13.0 0.2 fusion.26
  13.3 0.1 mul.206
  13.4 0.2 fusion.27
  13.7 0.1 reduce_sum.57
  13.8 0.1 reduce_sum.55
  14.0 0.2 fusion.8
  14.2 0.2 fusion.11
  14.5 0.1 fusion.5
  14.6 0.1 divide_bitcast_fusion
  14.7 0.2 fusion.9
  15.0 0.7 copy-done.15
  15.6 0.3 multiply_reduce_fusion
  16.0 0.6 copy-done.12
  16.6 0.2 fusion.14
  16.8 0.7 broadcast_in_dim.22
  17.6 3.4 %all-to-all-start.1 = ((f32[4,16,1024]{2,1,0:T(8,128)}), f32[4,16,1024]{2,1,0:T(8,128)S(1)}, u32[]{:S(2)}, u32[]{:S(2)}) async-start(f32[4,16,1024]{2,1,0:T(8,128)} %broadcast_in_dim.22), calls=%async_computation.1 | async-start | bytes 524288 | tf_op jit(solution)/shard_map/all_to_all | solution.py:26
  21.0 0.7 copy-done.3
  21.7 0.1 copy.30.ids_ref
  21.8 0.6 copy-done.11
  22.4 0.4 routes.1.refs_4_
  22.8 4.8 %all-to-all-done.1.refs_1_ = f32[4,16,1024]{2,1,0:T(8,128)S(1)} async-done(((f32[4,16,1024]{2,1,0:T(8,128)}), f32[4,16,1024]{2,1,0:T(8,128)S(1)}, u32[]{:S(2)}, u32[]{:S(2)}) %all-to-all-start.1) | async-done | bytes 262176 | tf_op jit(solution)/shard_map/all_to_all | solution.py:26
  27.6 0.8 mix.1
  28.4 15.2 %all-to-all-start.2 = ((bf16[16,16,384]{2,1,0:T(8,128)(2,1)}), bf16[16,16,384]{2,1,0:T(8,128)(2,1)S(1)}, u32[]{:S(2)}, u32[]{:S(2)}) async-start(bf16[16,16,384]{2,1,0:T(8,128)(2,1)} %get-tuple-element.10), calls=%async_computation.2 | async-start | bytes 393216 | tf_op jit(solution)/shard_map/all_to_all | solution.py:386
  43.7 4.7 %collective-permute-start.2 = (bf16[4,48,256]{2,1,0:T(8,128)(2,1)S(1)}, bf16[4,48,256]{2,1,0:T(8,128)(2,1)S(1)}, u32[]{:S(2)}, u32[]{:S(2)}) collective-permute-start(bf16[4,48,256]{2,1,0:T(8,128)(2,1)S(1)} %get-tuple-element.18), channel_id=1, source_target_pairs={{0,24},{8,0},{16,8},{24,16},{1,25},{9,1},{17,9},{25,17},{2,26},{10... | collective-permute-start | bytes 294920 | tf_op jit(solution)/shard_map/ppermute | solution.py:391
  48.3 2.7 %collective-permute-start.1 = (bf16[4,48,256]{2,1,0:T(8,128)(2,1)S(1)}, bf16[4,48,256]{2,1,0:T(8,128)(2,1)S(1)}, u32[]{:S(2)}, u32[]{:S(2)}) collective-permute-start(bf16[4,48,256]{2,1,0:T(8,128)(2,1)S(1)} %get-tuple-element.18), channel_id=1, source_target_pairs={{0,16},{8,24},{16,0},{24,8},{1,17},{9,25},{17,1},{25,9},{2,18},{10... | collective-permute-start | bytes 294920 | tf_op jit(solution)/shard_map/ppermute | solution.py:391
  51.1 2.8 %collective-permute-start = (bf16[4,48,256]{2,1,0:T(8,128)(2,1)S(1)}, bf16[4,48,256]{2,1,0:T(8,128)(2,1)S(1)}, u32[]{:S(2)}, u32[]{:S(2)}) collective-permute-start(bf16[4,48,256]{2,1,0:T(8,128)(2,1)S(1)} %get-tuple-element.18), channel_id=1, source_target_pairs={{0,8},{8,16},{16,24},{24,0},{1,9},{9,17},{17,25},{25,1},{2,10},{10... | collective-permute-start | bytes 294920 | tf_op jit(solution)/shard_map/ppermute | solution.py:391
  53.9 2.5 %collective-permute-done.1 = bf16[4,48,256]{2,1,0:T(8,128)(2,1)S(1)} collective-permute-done((bf16[4,48,256]{2,1,0:T(8,128)(2,1)S(1)}, bf16[4,48,256]{2,1,0:T(8,128)(2,1)S(1)}, u32[]{:S(2)}, u32[]{:S(2)}) %collective-permute-start.1) | collective-permute-done | bytes 98336 | tf_op jit(solution)/shard_map/ppermute | solution.py:391
  56.4 2.4 %collective-permute-done = bf16[4,48,256]{2,1,0:T(8,128)(2,1)S(1)} collective-permute-done((bf16[4,48,256]{2,1,0:T(8,128)(2,1)S(1)}, bf16[4,48,256]{2,1,0:T(8,128)(2,1)S(1)}, u32[]{:S(2)}, u32[]{:S(2)}) %collective-permute-start) | collective-permute-done | bytes 98336 | tf_op jit(solution)/shard_map/ppermute | solution.py:391
  58.8 1.3 %outward.1 = bf16[8,4,40,256]{3,2,1,0:T(8,128)(2,1)} custom-call(s32[1]{0:T(128)} %bitcast.21.refs_0_, bf16[16,16,384]{2,1,0:T(8,128)(2,1)S(1)} %all-to-all-done.2.refs_1_), custom_call_target="tpu_custom_call" | custom-call | tf_op jit(solution)/shard_map/outward/pallas_call | solution.py:397
  60.2 4.0 %all-to-all-start.3 = ((bf16[32,40,256]{2,1,0:T(8,128)(2,1)}), bf16[32,40,256]{2,1,0:T(8,128)(2,1)S(1)}, u32[]{:S(2)}, u32[]{:S(2)}) async-start(bf16[32,40,256]{2,1,0:T(8,128)(2,1)} %bitcast.26), calls=%async_computation.3 | async-start | bytes 1310720 | tf_op jit(solution)/shard_map/all_to_all | solution.py:404
  64.2 2.1 %collective-permute-start.3 = (bf16[4,4,48,256]{3,2,1,0:T(8,128)(2,1)S(1)}, bf16[4,4,48,256]{3,2,1,0:T(8,128)(2,1)}, u32[]{:S(2)}, u32[]{:S(2)}) collective-permute-start(bf16[4,4,48,256]{3,2,1,0:T(8,128)(2,1)S(1)} %pad_maximum_fusion.refs_4_), channel_id=1, source_target_pairs={{0,4},{4,0},{1,5},{5,1},{2,6},{6,2},{3,7},{7,3},{8,12},{12,8},{9,1... | collective-permute-start | bytes 1179656 | tf_op jit(solution)/shard_map/ppermute | solution.py:395
  66.3 1.6 %collective-permute-done.3.refs_5_ = bf16[4,4,48,256]{3,2,1,0:T(8,128)(2,1)} collective-permute-done((bf16[4,4,48,256]{3,2,1,0:T(8,128)(2,1)S(1)}, bf16[4,4,48,256]{3,2,1,0:T(8,128)(2,1)}, u32[]{:S(2)}, u32[]{:S(2)}) %collective-permute-start.3) | collective-permute-done | bytes 393248 | tf_op jit(solution)/shard_map/ppermute | solution.py:395
  68.0 9.3 %all-to-all-done.3 = bf16[32,40,256]{2,1,0:T(8,128)(2,1)S(1)} async-done(((bf16[32,40,256]{2,1,0:T(8,128)(2,1)}), bf16[32,40,256]{2,1,0:T(8,128)(2,1)S(1)}, u32[]{:S(2)}, u32[]{:S(2)}) %all-to-all-start.3) | async-done | bytes 655392 | tf_op jit(solution)/shard_map/all_to_all | solution.py:404
  77.3 2.9 %experts.1 = bf16[8,4,40,256]{3,2,1,0:T(8,128)(2,1)} custom-call(bf16[8,4,40,256]{3,2,1,0:T(8,128)(2,1)S(1)} %bitcast.58, bf16[1,1024,256]{2,1,0:T(8,128)(2,1)S(1)} %copy-done.1, bf16[1,1024,256]{2,1,0:T(8,128)(2,1)S(1)} %copy-done.2, bf16[1,256,1024]{2,1,0:T(8,128)(2,1)} %refs_3_.1, bf16[4,4,48,256]{3,2,1,0:T(8,128)(2,1)} %copy-done.5, ...), custom_call_target="tpu_custom_call" | custom-call | tf_op jit(solution)/shard_map/experts/pallas_call | solution.py:417
  80.3 3.9 %all-to-all-start.4 = ((bf16[32,40,256]{2,1,0:T(8,128)(2,1)}), bf16[32,40,256]{2,1,0:T(8,128)(2,1)S(1)}, u32[]{:S(2)}, u32[]{:S(2)}) async-start(bf16[32,40,256]{2,1,0:T(8,128)(2,1)} %bitcast.28), calls=%async_computation.4 | async-start | bytes 1310720 | tf_op jit(solution)/shard_map/all_to_all | solution.py:436
  84.2 0.7 weights.1
  84.8 12.4 %all-to-all-done.4 = bf16[32,40,256]{2,1,0:T(8,128)(2,1)S(1)} async-done(((bf16[32,40,256]{2,1,0:T(8,128)(2,1)}), bf16[32,40,256]{2,1,0:T(8,128)(2,1)S(1)}, u32[]{:S(2)}, u32[]{:S(2)}) %all-to-all-start.4) | async-done | bytes 655392 | tf_op jit(solution)/shard_map/all_to_all | solution.py:436
  97.3 0.9 inward.1
  98.2 12.0 %all-to-all-start.5 = ((bf16[16,16,256]{2,1,0:T(8,128)(2,1)}), bf16[16,16,256]{2,1,0:T(8,128)(2,1)S(1)}, u32[]{:S(2)}, u32[]{:S(2)}) async-start(bf16[16,16,256]{2,1,0:T(8,128)(2,1)} %inward.1), calls=%async_computation.5 | async-start | bytes 262144 | tf_op jit(solution)/shard_map/all_to_all | solution.py:445
  110.3 0.1 mul.231
  110.4 0.6 multiply_convert_fusion.2
  111.0 12.8 %all-to-all-done.5 = bf16[16,16,256]{2,1,0:T(8,128)(2,1)S(1)} async-done(((bf16[16,16,256]{2,1,0:T(8,128)(2,1)}), bf16[16,16,256]{2,1,0:T(8,128)(2,1)S(1)}, u32[]{:S(2)}, u32[]{:S(2)}) %all-to-all-start.5) | async-done | bytes 131104 | tf_op jit(solution)/shard_map/all_to_all | solution.py:445
  123.8 0.6 add_convert_fusion
  (51 shorter events, 0.9 us)
Async XLA Ops:
  0.6 14.0 %copy-start = (bf16[16,256,128]{2,1,0:T(8,128)(2,1)S(1)}, bf16[16,256,128]{2,1,0:T(8,128)(2,1)}, u32[]{:S(2)}) copy-start(bf16[16,256,128]{2,1,0:T(8,128)(2,1)} %param.34) | copy-start | bytes 3145732
  2.2 4.6 %copy-start.13 = (s32[16]{0:T(128)S(1)}, s32[16]{0:T(128)}, u32[]{:S(2)}) copy-start(s32[16]{0:T(128)} %param.35) | copy-start | bytes 196
  2.2 10.7 %all-to-all-start = ((bf16[4,72,256]{2,1,0:T(8,128)(2,1)}), bf16[4,72,256]{2,1,0:T(8,128)(2,1)S(1)}, u32[]{:S(2)}, u32[]{:S(2)}) async-start(bf16[4,72,256]{2,1,0:T(8,128)(2,1)} %opening.1), calls=%async_computation | async-start | bytes 294912 | tf_op jit(solution)/shard_map/all_to_all | solution.py:349
  6.8 1.6 %copy-start.14 = (f32[128]{0:T(128)S(1)}, f32[128]{0:T(128)}, u32[]{:S(2)}) copy-start(f32[128]{0:T(128)} %param.29) | copy-start | bytes 1540
  6.8 1.7 %copy-start.16 = (f32[128]{0:T(128)S(1)}, f32[128]{0:T(128)}, u32[]{:S(2)}) copy-start(f32[128]{0:T(128)} %param.28) | copy-start | bytes 1540
  6.8 6.1 %copy-start.6 = (bf16[1024,128]{1,0:T(8,128)(2,1)S(1)}, bf16[1024,128]{1,0:T(8,128)(2,1)}, u32[]{:S(2)}) copy-start(bf16[1024,128]{1,0:T(8,128)(2,1)} %param.26) | copy-start | bytes 786436
  6.9 6.1 %copy-start.9 = (f32[1024]{0:T(1024)S(1)}, f32[1024]{0:T(1024)}, u32[]{:S(2)}) copy-start(f32[1024]{0:T(1024)} %param.24) | copy-start | bytes 12292
  8.4 4.9 %copy-start.7 = (bf16[1024,128]{1,0:T(8,128)(2,1)S(1)}, bf16[1024,128]{1,0:T(8,128)(2,1)}, u32[]{:S(2)}) copy-start(bf16[1024,128]{1,0:T(8,128)(2,1)} %param.25) | copy-start | bytes 786436
  14.7 1.0 copy-start.15
  14.9 1.1 copy-start.8
  16.0 0.9 copy-start.10
  16.0 0.7 copy-start.12
  17.6 10.1 %all-to-all-start.1 = ((f32[4,16,1024]{2,1,0:T(8,128)}), f32[4,16,1024]{2,1,0:T(8,128)S(1)}, u32[]{:S(2)}, u32[]{:S(2)}) async-start(f32[4,16,1024]{2,1,0:T(8,128)} %broadcast_in_dim.22), calls=%async_computation.1 | async-start | bytes 524288 | tf_op jit(solution)/shard_map/all_to_all | solution.py:26
  21.0 0.7 copy-start.3
  21.7 0.7 copy-start.11
  22.8 4.8 %copy-start.4 = (f32[256]{0:T(256)S(1)}, f32[256]{0:T(256)}, u32[]{:S(2)}) copy-start(f32[256]{0:T(256)} %param.36) | copy-start | bytes 3076
  28.4 30.4 %all-to-all-start.2 = ((bf16[16,16,384]{2,1,0:T(8,128)(2,1)}), bf16[16,16,384]{2,1,0:T(8,128)(2,1)S(1)}, u32[]{:S(2)}, u32[]{:S(2)}) async-start(bf16[16,16,384]{2,1,0:T(8,128)(2,1)} %get-tuple-element.10), calls=%async_computation.2 | async-start | bytes 393216 | tf_op jit(solution)/shard_map/all_to_all | solution.py:386
  43.7 10.2 %collective-permute-start.2 = (bf16[4,48,256]{2,1,0:T(8,128)(2,1)S(1)}, bf16[4,48,256]{2,1,0:T(8,128)(2,1)S(1)}, u32[]{:S(2)}, u32[]{:S(2)}) collective-permute-start(bf16[4,48,256]{2,1,0:T(8,128)(2,1)S(1)} %get-tuple-element.18), channel_id=1, source_target_pairs={{0,24},{8,0},{16,8},{24,16},{1,25},{9,1},{17,9},{25,17},{2,26},{10... | collective-permute-start | bytes 294920 | tf_op jit(solution)/shard_map/ppermute | solution.py:391
  48.3 8.0 %collective-permute-start.1 = (bf16[4,48,256]{2,1,0:T(8,128)(2,1)S(1)}, bf16[4,48,256]{2,1,0:T(8,128)(2,1)S(1)}, u32[]{:S(2)}, u32[]{:S(2)}) collective-permute-start(bf16[4,48,256]{2,1,0:T(8,128)(2,1)S(1)} %get-tuple-element.18), channel_id=1, source_target_pairs={{0,16},{8,24},{16,0},{24,8},{1,17},{9,25},{17,1},{25,9},{2,18},{10... | collective-permute-start | bytes 294920 | tf_op jit(solution)/shard_map/ppermute | solution.py:391
  51.1 7.7 %collective-permute-start = (bf16[4,48,256]{2,1,0:T(8,128)(2,1)S(1)}, bf16[4,48,256]{2,1,0:T(8,128)(2,1)S(1)}, u32[]{:S(2)}, u32[]{:S(2)}) collective-permute-start(bf16[4,48,256]{2,1,0:T(8,128)(2,1)S(1)} %get-tuple-element.18), channel_id=1, source_target_pairs={{0,8},{8,16},{16,24},{24,0},{1,9},{9,17},{17,25},{25,1},{2,10},{10... | collective-permute-start | bytes 294920 | tf_op jit(solution)/shard_map/ppermute | solution.py:391
  58.8 5.4 %copy-start.5 = (bf16[4,4,48,256]{3,2,1,0:T(8,128)(2,1)}, bf16[4,4,48,256]{3,2,1,0:T(8,128)(2,1)S(1)}, u32[]{:S(2)}) copy-start(bf16[4,4,48,256]{3,2,1,0:T(8,128)(2,1)S(1)} %pad_maximum_fusion.refs_4_) | copy-start | bytes 1179652
  60.2 17.1 %copy-start.1 = (bf16[1,1024,256]{2,1,0:T(8,128)(2,1)S(1)}, bf16[1,1024,256]{2,1,0:T(8,128)(2,1)}, u32[]{:S(2)}) copy-start(bf16[1,1024,256]{2,1,0:T(8,128)(2,1)} %refs_1_.1) | copy-start | bytes 1572868
  60.2 17.1 %copy-start.2 = (bf16[1,1024,256]{2,1,0:T(8,128)(2,1)S(1)}, bf16[1,1024,256]{2,1,0:T(8,128)(2,1)}, u32[]{:S(2)}) copy-start(bf16[1,1024,256]{2,1,0:T(8,128)(2,1)} %refs_2_.1) | copy-start | bytes 1572868
  60.2 17.1 %all-to-all-start.3 = ((bf16[32,40,256]{2,1,0:T(8,128)(2,1)}), bf16[32,40,256]{2,1,0:T(8,128)(2,1)S(1)}, u32[]{:S(2)}, u32[]{:S(2)}) async-start(bf16[32,40,256]{2,1,0:T(8,128)(2,1)} %bitcast.26), calls=%async_computation.3 | async-start | bytes 1310720 | tf_op jit(solution)/shard_map/all_to_all | solution.py:404
  64.2 3.7 %collective-permute-start.3 = (bf16[4,4,48,256]{3,2,1,0:T(8,128)(2,1)S(1)}, bf16[4,4,48,256]{3,2,1,0:T(8,128)(2,1)}, u32[]{:S(2)}, u32[]{:S(2)}) collective-permute-start(bf16[4,4,48,256]{3,2,1,0:T(8,128)(2,1)S(1)} %pad_maximum_fusion.refs_4_), channel_id=1, source_target_pairs={{0,4},{4,0},{1,5},{5,1},{2,6},{6,2},{3,7},{7,3},{8,12},{12,8},{9,1... | collective-permute-start | bytes 1179656 | tf_op jit(solution)/shard_map/ppermute | solution.py:395
  80.3 17.0 %all-to-all-start.4 = ((bf16[32,40,256]{2,1,0:T(8,128)(2,1)}), bf16[32,40,256]{2,1,0:T(8,128)(2,1)S(1)}, u32[]{:S(2)}, u32[]{:S(2)}) async-start(bf16[32,40,256]{2,1,0:T(8,128)(2,1)} %bitcast.28), calls=%async_computation.4 | async-start | bytes 1310720 | tf_op jit(solution)/shard_map/all_to_all | solution.py:436
  98.2 25.6 %all-to-all-start.5 = ((bf16[16,16,256]{2,1,0:T(8,128)(2,1)}), bf16[16,16,256]{2,1,0:T(8,128)(2,1)S(1)}, u32[]{:S(2)}, u32[]{:S(2)}) async-start(bf16[16,16,256]{2,1,0:T(8,128)(2,1)} %inward.1), calls=%async_computation.5 | async-start | bytes 262144 | tf_op jit(solution)/shard_map/all_to_all | solution.py:445

commit v4 on v3

--- a/solution.py
+++ b/solution.py
@@ -168,7 +168,7 @@
     residual = jnp.concatenate([pieces_ref[k, :seq, :] for k in range(tp)], axis=1)
     residual = residual.astype(jnp.float32)
     for k in range(tp):
-        residual = residual + parts_ref[k]
+        residual = residual + parts_ref[k].astype(jnp.float32)
     ends = [pieces_ref[k, past:, :].astype(jnp.float32) for k in range(tp)]
     lean = jnp.concatenate([end[0:1] + end[1:2] for end in ends], axis=1)
     total = residual.shape[1]
@@ -291,6 +291,12 @@
     branch = notes[:, 3 * top : 3 * top + 1] + notes[:, 3 * top + 1 : 3 * top + 2]
     back = (routed + branch * dense).astype(jnp.bfloat16)
     out_ref[...] = back.reshape(line, seq, width)
+
+
+def doubled(held, step):
+    columns = lax.axis_size("ep_1")
+    other = lax.ppermute(held, "ep_1", [(i, i ^ step) for i in range(columns)])
+    return jnp.concatenate([held, other], axis=0)
 
 
 def shaped(shape, dtype):
@@ -366,7 +372,12 @@
         lengths,
     )
     head_terms = jnp.dot(head_out, out_weight, preferred_element_type=jnp.float32)
-    parts = from_everyone(head_terms, "tp")
+    parts = from_everyone(head_terms.astype(jnp.bfloat16), "tp")
+    columns = lax.axis_size("ep_1")
+    steps = [1 << k for k in reversed(range(columns.bit_length() - 1))]
+    own_dense = pieces[None, :, seq:past]
+    for step in steps[:1]:
+        own_dense = doubled(own_dense, step)
     residual, message = pl.pallas_call(
         lambda *refs: mix_kernel(*refs, top=top),
         out_shape=(
@@ -384,13 +395,9 @@
         near(routes),
     )
     seen = lax.all_to_all(message, "ep_0", 0, 0, tiled=True)
-    columns = lax.axis_size("ep_1")
-    held = [pieces[:, seq:past]]
-    for shift in range(1, columns):
-        held.append(
-            lax.ppermute(held[0], "ep_1", [(i, (i + shift) % columns) for i in range(columns)])
-        )
-    own_dense, seen = lax.optimization_barrier((jnp.stack(held), seen))
+    for step in steps[1:]:
+        own_dense = doubled(own_dense, step)
+    own_dense, seen = lax.optimization_barrier((own_dense, seen))
     seen = near(seen)
     other_dense = lax.ppermute(own_dense, "ep_2", [(0, 1), (1, 0)])
     first = (lax.axis_index("ep_0") * plane).reshape(1)

time: 125 us -> 126 us (level)
  waiting for transfers between devices: 49.5 us -> 51 us
    ppermute x3 -> x2, waiting for transfers between devices: 4.91 us -> 7.23 us  [doubled(): other = lax.ppermute(held, 'ep_1', [(i, i ^ step) for i in range(columns)])]
    ppermute x3 -> x2, starting transfers between devices: 10.2 us -> 8.33 us  [doubled(): other = lax.ppermute(held, 'ep_1', [(i, i ^ step) for i in range(columns)])]
    all_to_all x1, starting transfers between devices: 4.03 us -> 5.42 us  [body(): lax.all_to_all(outward.reshape(plane * tp, slots + dealt, width), BLOCK,...]
  transfers between devices with their start and end apart: 10 -> 9, of which waited for: 8 -> 8; matrix products, arithmetic and copies ran while one was open for 2% -> 2% of each run, Pallas kernels for 1% -> 1%
where the time goes in v4:
time: 126 us; the launch traced here: 125 us
  starting transfers between devices  55 us (44%)
  waiting for transfers between devices  51 us (40%)
  Pallas kernels  8.49 us (7%)
  local copies, waits for them, and re-layouts  5.77 us (5%)
  other arithmetic  2.1 us (2%)
  between operations  1.6 us (1%)
  matrix products  1.4 us (1%)
    all_to_all x1, starting transfers between devices, body(): seen = lax.all_to_all(message, 'ep_0', 0, 0, tiled=True)  15.2 us
    all_to_all x1, waiting for transfers between devices, body(): home = lax.all_to_all(back, 'ep_0', 0, 0, tiled=True)  12.8 us
    all_to_all x1, waiting for transfers between devices, body(): lax.all_to_all(sent.reshape(plane * tp, slots + dealt, width), BLOCK, 0,...  12.4 us
    all_to_all x1, starting transfers between devices, body(): home = lax.all_to_all(back, 'ep_0', 0, 0, tiled=True)  12 us
    all_to_all x1, waiting for transfers between devices, body(): lax.all_to_all(outward.reshape(plane * tp, slots + dealt, width), BLOCK,...  9.32 us
    ppermute x2, starting transfers between devices, doubled(): other = lax.ppermute(held, 'ep_1', [(i, i ^ step) for i in range(columns)])  8.33 us
    ppermute x2, waiting for transfers between devices, doubled(): other = lax.ppermute(held, 'ep_1', [(i, i ^ step) for i in range(columns)])  7.23 us
    all_to_all x1, starting transfers between devices, body(): lax.all_to_all(outward.reshape(plane * tp, slots + dealt, width), BLOCK,...  5.42 us
  transfers between devices with their start and end apart: 9, of which 8 were waited for; matrix products, arithmetic and copies ran while one was open for 2% of the time, Pallas kernels for 1%

profile of v4, /device:TPU:32, one launch (start us, length us, event | category | flops | bytes accessed | tf_op | source)
XLA Modules:
  0.0 125.4 jit_solution(2891959057991822015)
XLA Ops:
  0.6 1.5 %opening.1 = bf16[4,72,256]{2,1,0:T(8,128)(2,1)} custom-call(bf16[16,256]{1,0:T(8,128)(2,1)} %hidden_ref.1, bf16[16,256]{1,0:T(8,128)(2,1)} %bitcast.64, bf16[16,256]{1,0:T(8,128)(2,1)} %bitcast.65, bf16[16,256]{1,0:T(8,128)(2,1)} %down_ref.1, f32[1,256]{1,0:T(1,128)} %bitcast.58, f32[1,256]{1,0:T(1,128)} %bitcast.66), custom_call_target="tpu_custom_call" | custom-call | tf_op jit(solution)/shard_map/opening/pallas_call | solution.py:340
  2.2 4.6 %all-to-all-start = ((bf16[4,72,256]{2,1,0:T(8,128)(2,1)}), bf16[4,72,256]{2,1,0:T(8,128)(2,1)S(1)}, u32[]{:S(2)}, u32[]{:S(2)}) async-start(bf16[4,72,256]{2,1,0:T(8,128)(2,1)} %opening.1), calls=%async_computation | async-start | bytes 294912 | tf_op jit(solution)/shard_map/all_to_all | solution.py:355
  6.9 1.5 %copy.29 = bf16[16,256,128]{1,2,0:T(8,128)(2,1)S(1)} copy(bf16[16,256,128]{2,1,0:T(8,128)(2,1)} %param.33) | data formatting | bytes 2097152 | tf_op args[10]
  9.2 3.6 %all-to-all-done.refs_2_ = bf16[4,72,256]{2,1,0:T(8,128)(2,1)S(1)} async-done(((bf16[4,72,256]{2,1,0:T(8,128)(2,1)}), bf16[4,72,256]{2,1,0:T(8,128)(2,1)S(1)}, u32[]{:S(2)}, u32[]{:S(2)}) %all-to-all-start) | async-done | bytes 147488 | tf_op jit(solution)/shard_map/all_to_all | solution.py:355
  12.8 0.1 fusion
  13.0 0.2 fusion.25
  13.3 0.1 mul.206
  13.4 0.2 fusion.26
  13.6 0.1 reduce_sum.57
  13.7 0.1 reduce_sum.55
  13.9 0.2 fusion.8
  14.2 0.2 fusion.11
  14.5 0.1 fusion.5
  14.6 0.1 divide_bitcast_fusion
  14.7 0.2 fusion.9
  15.0 0.7 copy-done.12
  15.6 0.3 multiply_reduce_fusion
  16.0 0.6 copy-done.15
  16.6 0.2 convolution_convert_fusion
  16.8 0.7 broadcast_in_dim.24
  17.5 3.3 %all-to-all-start.1 = ((bf16[4,16,1024]{2,1,0:T(8,128)(2,1)}), bf16[4,16,1024]{2,1,0:T(8,128)(2,1)S(1)}, u32[]{:S(2)}, u32[]{:S(2)}) async-start(bf16[4,16,1024]{2,1,0:T(8,128)(2,1)} %broadcast_in_dim.24), calls=%async_computation.1 | async-start | bytes 262144 | tf_op jit(solution)/shard_map/all_to_all | solution.py:26
  20.8 0.7 copy-done.3
  21.5 0.1 copy.30.ids_ref
  21.6 0.6 copy-done.9
  22.2 0.1 copy.31.logits_ref
  22.3 0.4 routes.1.refs_4_
  22.7 4.1 %all-to-all-done.1.refs_1_ = bf16[4,16,1024]{2,1,0:T(8,128)(2,1)S(1)} async-done(((bf16[4,16,1024]{2,1,0:T(8,128)(2,1)}), bf16[4,16,1024]{2,1,0:T(8,128)(2,1)S(1)}, u32[]{:S(2)}, u32[]{:S(2)}) %all-to-all-start.1) | async-done | bytes 131104 | tf_op jit(solution)/shard_map/all_to_all | solution.py:26
  26.8 0.8 mix.1
  27.6 15.2 %all-to-all-start.2 = ((bf16[16,16,384]{2,1,0:T(8,128)(2,1)}), bf16[16,16,384]{2,1,0:T(8,128)(2,1)S(1)}, u32[]{:S(2)}, u32[]{:S(2)}) async-start(bf16[16,16,384]{2,1,0:T(8,128)(2,1)} %get-tuple-element.10), calls=%async_computation.2 | async-start | bytes 393216 | tf_op jit(solution)/shard_map/all_to_all | solution.py:397
  42.8 4.9 %collective-permute-start = (bf16[1,4,48,256]{3,2,1,0:T(8,128)(2,1)S(1)}, bf16[1,4,48,256]{3,2,1,0:T(8,128)(2,1)S(1)}, u32[]{:S(2)}, u32[]{:S(2)}) collective-permute-start(bf16[1,4,48,256]{3,2,1,0:T(8,128)(2,1)S(1)} %slice_bitcast_fusion), channel_id=1, source_target_pairs={{0,16},{8,24},{16,0},{24,8},{1,17},{9,25},{17,1},{25,9},{2,18},{10... | collective-permute-start | bytes 294920 | tf_op jit(solution)/shard_map/ppermute | solution.py:298
  47.7 3.1 %collective-permute-done = bf16[1,4,48,256]{3,2,1,0:T(8,128)(2,1)S(1)} collective-permute-done((bf16[1,4,48,256]{3,2,1,0:T(8,128)(2,1)S(1)}, bf16[1,4,48,256]{3,2,1,0:T(8,128)(2,1)S(1)}, u32[]{:S(2)}, u32[]{:S(2)}) %collective-permute-start) | collective-permute-done | bytes 98336 | tf_op jit(solution)/shard_map/ppermute | solution.py:298
  50.8 3.4 %collective-permute-start.1 = (bf16[2,4,48,256]{3,2,1,0:T(8,128)(2,1)S(1)}, bf16[2,4,48,256]{3,2,1,0:T(8,128)(2,1)S(1)}, u32[]{:S(2)}, u32[]{:S(2)}) collective-permute-start(bf16[2,4,48,256]{3,2,1,0:T(8,128)(2,1)S(1)} %pad_maximum_fusion.1), channel_id=1, source_target_pairs={{0,8},{8,0},{16,24},{24,16},{1,9},{9,1},{17,25},{25,17},{2,10},{10... | collective-permute-start | bytes 589832 | tf_op jit(solution)/shard_map/ppermute | solution.py:298
  54.3 4.2 %collective-permute-done.1 = bf16[2,4,48,256]{3,2,1,0:T(8,128)(2,1)S(1)} collective-permute-done((bf16[2,4,48,256]{3,2,1,0:T(8,128)(2,1)S(1)}, bf16[2,4,48,256]{3,2,1,0:T(8,128)(2,1)S(1)}, u32[]{:S(2)}, u32[]{:S(2)}) %collective-permute-start.1) | collective-permute-done | bytes 196640 | tf_op jit(solution)/shard_map/ppermute | solution.py:298
  58.5 1.3 %outward.1 = bf16[8,4,40,256]{3,2,1,0:T(8,128)(2,1)} custom-call(s32[1]{0:T(128)} %bitcast.21.refs_0_, bf16[16,16,384]{2,1,0:T(8,128)(2,1)S(1)} %all-to-all-done.2.refs_1_), custom_call_target="tpu_custom_call" | custom-call | tf_op jit(solution)/shard_map/outward/pallas_call | solution.py:404
  59.8 5.4 %all-to-all-start.3 = ((bf16[32,40,256]{2,1,0:T(8,128)(2,1)}), bf16[32,40,256]{2,1,0:T(8,128)(2,1)S(1)}, u32[]{:S(2)}, u32[]{:S(2)}) async-start(bf16[32,40,256]{2,1,0:T(8,128)(2,1)} %bitcast.23), calls=%async_computation.3 | async-start | bytes 1310720 | tf_op jit(solution)/shard_map/all_to_all | solution.py:411
  65.2 2.2 %collective-permute-start.2 = (bf16[4,4,48,256]{3,2,1,0:T(8,128)(2,1)S(1)}, bf16[4,4,48,256]{3,2,1,0:T(8,128)(2,1)}, u32[]{:S(2)}, u32[]{:S(2)}) collective-permute-start(bf16[4,4,48,256]{3,2,1,0:T(8,128)(2,1)S(1)} %pad_maximum_fusion.refs_4_), channel_id=1, source_target_pairs={{0,4},{4,0},{1,5},{5,1},{2,6},{6,2},{3,7},{7,3},{8,12},{12,8},{9,1... | collective-permute-start | bytes 1179656 | tf_op jit(solution)/shard_map/ppermute | solution.py:402
  67.4 1.6 %collective-permute-done.2.refs_5_ = bf16[4,4,48,256]{3,2,1,0:T(8,128)(2,1)} collective-permute-done((bf16[4,4,48,256]{3,2,1,0:T(8,128)(2,1)S(1)}, bf16[4,4,48,256]{3,2,1,0:T(8,128)(2,1)}, u32[]{:S(2)}, u32[]{:S(2)}) %collective-permute-start.2) | collective-permute-done | bytes 393248 | tf_op jit(solution)/shard_map/ppermute | solution.py:402
  69.0 9.3 %all-to-all-done.3 = bf16[32,40,256]{2,1,0:T(8,128)(2,1)S(1)} async-done(((bf16[32,40,256]{2,1,0:T(8,128)(2,1)}), bf16[32,40,256]{2,1,0:T(8,128)(2,1)S(1)}, u32[]{:S(2)}, u32[]{:S(2)}) %all-to-all-start.3) | async-done | bytes 655392 | tf_op jit(solution)/shard_map/all_to_all | solution.py:411
  78.3 2.9 %experts.1 = bf16[8,4,40,256]{3,2,1,0:T(8,128)(2,1)} custom-call(bf16[8,4,40,256]{3,2,1,0:T(8,128)(2,1)S(1)} %bitcast.55, bf16[1,1024,256]{2,1,0:T(8,128)(2,1)S(1)} %copy-done.1, bf16[1,1024,256]{2,1,0:T(8,128)(2,1)S(1)} %copy-done.2, bf16[1,256,1024]{2,1,0:T(8,128)(2,1)} %refs_3_.1, bf16[4,4,48,256]{3,2,1,0:T(8,128)(2,1)} %copy-done.5, ...), custom_call_target="tpu_custom_call" | custom-call | tf_op jit(solution)/shard_map/experts/pallas_call | solution.py:424
  81.2 3.9 %all-to-all-start.4 = ((bf16[32,40,256]{2,1,0:T(8,128)(2,1)}), bf16[32,40,256]{2,1,0:T(8,128)(2,1)S(1)}, u32[]{:S(2)}, u32[]{:S(2)}) async-start(bf16[32,40,256]{2,1,0:T(8,128)(2,1)} %bitcast.25), calls=%async_computation.4 | async-start | bytes 1310720 | tf_op jit(solution)/shard_map/all_to_all | solution.py:443
  85.1 0.7 weights.1
  85.8 12.4 %all-to-all-done.4 = bf16[32,40,256]{2,1,0:T(8,128)(2,1)S(1)} async-done(((bf16[32,40,256]{2,1,0:T(8,128)(2,1)}), bf16[32,40,256]{2,1,0:T(8,128)(2,1)S(1)}, u32[]{:S(2)}, u32[]{:S(2)}) %all-to-all-start.4) | async-done | bytes 655392 | tf_op jit(solution)/shard_map/all_to_all | solution.py:443
  98.2 0.9 inward.1
  99.1 12.0 %all-to-all-start.5 = ((bf16[16,16,256]{2,1,0:T(8,128)(2,1)}), bf16[16,16,256]{2,1,0:T(8,128)(2,1)S(1)}, u32[]{:S(2)}, u32[]{:S(2)}) async-start(bf16[16,16,256]{2,1,0:T(8,128)(2,1)} %inward.1), calls=%async_computation.5 | async-start | bytes 262144 | tf_op jit(solution)/shard_map/all_to_all | solution.py:452
  111.2 0.1 mul.231
  111.3 0.6 multiply_convert_fusion.2
  111.9 12.8 %all-to-all-done.5 = bf16[16,16,256]{2,1,0:T(8,128)(2,1)S(1)} async-done(((bf16[16,16,256]{2,1,0:T(8,128)(2,1)}), bf16[16,16,256]{2,1,0:T(8,128)(2,1)S(1)}, u32[]{:S(2)}, u32[]{:S(2)}) %all-to-all-start.5) | async-done | bytes 131104 | tf_op jit(solution)/shard_map/all_to_all | solution.py:452
  124.8 0.6 add_convert_fusion
  (50 shorter events, 0.9 us)
Async XLA Ops:
  0.6 14.0 %copy-start = (bf16[16,256,128]{2,1,0:T(8,128)(2,1)S(1)}, bf16[16,256,128]{2,1,0:T(8,128)(2,1)}, u32[]{:S(2)}) copy-start(bf16[16,256,128]{2,1,0:T(8,128)(2,1)} %param.34) | copy-start | bytes 3145732
  2.2 4.6 %copy-start.10 = (s32[16]{0:T(128)S(1)}, s32[16]{0:T(128)}, u32[]{:S(2)}) copy-start(s32[16]{0:T(128)} %param.35) | copy-start | bytes 196
  2.2 10.7 %all-to-all-start = ((bf16[4,72,256]{2,1,0:T(8,128)(2,1)}), bf16[4,72,256]{2,1,0:T(8,128)(2,1)S(1)}, u32[]{:S(2)}, u32[]{:S(2)}) async-start(bf16[4,72,256]{2,1,0:T(8,128)(2,1)} %opening.1), calls=%async_computation | async-start | bytes 294912 | tf_op jit(solution)/shard_map/all_to_all | solution.py:355
  6.8 1.6 %copy-start.11 = (f32[128]{0:T(128)S(1)}, f32[128]{0:T(128)}, u32[]{:S(2)}) copy-start(f32[128]{0:T(128)} %param.29) | copy-start | bytes 1540
  6.8 1.7 %copy-start.14 = (f32[128]{0:T(128)S(1)}, f32[128]{0:T(128)}, u32[]{:S(2)}) copy-start(f32[128]{0:T(128)} %param.28) | copy-start | bytes 1540
  6.8 6.1 %copy-start.6 = (bf16[1024,128]{1,0:T(8,128)(2,1)S(1)}, bf16[1024,128]{1,0:T(8,128)(2,1)}, u32[]{:S(2)}) copy-start(bf16[1024,128]{1,0:T(8,128)(2,1)} %param.26) | copy-start | bytes 786436
  6.8 6.1 %copy-start.8 = (f32[1024]{0:T(1024)S(1)}, f32[1024]{0:T(1024)}, u32[]{:S(2)}) copy-start(f32[1024]{0:T(1024)} %param.24) | copy-start | bytes 12292
  8.4 4.9 %copy-start.7 = (bf16[1024,128]{1,0:T(8,128)(2,1)S(1)}, bf16[1024,128]{1,0:T(8,128)(2,1)}, u32[]{:S(2)}) copy-start(bf16[1024,128]{1,0:T(8,128)(2,1)} %param.25) | copy-start | bytes 786436
  14.7 1.0 copy-start.12
  14.9 1.1 copy-start.13
  15.9 0.9 copy-start.16
  16.0 0.7 copy-start.15
  17.5 9.3 %all-to-all-start.1 = ((bf16[4,16,1024]{2,1,0:T(8,128)(2,1)}), bf16[4,16,1024]{2,1,0:T(8,128)(2,1)S(1)}, u32[]{:S(2)}, u32[]{:S(2)}) async-start(bf16[4,16,1024]{2,1,0:T(8,128)(2,1)} %broadcast_in_dim.24), calls=%async_computation.1 | async-start | bytes 262144 | tf_op jit(solution)/shard_map/all_to_all | solution.py:26
  20.8 0.7 copy-start.3
  21.5 0.7 copy-start.9
  22.7 4.1 %copy-start.4 = (f32[256]{0:T(256)S(1)}, f32[256]{0:T(256)}, u32[]{:S(2)}) copy-start(f32[256]{0:T(256)} %param.36) | copy-start | bytes 3076
  27.6 30.9 %all-to-all-start.2 = ((bf16[16,16,384]{2,1,0:T(8,128)(2,1)}), bf16[16,16,384]{2,1,0:T(8,128)(2,1)S(1)}, u32[]{:S(2)}, u32[]{:S(2)}) async-start(bf16[16,16,384]{2,1,0:T(8,128)(2,1)} %get-tuple-element.10), calls=%async_computation.2 | async-start | bytes 393216 | tf_op jit(solution)/shard_map/all_to_all | solution.py:397
  42.8 8.0 %collective-permute-start = (bf16[1,4,48,256]{3,2,1,0:T(8,128)(2,1)S(1)}, bf16[1,4,48,256]{3,2,1,0:T(8,128)(2,1)S(1)}, u32[]{:S(2)}, u32[]{:S(2)}) collective-permute-start(bf16[1,4,48,256]{3,2,1,0:T(8,128)(2,1)S(1)} %slice_bitcast_fusion), channel_id=1, source_target_pairs={{0,16},{8,24},{16,0},{24,8},{1,17},{9,25},{17,1},{25,9},{2,18},{10... | collective-permute-start | bytes 294920 | tf_op jit(solution)/shard_map/ppermute | solution.py:298
  50.8 7.6 %collective-permute-start.1 = (bf16[2,4,48,256]{3,2,1,0:T(8,128)(2,1)S(1)}, bf16[2,4,48,256]{3,2,1,0:T(8,128)(2,1)S(1)}, u32[]{:S(2)}, u32[]{:S(2)}) collective-permute-start(bf16[2,4,48,256]{3,2,1,0:T(8,128)(2,1)S(1)} %pad_maximum_fusion.1), channel_id=1, source_target_pairs={{0,8},{8,0},{16,24},{24,16},{1,9},{9,1},{17,25},{25,17},{2,10},{10... | collective-permute-start | bytes 589832 | tf_op jit(solution)/shard_map/ppermute | solution.py:298
  58.5 6.8 %copy-start.5 = (bf16[4,4,48,256]{3,2,1,0:T(8,128)(2,1)}, bf16[4,4,48,256]{3,2,1,0:T(8,128)(2,1)S(1)}, u32[]{:S(2)}) copy-start(bf16[4,4,48,256]{3,2,1,0:T(8,128)(2,1)S(1)} %pad_maximum_fusion.refs_4_) | copy-start | bytes 1179652
  59.8 18.5 %copy-start.1 = (bf16[1,1024,256]{2,1,0:T(8,128)(2,1)S(1)}, bf16[1,1024,256]{2,1,0:T(8,128)(2,1)}, u32[]{:S(2)}) copy-start(bf16[1,1024,256]{2,1,0:T(8,128)(2,1)} %refs_1_.1) | copy-start | bytes 1572868
  59.8 18.5 %copy-start.2 = (bf16[1,1024,256]{2,1,0:T(8,128)(2,1)S(1)}, bf16[1,1024,256]{2,1,0:T(8,128)(2,1)}, u32[]{:S(2)}) copy-start(bf16[1,1024,256]{2,1,0:T(8,128)(2,1)} %refs_2_.1) | copy-start | bytes 1572868
  59.8 18.5 %all-to-all-start.3 = ((bf16[32,40,256]{2,1,0:T(8,128)(2,1)}), bf16[32,40,256]{2,1,0:T(8,128)(2,1)S(1)}, u32[]{:S(2)}, u32[]{:S(2)}) async-start(bf16[32,40,256]{2,1,0:T(8,128)(2,1)} %bitcast.23), calls=%async_computation.3 | async-start | bytes 1310720 | tf_op jit(solution)/shard_map/all_to_all | solution.py:411
  65.2 3.7 %collective-permute-start.2 = (bf16[4,4,48,256]{3,2,1,0:T(8,128)(2,1)S(1)}, bf16[4,4,48,256]{3,2,1,0:T(8,128)(2,1)}, u32[]{:S(2)}, u32[]{:S(2)}) collective-permute-start(bf16[4,4,48,256]{3,2,1,0:T(8,128)(2,1)S(1)} %pad_maximum_fusion.refs_4_), channel_id=1, source_target_pairs={{0,4},{4,0},{1,5},{5,1},{2,6},{6,2},{3,7},{7,3},{8,12},{12,8},{9,1... | collective-permute-start | bytes 1179656 | tf_op jit(solution)/shard_map/ppermute | solution.py:402
  81.2 17.0 %all-to-all-start.4 = ((bf16[32,40,256]{2,1,0:T(8,128)(2,1)}), bf16[32,40,256]{2,1,0:T(8,128)(2,1)S(1)}, u32[]{:S(2)}, u32[]{:S(2)}) async-start(bf16[32,40,256]{2,1,0:T(8,128)(2,1)} %bitcast.25), calls=%async_computation.4 | async-start | bytes 1310720 | tf_op jit(solution)/shard_map/all_to_all | solution.py:443
  99.1 25.6 %all-to-all-start.5 = ((bf16[16,16,256]{2,1,0:T(8,128)(2,1)}), bf16[16,16,256]{2,1,0:T(8,128)(2,1)S(1)}, u32[]{:S(2)}, u32[]{:S(2)}) async-start(bf16[16,16,256]{2,1,0:T(8,128)(2,1)} %inward.1), calls=%async_computation.5 | async-start | bytes 262144 | tf_op jit(solution)/shard_map/all_to_all | solution.py:452

commit v5 on v4

--- a/solution.py
+++ b/solution.py
@@ -21,83 +21,10 @@
 OUT_SCALE = 0.2 + 0.6 * math.exp(-0.6)
 
 
-def from_everyone(x, axis):
-    copies = jnp.broadcast_to(x, (lax.axis_size(axis), *x.shape))
-    return lax.all_to_all(copies, axis, split_axis=0, concat_axis=0, tiled=True)
-
-
-def rms_scale(values, scale_gain):
-    mean_square = jnp.mean(values * values, axis=-1, keepdims=True)
-    return values * lax.rsqrt(mean_square + EPSILON) * scale_gain
-
-
 def clamped_unit(gate_pre, up_pre):
     gate_cut = jnp.minimum(gate_pre, CLAMP_LIMIT)
     up_cut = jnp.clip(up_pre, -CLAMP_LIMIT, CLAMP_LIMIT)
     return (up_cut + 1.0) * gate_cut * jax.nn.sigmoid(SWISH_ALPHA * gate_cut)
-
-
-def attend(
-    normed,
-    query_weight,
-    key_weight,
-    value_weight,
-    query_gain,
-    key_gain,
-    lambda_head,
-    sub_gain,
-    cache_key,
-    cache_value,
-    lengths,
-):
-    seq_count = normed.shape[0]
-    head_count = lambda_head.shape[0]
-    qk_size = query_gain.shape[0] // 2
-    val_size = value_weight.shape[1] // head_count
-    cache_len = cache_key.shape[1]
-    scale_factor = qk_size ** (-0.5)
-    query_pre = jnp.dot(normed, query_weight, preferred_element_type=jnp.float32)
-    query_rows = rms_scale(
-        query_pre.reshape(seq_count, head_count, 2, qk_size), query_gain.reshape(2, qk_size)
-    ).astype(jnp.bfloat16)
-    key_pre = jnp.dot(normed, key_weight, preferred_element_type=jnp.float32)
-    key_rows = rms_scale(
-        key_pre.reshape(seq_count, head_count, 2, qk_size), key_gain.reshape(2, qk_size)
-    ).astype(jnp.bfloat16)
-    value_rows = jnp.dot(normed, value_weight, preferred_element_type=jnp.float32).astype(
-        jnp.bfloat16
-    )
-    key_past = cache_key.reshape(seq_count, cache_len, head_count, 2, qk_size)
-    past_score = (
-        jnp.einsum("shmd,sjhmd->shmj", query_rows, key_past, preferred_element_type=jnp.float32)
-        * scale_factor
-    )
-    own_score = (
-        jnp.einsum("shmd,shmd->shm", query_rows, key_rows, preferred_element_type=jnp.float32)
-        * scale_factor
-    )
-    valid_mask = lax.iota(jnp.int32, cache_len)[None, :] < lengths[:, None]
-    past_exp = jnp.where(valid_mask[:, None, None, :], jnp.exp(past_score), 0.0)
-    own_exp = jnp.exp(own_score)
-    denominator = jnp.sum(past_exp, axis=-1) + own_exp
-    past_prob = past_exp / denominator[..., None]
-    own_prob = own_exp / denominator
-    weight_past = (past_prob[:, :, 0] - lambda_head[None, :, None] * past_prob[:, :, 1]).astype(
-        jnp.bfloat16
-    )
-    weight_own = (own_prob[:, :, 0] - lambda_head[None, :] * own_prob[:, :, 1]).astype(jnp.bfloat16)
-    value_past = cache_value.reshape(seq_count, cache_len, head_count, val_size)
-    head_mix = jnp.einsum(
-        "shj,sjhe->she", weight_past, value_past, preferred_element_type=jnp.float32
-    )
-    own_value = value_rows.reshape(seq_count, head_count, val_size).astype(jnp.float32)
-    head_mix = head_mix + weight_own.astype(jnp.float32)[..., None] * own_value
-    head_out = (rms_scale(head_mix, sub_gain) * OUT_SCALE).astype(jnp.bfloat16)
-    return (
-        head_out.reshape(seq_count, head_count * val_size),
-        key_rows.reshape(seq_count, -1),
-        value_rows,
-    )
 
 
 LANES = 128
@@ -110,6 +37,10 @@
 
 def mm(a, b):
     return jnp.dot(a, b, preferred_element_type=jnp.float32)
+
+
+def kept(x):
+    return pltpu.VMEM(x.shape, x.dtype)
 
 
 def far(x):
@@ -160,6 +91,97 @@
         packed = jnp.where(lane == top + k, upper[:, k : k + 1], packed)
         packed = jnp.where(lane == 2 * top + k, lower[:, k : k + 1], packed)
     out_ref[...] = packed
+
+
+def stage_kernel(*refs):
+    count = len(refs) // 2
+    sems = refs[-1]
+    moves = [
+        pltpu.make_async_copy(refs[k], refs[count + k], sems.at[k]) for k in range(count)
+    ]
+    for move in moves:
+        move.start()
+    for move in moves:
+        move.wait()
+
+
+def attend_kernel(
+    lambda_ref,
+    pieces_ref,
+    gain_ref,
+    query_ref,
+    key_ref,
+    value_ref,
+    query_gain_ref,
+    key_gain_ref,
+    sub_ref,
+    out_weight_ref,
+    past_key_ref,
+    past_value_ref,
+    lengths_ref,
+    out_ref,
+    key_rows_ref,
+    value_rows_ref,
+):
+    seq, past, size = past_key_ref.shape
+    tp = pieces_ref.shape[0]
+    half = size // 2
+    full = jnp.concatenate([pieces_ref[k, :seq, :] for k in range(tp)], axis=1)
+    full = full.astype(jnp.float32)
+    square = jnp.sum(full * full, axis=1, keepdims=True) / full.shape[1]
+    normed = (full * lax.rsqrt(square + EPSILON) * gain_ref[...]).astype(jnp.bfloat16)
+    first = lax.broadcasted_iota(jnp.int32, (seq, size), 1) < half
+
+    def halves(x):
+        return (
+            jnp.sum(jnp.where(first, x, 0.0), axis=1, keepdims=True),
+            jnp.sum(jnp.where(first, 0.0, x), axis=1, keepdims=True),
+        )
+
+    def scaled(x, gain):
+        low, high = halves(x * x)
+        inverse = jnp.where(
+            first, lax.rsqrt(low / half + EPSILON), lax.rsqrt(high / half + EPSILON)
+        )
+        return (x * inverse * gain).astype(jnp.bfloat16)
+
+    query = scaled(mm(normed, query_ref[...]), query_gain_ref[...])
+    key = scaled(mm(normed, key_ref[...]), key_gain_ref[...])
+    value = mm(normed, value_ref[...]).astype(jnp.bfloat16)
+    key_rows_ref[...] = key
+    value_rows_ref[...] = value
+    query = query.astype(jnp.float32)
+    both = jnp.concatenate(
+        [jnp.where(first, query, 0.0), jnp.where(first, 0.0, query)], axis=0
+    )
+    row = lax.broadcasted_iota(jnp.int32, (2 * seq, size), 0) % seq
+    score = jnp.zeros((2 * seq, past), jnp.float32)
+    for k in range(seq):
+        mine = jnp.where(row == k, both, 0.0).astype(jnp.bfloat16)
+        score = score + lax.dot_general(
+            mine, past_key_ref[k], ACROSS, preferred_element_type=jnp.float32
+        )
+    scale = half**-0.5
+    valid = lax.broadcasted_iota(jnp.int32, (seq, past), 1) < lengths_ref[...]
+    own = [jnp.exp(o * scale) for o in halves(query * key.astype(jnp.float32))]
+    grown = [
+        jnp.where(valid, jnp.exp(score[m * seq : (m + 1) * seq] * scale), 0.0) for m in range(2)
+    ]
+    total = [jnp.sum(g, axis=1, keepdims=True) + o for g, o in zip(grown, own)]
+    share = lambda_ref[0]
+    weight = (grown[0] / total[0] - share * (grown[1] / total[1])).astype(jnp.bfloat16)
+    weight_own = (own[0] / total[0] - share * (own[1] / total[1])).astype(jnp.bfloat16)
+    weight = weight.astype(jnp.float32)
+    row = lax.broadcasted_iota(jnp.int32, (seq, past), 0)
+    mixed = weight_own.astype(jnp.float32) * value.astype(jnp.float32)
+    for k in range(seq):
+        mine = jnp.where(row == k, weight, 0.0).astype(jnp.bfloat16)
+        mixed = mixed + mm(mine, past_value_ref[k])
+    square = jnp.sum(mixed * mixed, axis=1, keepdims=True) / size
+    head = mixed * lax.rsqrt(square + EPSILON) * sub_ref[...] * OUT_SCALE
+    part = mm(head.astype(jnp.bfloat16), out_weight_ref[...]).astype(jnp.bfloat16)
+    for k in range(tp):
+        out_ref[k] = part
 
 
 def mix_kernel(tp_ref, parts_ref, pieces_ref, gain_ref, routes_ref, res_ref, out_ref, *, top):
@@ -353,26 +375,49 @@
         )
     )
     pieces = lax.all_to_all(mine, "tp", 0, 0, tiled=True)
-    full_rows = jnp.concatenate([pieces[k, :seq] for k in range(tp)], axis=1).astype(jnp.float32)
+    needed = (
+        norm_gain_attn[None, :],
+        query_weight,
+        key_weight,
+        value_weight,
+        query_gain[None, :],
+        key_gain[None, :],
+        sub_gain[None, :],
+        out_weight,
+        cache_key,
+        cache_value,
+        norm_gain_mix[None, :],
+    )
+    *staged, gain_here = pl.pallas_call(
+        stage_kernel,
+        out_shape=tuple(map(kept, needed)),
+        in_specs=[pl.BlockSpec(memory_space=pl.ANY)] * len(needed),
+        out_specs=(WHOLE,) * len(needed),
+        scratch_shapes=[pltpu.SemaphoreType.DMA((len(needed),))],
+        name="stage",
+        compiler_params=LIMIT,
+    )(*map(far, needed))
     routes = pl.pallas_call(
         routes_kernel, out_shape=shaped((seq, LANES), jnp.float32), name="routes", compiler_params=LIMIT
     )(route_ids, route_ids.T, route_logits)
-    normed = rms_scale(full_rows, norm_gain_attn).astype(jnp.bfloat16)
-    head_out, key_rows, value_rows = attend(
-        normed,
-        query_weight,
-        key_weight,
-        value_weight,
-        query_gain,
-        key_gain,
+    size = value_weight.shape[1]
+    parts, key_rows, value_rows = pl.pallas_call(
+        attend_kernel,
+        out_shape=(
+            shaped((tp, seq, out_weight.shape[1]), jnp.bfloat16),
+            shaped((seq, size), jnp.bfloat16),
+            shaped((seq, size), jnp.bfloat16),
+        ),
+        in_specs=[SCALARS] + [WHOLE] * 12,
+        name="attend",
+        compiler_params=LIMIT,
+    )(
         lambda_head,
-        sub_gain,
-        cache_key,
-        cache_value,
-        lengths,
-    )
-    head_terms = jnp.dot(head_out, out_weight, preferred_element_type=jnp.float32)
-    parts = from_everyone(head_terms.astype(jnp.bfloat16), "tp")
+        near(pieces),
+        *map(near, staged),
+        near(lengths[:, None]),
+    )
+    parts = lax.all_to_all(parts, "tp", 0, 0, tiled=True)
     columns = lax.axis_size("ep_1")
     steps = [1 << k for k in reversed(range(columns.bit_length() - 1))]
     own_dense = pieces[None, :, seq:past]
@@ -391,7 +436,7 @@
         lax.axis_index("tp").reshape(1),
         near(parts),
         near(pieces),
-        norm_gain_mix[None, :],
+        near(gain_here),
         near(routes),
     )
     seen = lax.all_to_all(message, "ep_0", 0, 0, tiled=True)

time: 126 us -> 123 us (0.976)
  blocking collectives: 0 us -> 25.4 us
  waiting for transfers between devices: 51 us -> 37.3 us
  starting transfers between devices: 55 us -> 42.8 us
  local copies, waits for them, and re-layouts: 5.77 us -> 2.2 us
  Pallas kernels: 8.49 us -> 12 us
  other arithmetic: 2.1 us -> 0.69 us
  matrix products: 1.4 us -> 0 us
    all_to_all x0 -> x1, blocking collectives: none -> 25.4 us  [body(): home = lax.all_to_all(back, 'ep_0', 0, 0, tiled=True)]
    all_to_all x2 -> x1, waiting for transfers between devices: 16.9 us -> 4.1 us  [body(): parts = lax.all_to_all(parts, 'tp', 0, 0, tiled=True)]
    all_to_all x2 -> x1, starting transfers between devices: 15.3 us -> 3.32 us  [body(): parts = lax.all_to_all(parts, 'tp', 0, 0, tiled=True)]
    pallas_call x0 -> x2, Pallas kernels: none -> 4.27 us  [the longest x1 2.25 us: body(): pl.pallas_call(attend_kernel, out_shape=(shaped((tp, seq, out_weight.shap...]
    unnamed x37 -> x16, local copies, waits for them, and re-layouts: 4.36 us -> 2.11 us
    dot_general x6 -> x0, matrix products: 1.4 us -> none  [the longest x1 0.31 us: attend(): jnp.dot(normed, value_weight, preferred_element_type=jnp.float32)]
  transfers between devices with their start and end apart: 9 -> 8, of which waited for: 8 -> 7; matrix products, arithmetic and copies ran while one was open for 2% -> 0% of each run, Pallas kernels for 1% -> 3%
where the time goes in v5:
time: 123 us; the launch traced here: 122 us
  starting transfers between devices  42.8 us (35%)
  waiting for transfers between devices  37.3 us (30%)
  blocking collectives  25.4 us (21%)
  Pallas kernels  12 us (10%)
  local copies, waits for them, and re-layouts  2.2 us (2%)
  between operations  1.44 us (1%)
    all_to_all x1, blocking collectives, body(): home = lax.all_to_all(back, 'ep_0', 0, 0, tiled=True)  25.4 us
    all_to_all x1, starting transfers between devices, body(): seen = lax.all_to_all(message, 'ep_0', 0, 0, tiled=True)  15.2 us
    all_to_all x1, waiting for transfers between devices, body(): lax.all_to_all(sent.reshape(plane * tp, slots + dealt, width), BLOCK, 0,...  12.4 us
    all_to_all x1, waiting for transfers between devices, body(): lax.all_to_all(outward.reshape(plane * tp, slots + dealt, width), BLOCK,...  9.45 us
    ppermute x2, starting transfers between devices, doubled(): other = lax.ppermute(held, 'ep_1', [(i, i ^ step) for i in range(columns)])  8.34 us
    ppermute x2, waiting for transfers between devices, doubled(): other = lax.ppermute(held, 'ep_1', [(i, i ^ step) for i in range(columns)])  7.22 us
    all_to_all x1, starting transfers between devices, body(): lax.all_to_all(outward.reshape(plane * tp, slots + dealt, width), BLOCK,...  5.42 us
    all_to_all x1, starting transfers between devices, body(): pieces = lax.all_to_all(mine, 'tp', 0, 0, tiled=True)  4.46 us
  transfers between devices with their start and end apart: 8, of which 7 were waited for; matrix products, arithmetic and copies ran while one was open for 0% of the time, Pallas kernels for 3%

profile of v5, /device:TPU:32, one launch (start us, length us, event | category | flops | bytes accessed | tf_op | source)
XLA Modules:
  0.0 121.9 jit_solution(13788064313934305379)
XLA Ops:
  0.6 1.4 %opening.1 = bf16[4,72,256]{2,1,0:T(8,128)(2,1)} custom-call(bf16[16,256]{1,0:T(8,128)(2,1)} %hidden_ref.1, bf16[16,256]{1,0:T(8,128)(2,1)} %bitcast.21, bf16[16,256]{1,0:T(8,128)(2,1)} %bitcast.22, bf16[16,256]{1,0:T(8,128)(2,1)} %down_ref.1, f32[1,256]{1,0:T(1,128)} %bitcast.24, f32[1,256]{1,0:T(1,128)} %bitcast.26), custom_call_target="tpu_custom_call" | custom-call | tf_op jit(solution)/shard_map/opening/pallas_call | solution.py:362
  2.1 4.5 %all-to-all-start = ((bf16[4,72,256]{2,1,0:T(8,128)(2,1)}), bf16[4,72,256]{2,1,0:T(8,128)(2,1)S(1)}, u32[]{:S(2)}, u32[]{:S(2)}) async-start(bf16[4,72,256]{2,1,0:T(8,128)(2,1)} %opening.1), calls=%async_computation | async-start | bytes 294912 | tf_op jit(solution)/shard_map/all_to_all | solution.py:377
  7.2 0.0 copy-start.6
  7.2 0.6 copy-done.6
  7.8 0.1 copy.26.lengths_ref
  7.9 2.0 %stage.1 = (f32[1,1024]{1,0:T(1,128)S(1)}, bf16[1024,128]{1,0:T(8,128)(2,1)S(1)}, bf16[1024,128]{1,0:T(8,128)(2,1)S(1)}, bf16[1024,128]{1,0:T(8,128)(2,1)S(1)}, ...) custom-call(f32[1,1024]{1,0:T(1,128)} %bitcast.23, ...), custom_call_target="tpu_custom_call" | custom-call | tf_op jit(solution)/shard_map/stage/pallas_call | solution.py:391
  10.0 2.6 %all-to-all-done.pieces_ref.refs_2_ = bf16[4,72,256]{2,1,0:T(8,128)(2,1)S(1)} async-done(((bf16[4,72,256]{2,1,0:T(8,128)(2,1)}), bf16[4,72,256]{2,1,0:T(8,128)(2,1)S(1)}, u32[]{:S(2)}, u32[]{:S(2)}) %all-to-all-start) | async-done | bytes 147488 | tf_op jit(solution)/shard_map/all_to_all | solution.py:377
  12.6 2.2 %attend.1 = (bf16[4,16,1024]{2,1,0:T(8,128)(2,1)}, bf16[16,128]{1,0:T(8,128)(2,1)}, bf16[16,128]{1,0:T(8,128)(2,1)}) custom-call(f32[1]{0:T(128)S(6)} %copy.29.lambda_ref, bf16[4,72,256]{2,1,0:T(8,128)(2,1)S(1)} %all-to-all-done.pieces_ref.refs_2_, f32[1,1024]{1,0:T(1,128)S(1)} %get-tuple-element.23.gain_ref, ...), custom_call_target="tpu_custom_call" | custom-call | tf_op jit(solution)/shard_map/attend/pallas_call | solution.py:404
  14.8 3.3 %all-to-all-start.1 = ((bf16[4,16,1024]{2,1,0:T(8,128)(2,1)}), bf16[4,16,1024]{2,1,0:T(8,128)(2,1)S(1)}, u32[]{:S(2)}, u32[]{:S(2)}) async-start(bf16[4,16,1024]{2,1,0:T(8,128)(2,1)} %get-tuple-element.33), calls=%async_computation.1 | async-start | bytes 262144 | tf_op jit(solution)/shard_map/all_to_all | solution.py:420
  18.2 0.0 copy-start.2
  18.2 0.7 copy-done.2
  18.9 0.0 copy-start.5
  18.9 0.1 copy.27.ids_ref
  19.0 0.6 copy-done.5
  19.6 0.1 copy.28.logits_ref
  19.6 0.4 routes.1.refs_4_
  20.0 4.1 %all-to-all-done.1.refs_1_ = bf16[4,16,1024]{2,1,0:T(8,128)(2,1)S(1)} async-done(((bf16[4,16,1024]{2,1,0:T(8,128)(2,1)}), bf16[4,16,1024]{2,1,0:T(8,128)(2,1)S(1)}, u32[]{:S(2)}, u32[]{:S(2)}) %all-to-all-start.1) | async-done | bytes 131104 | tf_op jit(solution)/shard_map/all_to_all | solution.py:420
  24.1 0.8 mix.1
  24.9 15.2 %all-to-all-start.2 = ((bf16[16,16,384]{2,1,0:T(8,128)(2,1)}), bf16[16,16,384]{2,1,0:T(8,128)(2,1)S(1)}, u32[]{:S(2)}, u32[]{:S(2)}) async-start(bf16[16,16,384]{2,1,0:T(8,128)(2,1)} %get-tuple-element.36), calls=%async_computation.2 | async-start | bytes 393216 | tf_op jit(solution)/shard_map/all_to_all | solution.py:442
  40.1 4.9 %collective-permute-start = (bf16[1,4,48,256]{3,2,1,0:T(8,128)(2,1)S(1)}, bf16[1,4,48,256]{3,2,1,0:T(8,128)(2,1)S(1)}, u32[]{:S(2)}, u32[]{:S(2)}) collective-permute-start(bf16[1,4,48,256]{3,2,1,0:T(8,128)(2,1)S(1)} %slice_bitcast_fusion), channel_id=1, source_target_pairs={{0,16},{8,24},{16,0},{24,8},{1,17},{9,25},{17,1},{25,9},{2,18},{10... | collective-permute-start | bytes 294920 | tf_op jit(solution)/shard_map/ppermute | solution.py:320
  45.1 3.1 %collective-permute-done = bf16[1,4,48,256]{3,2,1,0:T(8,128)(2,1)S(1)} collective-permute-done((bf16[1,4,48,256]{3,2,1,0:T(8,128)(2,1)S(1)}, bf16[1,4,48,256]{3,2,1,0:T(8,128)(2,1)S(1)}, u32[]{:S(2)}, u32[]{:S(2)}) %collective-permute-start) | collective-permute-done | bytes 98336 | tf_op jit(solution)/shard_map/ppermute | solution.py:320
  48.2 3.4 %collective-permute-start.1 = (bf16[2,4,48,256]{3,2,1,0:T(8,128)(2,1)S(1)}, bf16[2,4,48,256]{3,2,1,0:T(8,128)(2,1)S(1)}, u32[]{:S(2)}, u32[]{:S(2)}) collective-permute-start(bf16[2,4,48,256]{3,2,1,0:T(8,128)(2,1)S(1)} %pad_maximum_fusion.1), channel_id=1, source_target_pairs={{0,8},{8,0},{16,24},{24,16},{1,9},{9,1},{17,25},{25,17},{2,10},{10... | collective-permute-start | bytes 589832 | tf_op jit(solution)/shard_map/ppermute | solution.py:320
  51.6 4.2 %collective-permute-done.1 = bf16[2,4,48,256]{3,2,1,0:T(8,128)(2,1)S(1)} collective-permute-done((bf16[2,4,48,256]{3,2,1,0:T(8,128)(2,1)S(1)}, bf16[2,4,48,256]{3,2,1,0:T(8,128)(2,1)S(1)}, u32[]{:S(2)}, u32[]{:S(2)}) %collective-permute-start.1) | collective-permute-done | bytes 196640 | tf_op jit(solution)/shard_map/ppermute | solution.py:320
  55.8 0.0 copy-start.3
  55.8 0.0 all-to-all-done.2.refs_1_
  55.8 1.3 %outward.1 = bf16[8,4,40,256]{3,2,1,0:T(8,128)(2,1)} custom-call(s32[1]{0:T(128)} %bitcast.11.refs_0_, bf16[16,16,384]{2,1,0:T(8,128)(2,1)S(1)} %all-to-all-done.2.refs_1_), custom_call_target="tpu_custom_call" | custom-call | tf_op jit(solution)/shard_map/outward/pallas_call | solution.py:449
  57.1 0.0 copy-start
  57.1 0.0 copy-start.1
  57.1 5.4 %all-to-all-start.3 = ((bf16[32,40,256]{2,1,0:T(8,128)(2,1)}), bf16[32,40,256]{2,1,0:T(8,128)(2,1)S(1)}, u32[]{:S(2)}, u32[]{:S(2)}) async-start(bf16[32,40,256]{2,1,0:T(8,128)(2,1)} %bitcast.13), calls=%async_computation.3 | async-start | bytes 1310720 | tf_op jit(solution)/shard_map/all_to_all | solution.py:456
  62.6 0.0 copy-done.3
  62.6 2.2 %collective-permute-start.2 = (bf16[4,4,48,256]{3,2,1,0:T(8,128)(2,1)S(1)}, bf16[4,4,48,256]{3,2,1,0:T(8,128)(2,1)S(1)}, u32[]{:S(2)}, u32[]{:S(2)}) collective-permute-start(bf16[4,4,48,256]{3,2,1,0:T(8,128)(2,1)S(1)} %pad_maximum_fusion.refs_4_), channel_id=1, source_target_pairs={{0,4},{4,0},{1,5},{5,1},{2,6},{6,2},{3,7},{7,3},{8,12},{12,8},{9,1... | collective-permute-start | bytes 1179656 | tf_op jit(solution)/shard_map/ppermute | solution.py:447
  64.8 1.4 %collective-permute-done.2.refs_5_ = bf16[4,4,48,256]{3,2,1,0:T(8,128)(2,1)S(1)} collective-permute-done((bf16[4,4,48,256]{3,2,1,0:T(8,128)(2,1)S(1)}, bf16[4,4,48,256]{3,2,1,0:T(8,128)(2,1)S(1)}, u32[]{:S(2)}, u32[]{:S(2)}) %collective-permute-start.2) | collective-permute-done | bytes 393248 | tf_op jit(solution)/shard_map/ppermute | solution.py:447
  66.2 0.0 copy-start.4
  66.2 9.5 %all-to-all-done.3 = bf16[32,40,256]{2,1,0:T(8,128)(2,1)S(1)} async-done(((bf16[32,40,256]{2,1,0:T(8,128)(2,1)}), bf16[32,40,256]{2,1,0:T(8,128)(2,1)S(1)}, u32[]{:S(2)}, u32[]{:S(2)}) %all-to-all-start.3) | async-done | bytes 655392 | tf_op jit(solution)/shard_map/all_to_all | solution.py:456
  75.6 0.0 copy-done.4
  75.7 0.0 copy-done
  75.7 0.0 copy-done.1
  75.7 2.9 %experts.1 = bf16[8,4,40,256]{3,2,1,0:T(8,128)(2,1)} custom-call(bf16[8,4,40,256]{3,2,1,0:T(8,128)(2,1)S(1)} %bitcast.18, bf16[1,1024,256]{2,1,0:T(8,128)(2,1)S(1)} %copy-done, bf16[1,1024,256]{2,1,0:T(8,128)(2,1)S(1)} %copy-done.1, bf16[1,256,1024]{2,1,0:T(8,128)(2,1)} %refs_3_.3, bf16[4,4,48,256]{3,2,1,0:T(8,128)(2,1)} %copy-done.3, ...), custom_call_target="tpu_custom_call" | custom-call | tf_op jit(solution)/shard_map/experts/pallas_call | solution.py:469
  78.6 3.9 %all-to-all-start.4 = ((bf16[32,40,256]{2,1,0:T(8,128)(2,1)}), bf16[32,40,256]{2,1,0:T(8,128)(2,1)S(1)}, u32[]{:S(2)}, u32[]{:S(2)}) async-start(bf16[32,40,256]{2,1,0:T(8,128)(2,1)} %bitcast.15), calls=%async_computation.4 | async-start | bytes 1310720 | tf_op jit(solution)/shard_map/all_to_all | solution.py:488
  82.5 0.7 weights.1
  83.2 12.4 %all-to-all-done.4 = bf16[32,40,256]{2,1,0:T(8,128)(2,1)S(1)} async-done(((bf16[32,40,256]{2,1,0:T(8,128)(2,1)}), bf16[32,40,256]{2,1,0:T(8,128)(2,1)S(1)}, u32[]{:S(2)}, u32[]{:S(2)}) %all-to-all-start.4) | async-done | bytes 655392 | tf_op jit(solution)/shard_map/all_to_all | solution.py:488
  95.6 0.3 inward.1
  95.9 25.4 %all_to_all.30 = bf16[16,16,256]{2,1,0:T(8,128)(2,1)S(1)} all-to-all(bf16[16,16,256]{2,1,0:T(8,128)(2,1)S(1)} %inward.1), channel_id=1, replica_groups=mesh['ep_0'=16,'ep_1'=4,'ep_2'=2,'tp'=4] {'ep_0'}, dimensions={0} | all-to-all | bytes 262144 | tf_op jit(solution)/shard_map/all_to_all | solution.py:497
  121.3 0.6 add_convert_fusion
  (4 shorter events, 0.1 us)
Async XLA Ops:
  2.1 10.5 %all-to-all-start = ((bf16[4,72,256]{2,1,0:T(8,128)(2,1)}), bf16[4,72,256]{2,1,0:T(8,128)(2,1)S(1)}, u32[]{:S(2)}, u32[]{:S(2)}) async-start(bf16[4,72,256]{2,1,0:T(8,128)(2,1)} %opening.1), calls=%async_computation | async-start | bytes 294912 | tf_op jit(solution)/shard_map/all_to_all | solution.py:377
  7.2 0.7 copy-start.6
  14.8 9.3 %all-to-all-start.1 = ((bf16[4,16,1024]{2,1,0:T(8,128)(2,1)}), bf16[4,16,1024]{2,1,0:T(8,128)(2,1)S(1)}, u32[]{:S(2)}, u32[]{:S(2)}) async-start(bf16[4,16,1024]{2,1,0:T(8,128)(2,1)} %get-tuple-element.33), calls=%async_computation.1 | async-start | bytes 262144 | tf_op jit(solution)/shard_map/all_to_all | solution.py:420
  18.2 0.7 copy-start.2
  18.9 0.7 copy-start.5
  24.9 30.9 %all-to-all-start.2 = ((bf16[16,16,384]{2,1,0:T(8,128)(2,1)}), bf16[16,16,384]{2,1,0:T(8,128)(2,1)S(1)}, u32[]{:S(2)}, u32[]{:S(2)}) async-start(bf16[16,16,384]{2,1,0:T(8,128)(2,1)} %get-tuple-element.36), calls=%async_computation.2 | async-start | bytes 393216 | tf_op jit(solution)/shard_map/all_to_all | solution.py:442
  40.1 8.0 %collective-permute-start = (bf16[1,4,48,256]{3,2,1,0:T(8,128)(2,1)S(1)}, bf16[1,4,48,256]{3,2,1,0:T(8,128)(2,1)S(1)}, u32[]{:S(2)}, u32[]{:S(2)}) collective-permute-start(bf16[1,4,48,256]{3,2,1,0:T(8,128)(2,1)S(1)} %slice_bitcast_fusion), channel_id=1, source_target_pairs={{0,16},{8,24},{16,0},{24,8},{1,17},{9,25},{17,1},{25,9},{2,18},{10... | collective-permute-start | bytes 294920 | tf_op jit(solution)/shard_map/ppermute | solution.py:320
  48.2 7.6 %collective-permute-start.1 = (bf16[2,4,48,256]{3,2,1,0:T(8,128)(2,1)S(1)}, bf16[2,4,48,256]{3,2,1,0:T(8,128)(2,1)S(1)}, u32[]{:S(2)}, u32[]{:S(2)}) collective-permute-start(bf16[2,4,48,256]{3,2,1,0:T(8,128)(2,1)S(1)} %pad_maximum_fusion.1), channel_id=1, source_target_pairs={{0,8},{8,0},{16,24},{24,16},{1,9},{9,1},{17,25},{25,17},{2,10},{10... | collective-permute-start | bytes 589832 | tf_op jit(solution)/shard_map/ppermute | solution.py:320
  55.8 6.8 %copy-start.3 = (bf16[4,4,48,256]{3,2,1,0:T(8,128)(2,1)}, bf16[4,4,48,256]{3,2,1,0:T(8,128)(2,1)S(1)}, u32[]{:S(2)}) copy-start(bf16[4,4,48,256]{3,2,1,0:T(8,128)(2,1)S(1)} %pad_maximum_fusion.refs_4_) | copy-start | bytes 1179652
  57.1 18.5 %copy-start = (bf16[1,1024,256]{2,1,0:T(8,128)(2,1)S(1)}, bf16[1,1024,256]{2,1,0:T(8,128)(2,1)}, u32[]{:S(2)}) copy-start(bf16[1,1024,256]{2,1,0:T(8,128)(2,1)} %refs_1_.3) | copy-start | bytes 1572868
  57.1 18.5 %copy-start.1 = (bf16[1,1024,256]{2,1,0:T(8,128)(2,1)S(1)}, bf16[1,1024,256]{2,1,0:T(8,128)(2,1)}, u32[]{:S(2)}) copy-start(bf16[1,1024,256]{2,1,0:T(8,128)(2,1)} %refs_2_.3) | copy-start | bytes 1572868
  57.1 18.5 %all-to-all-start.3 = ((bf16[32,40,256]{2,1,0:T(8,128)(2,1)}), bf16[32,40,256]{2,1,0:T(8,128)(2,1)S(1)}, u32[]{:S(2)}, u32[]{:S(2)}) async-start(bf16[32,40,256]{2,1,0:T(8,128)(2,1)} %bitcast.13), calls=%async_computation.3 | async-start | bytes 1310720 | tf_op jit(solution)/shard_map/all_to_all | solution.py:456
  62.6 3.6 %collective-permute-start.2 = (bf16[4,4,48,256]{3,2,1,0:T(8,128)(2,1)S(1)}, bf16[4,4,48,256]{3,2,1,0:T(8,128)(2,1)S(1)}, u32[]{:S(2)}, u32[]{:S(2)}) collective-permute-start(bf16[4,4,48,256]{3,2,1,0:T(8,128)(2,1)S(1)} %pad_maximum_fusion.refs_4_), channel_id=1, source_target_pairs={{0,4},{4,0},{1,5},{5,1},{2,6},{6,2},{3,7},{7,3},{8,12},{12,8},{9,1... | collective-permute-start | bytes 1179656 | tf_op jit(solution)/shard_map/ppermute | solution.py:447
  66.2 9.5 %copy-start.4 = (bf16[4,4,48,256]{3,2,1,0:T(8,128)(2,1)}, bf16[4,4,48,256]{3,2,1,0:T(8,128)(2,1)S(1)}, u32[]{:S(2)}) copy-start(bf16[4,4,48,256]{3,2,1,0:T(8,128)(2,1)S(1)} %collective-permute-done.2.refs_5_) | copy-start | bytes 1179652
  78.6 17.0 %all-to-all-start.4 = ((bf16[32,40,256]{2,1,0:T(8,128)(2,1)}), bf16[32,40,256]{2,1,0:T(8,128)(2,1)S(1)}, u32[]{:S(2)}, u32[]{:S(2)}) async-start(bf16[32,40,256]{2,1,0:T(8,128)(2,1)} %bitcast.15), calls=%async_computation.4 | async-start | bytes 1310720 | tf_op jit(solution)/shard_map/all_to_all | solution.py:488
